TPU v7x, 512 devices: a whole 4x8x8 slice. The times are simulated.
512 devices in a mesh: rep: 2 (over z_hi), fs: 32 (over z_lo, y), tp: 8 (over x, core).
Axes of the slice: x: 4, y: 8, z: 8 (z_hi: 2, z_lo: 4; z = z_hi * 4 + z_lo), core: 2. Of those that a mesh axis runs over, the one named last changes fastest.
Arguments:
- states: bfloat16 [24576, 2048], P(('rep', 'fs'), 'tp'), may hold values from -6 to 6
- mix_gain: float32 [2048], replicated, may hold values from 0.1 to 1.9
- w_value: bfloat16 [2048, 2048], P('fs', 'tp'), may hold values from -1 to 1
- w_gate: bfloat16 [2048, 2048], P('fs', 'tp'), may hold values from -0.125 to 0.125
- conv_kernel: float32 [31, 2048], replicated, may hold values from -1 to 1
- chan_gain: float32 [2048], replicated, may hold values from 0.1 to 1.9
- w_mix_out: bfloat16 [2048, 2048], P('fs', 'tp'), may hold values from -0.125 to 0.125
- mlp_gain: float32 [2048], replicated, may hold values from 0.1 to 1.9
- w_up: bfloat16 [2048, 6144], P('fs', 'tp'), may hold values from -0.125 to 0.125
- w_down_t: bfloat16 [2048, 6144], P('fs', 'tp'), may hold values from -0.078125 to 0.078125
Outputs:
- layer_out: bfloat16 [24576, 2048], P(('rep', 'fs'), 'tp')
All inputs are finite; a program needn't handle non-finite values.
Results may differ from a plain program's by a relative error of at most 0.017.
Values may be sent and summed in bfloat16 or wider, within the bound.
No kernel may reach another device: no remote copies, remote signals or barrier semaphores. Data moves between devices by JAX's collectives and lax.ppermute only.
A program may use at most 64 MiB of HBM per device.

v0:
```python
import jax
import jax.numpy as jnp
from jax import lax
from jax.experimental import pallas as pl
from jax.experimental.pallas import tpu as pltpu
from jax.sharding import Mesh
from jax.sharding import PartitionSpec as P

D = 2048
KWIDTH = 31
LENGTH = 128
EPS = 1e-06
TP = ("x", "c")
SWAP = [(0, 1), (1, 0)]


MIB = 1 << 20
LANES = 128
LATE = 256


def times_t(left, right):
    return lax.dot_general(
        left, right, (((1,), (1,)), ((), ())), preferred_element_type=jnp.float32
    )


def pack_kernel(value_ref, gate_ref, out_ref, up_ref, down_ref, early_ref, late_ref):
    width, first = value_ref.shape[1], up_ref.shape[1] - LATE
    at = 0
    for ref, count in ((value_ref, width), (gate_ref, width), (up_ref, first), (down_ref, first)):
        early_ref[:, at : at + count] = ref[:, :count]
        at += count
    for copy in range(late_ref.shape[0]):
        late_ref[copy, :, :width] = out_ref[...]
        late_ref[copy, :, width : width + LATE] = up_ref[:, first:]
        late_ref[copy, :, width + LATE :] = down_ref[:, first:]


def packed(w_value, w_gate, w_mix_out, w_up, w_down_t):
    rows, width = w_value.shape
    first = w_up.shape[1] - LATE
    return pl.pallas_call(
        pack_kernel,
        out_shape=(
            jax.ShapeDtypeStruct((rows, 2 * (width + first)), jnp.bfloat16),
            jax.ShapeDtypeStruct((lax.axis_size("y"), rows, width + 2 * LATE), jnp.bfloat16),
        ),
        compiler_params=pltpu.CompilerParams(vmem_limit_bytes=60 * MIB),
        cost_estimate=pl.CostEstimate(flops=0, bytes_accessed=MIB, transcendentals=0),
        name="pack",
    )(w_value, w_gate, w_mix_out, w_up, w_down_t)


def over_y(run):
    return lax.all_gather(run, "y", axis=1, tiled=True)


def over_z(slab):
    half = slab.shape[0] // 2

    def from_z(piece, step):
        return lax.ppermute(piece, ("rep", "zl"), [((i + step) % 8, i) for i in range(8)])

    return [slab, from_z(slab, 1), from_z(slab[:half], 2), from_z(slab[half:], -2), from_z(slab, -1)]


def gate_kernel(x_ref, taps_ref, weight_ref, filtered_ref, sums_ref, padded_ref, held_ref, sems):
    count, depth, width = held_ref.shape[0], held_ref.shape[1], held_ref.shape[2] // 2
    copies = [
        pltpu.make_async_copy(weight_ref.at[z, :, : 2 * width], held_ref.at[z], sems.at[z])
        for z in range(count)
    ]
    for copy in copies:
        copy.start()
    value, gate = 0.0, 0.0
    for z, copy in enumerate(copies):
        copy.wait()
        x = x_ref[:, z * depth : (z + 1) * depth]
        value += jnp.dot(x, held_ref[z, :, :width], preferred_element_type=jnp.float32)
        gate += jnp.dot(x, held_ref[z, :, width:], preferred_element_type=jnp.float32)
    gated = value * jax.nn.sigmoid(gate)
    pad = padded_ref.shape[1] - LENGTH
    sequences = padded_ref.shape[0]
    for s in range(sequences):
        padded_ref[s, :pad] = jnp.zeros((pad, width), jnp.float32)
        padded_ref[s, pad:] = gated[s * LENGTH : (s + 1) * LENGTH]
    first = lax.axis_index(TP) * width
    for lane in range(0, width, LANES):
        taps = taps_ref[:, pl.ds(pl.multiple_of(first + lane, LANES), LANES)]
        for s in range(sequences):
            total = jnp.zeros((LENGTH, LANES), jnp.float32)
            for shift in range(8):
                offsets = [o for o in range(pad - KWIDTH + 1, pad + 1) if o % 8 == shift]
                span = offsets[-1] - shift + LENGTH
                rows = padded_ref[s, shift : shift + span, lane : lane + LANES]
                for o in offsets:
                    tap = o - (pad - KWIDTH + 1)
                    total += taps[tap : tap + 1] * rows[o - shift : o - shift + LENGTH]
            filtered_ref[s * LENGTH : (s + 1) * LENGTH, lane : lane + LANES] = total
    filtered = filtered_ref[...]
    ones = jnp.ones((8, width), jnp.float32)
    rows = x_ref.shape[0]
    for i, terms in enumerate((filtered, filtered * filtered)):
        sums = lax.dot_general(
            ones,
            terms,
            (((1,), (1,)), ((), ())),
            precision=lax.Precision.HIGHEST,
            preferred_element_type=jnp.float32,
        )
        for copy in range(sums_ref.shape[0]):
            sums_ref[copy, :, i * rows : (i + 1) * rows] = sums[:1]


def gated_filter(x, taps, weights, width):
    rows = x.shape[0]
    count, depth, _ = weights.shape
    vmem = pl.BlockSpec(memory_space=pltpu.VMEM)
    return pl.pallas_call(
        gate_kernel,
        in_specs=[vmem, vmem, pl.BlockSpec(memory_space=pl.ANY)],
        out_specs=(vmem, vmem),
        out_shape=(
            jax.ShapeDtypeStruct((rows, width), jnp.float32),
            jax.ShapeDtypeStruct((lax.axis_size(TP), 1, 2 * rows), jnp.float32),
        ),
        scratch_shapes=[
            pltpu.VMEM((rows // LENGTH, LENGTH + 32, width), jnp.float32),
            pltpu.VMEM((count, depth, 2 * width), jnp.bfloat16),
            pltpu.SemaphoreType.DMA((count,)),
        ],
        compiler_params=pltpu.CompilerParams(vmem_limit_bytes=51 * MIB),
        cost_estimate=pl.CostEstimate(
            flops=4 * rows * D * width, bytes_accessed=4 * D * width, transcendentals=rows * width
        ),
        name="gated_filter",
    )(x, taps, weights)


def mixer_kernel(filtered_ref, sums_ref, gain_ref, *refs):
    *slab_refs, theirs_ref, mine_ref = refs
    core, here, count = lax.axis_index("c"), lax.axis_index("zl"), lax.axis_size("zl")
    rows, width = filtered_ref.shape
    sums = sum(sums_ref[d] for d in range(sums_ref.shape[0])) / D
    mean = sums[:, :rows]
    scale = lax.rsqrt(sums[:, rows:] - mean * mean + EPS)

    def down_rows(row):
        column = jnp.broadcast_to(row, (LANES, rows)).T
        return jnp.concatenate([column] * (width // LANES), axis=1)

    gain = gain_ref[:, pl.ds(pl.multiple_of(lax.axis_index(TP) * width, width), width)]
    values = (filtered_ref[...] - down_rows(mean)) * down_rows(scale) * gain
    activated = (values / (1.0 + jnp.exp(-values))).astype(jnp.bfloat16)
    near, one, low, high, three = slab_refs
    for turn, ref in ((0, near), (1, one), (2, None), (3, three)):
        z = lax.rem(here + turn, count)
        for out_ref, which in ((theirs_ref, 1 - core), (mine_ref, core)):
            if ref is None:
                weight = jnp.where(which == 0, low[:, :width], high[:, :width])
            else:
                weight = ref[pl.ds(pl.multiple_of(which * width, width), width), :width]
            out_ref[z] = times_t(activated, weight).astype(out_ref.dtype)


def mixer(filtered, sums, gain, slabs):
    rows, width = filtered.shape
    vmem = pl.BlockSpec(memory_space=pltpu.VMEM)
    out = (lax.axis_size("zl"), rows, width)
    return pl.pallas_call(
        mixer_kernel,
        in_specs=[vmem] * (3 + len(slabs)),
        out_specs=(vmem, vmem),
        out_shape=(
            jax.ShapeDtypeStruct(out, jnp.bfloat16),
            jax.ShapeDtypeStruct(out, jnp.float32),
        ),
        compiler_params=pltpu.CompilerParams(vmem_limit_bytes=24 * MIB),
        cost_estimate=pl.CostEstimate(
            flops=2 * rows * D * width, bytes_accessed=2 * D * width, transcendentals=rows * width
        ),
        name="mixer",
    )(filtered, sums, gain[None], *slabs)


def norm_kernel(own_ref, other_ref, gain_ref, out_ref):
    core = lax.axis_index("c")
    count, _, width = own_ref.shape
    pieces = [(r[i].astype(jnp.float32), i, s) for s, r in enumerate((own_ref, other_ref)) for i in range(count)]
    total = sum(jnp.sum(v * v, axis=-1, keepdims=True) for v, _, _ in pieces)
    scale = lax.rsqrt(total / D + EPS)
    for values, i, side in pieces:
        which = core if side == 0 else 1 - core
        at = pl.ds(pl.multiple_of((2 * i + which) * width, width), width)
        out_ref[:, at] = (values * scale * gain_ref[:, at]).astype(jnp.bfloat16)


def normed_channels(block, gain):
    own = lax.all_gather(block, "x", axis=0)
    other = lax.ppermute(own, "c", SWAP)
    count, rows, width = own.shape
    part = pl.BlockSpec((count, LENGTH, width), lambda i: (0, i, 0))
    return pl.pallas_call(
        norm_kernel,
        grid=(rows // LENGTH,),
        in_specs=[part, part, pl.BlockSpec((1, D), lambda i: (0, 0))],
        out_specs=pl.BlockSpec((LENGTH, D), lambda i: (i, 0)),
        out_shape=jax.ShapeDtypeStruct((rows, D), jnp.bfloat16),
        cost_estimate=pl.CostEstimate(
            flops=6 * rows * D, bytes_accessed=4 * rows * D, transcendentals=rows
        ),
        compiler_params=pltpu.CompilerParams(vmem_limit_bytes=12 * MIB),
        name="norm",
    )(own, other, gain[None])


def over_group(mine, theirs):
    got = lax.ppermute(theirs, "c", SWAP)
    pair = (mine + got.astype(jnp.float32)).astype(jnp.bfloat16)
    return jnp.sum(lax.all_to_all(pair, "x", 0, 0, tiled=True).astype(jnp.float32), axis=0)


def feed_forward_kernel(x_ref, first_ref, *refs):
    *slab_refs, theirs_ref, mine_ref, up_ref, down_ref, hidden_ref, sems = refs
    core, here = lax.axis_index("c"), lax.axis_index("zl")
    count, depth, columns = up_ref.shape
    width = depth // 2
    up_at, down_at = slice(width, width + LATE), slice(width + LATE, width + 2 * LATE)
    steps = [slice(low, low + width) for low in range(0, columns, width)]
    copies = [
        pltpu.make_async_copy(first_ref.at[:, :, at], up_ref.at[:, :, at], sems.at[i])
        for i, at in enumerate(steps)
    ]
    down = first_ref.at[:, :, columns:]
    copies.append(pltpu.make_async_copy(down, down_ref, sems.at[len(steps)]))
    for copy in copies:
        copy.start()

    def squared_relu(upward):
        return jnp.square(jnp.maximum(upward, 0.0)).astype(jnp.bfloat16)

    upward = 0.0
    for ref, turn, low in zip(slab_refs, (0, 1, 2, 2, 3), (0, 0, 0, width, 0)):
        start = lax.rem(here + turn, count) * depth + low
        x = x_ref[:, pl.ds(pl.multiple_of(start, width), ref.shape[0])]
        upward += jnp.dot(x, ref[:, up_at], preferred_element_type=jnp.float32)
    hidden_ref[:, columns:] = squared_relu(upward)
    for copy, at in zip(copies, steps):
        copy.wait()
        upward = 0.0
        for z in range(count):
            x = x_ref[:, z * depth : (z + 1) * depth]
            upward += jnp.dot(x, up_ref[z, :, at], preferred_element_type=jnp.float32)
        hidden_ref[:, at] = squared_relu(upward)
    copies[-1].wait()
    near, one, low, high, three = slab_refs
    for out_ref, which in ((theirs_ref, 1 - core), (mine_ref, core)):
        rows = pl.ds(pl.multiple_of(which * width, width), width)
        for turn, ref in ((0, near), (1, one), (2, None), (3, three)):
            z = lax.rem(here + turn, count)
            if ref is None:
                late = jnp.where(which == 0, low[:, down_at], high[:, down_at])
            else:
                late = ref[rows, down_at]
            part = times_t(hidden_ref[:, :columns], down_ref[z, rows])
            out_ref[z] = (part + times_t(hidden_ref[:, columns:], late)).astype(out_ref.dtype)


def feed_forward(x, first, late):
    rows = x.shape[0]
    count, depth, columns = first.shape
    columns //= 2
    width = depth // 2
    out = (count, rows, width)
    vmem = pl.BlockSpec(memory_space=pltpu.VMEM)
    weights = pltpu.VMEM((count, depth, columns), jnp.bfloat16)
    hidden = columns + LATE
    return pl.pallas_call(
        feed_forward_kernel,
        in_specs=[vmem, pl.BlockSpec(memory_space=pl.ANY), *(vmem for _ in late)],
        out_specs=(vmem, vmem),
        out_shape=(
            jax.ShapeDtypeStruct(out, jnp.bfloat16),
            jax.ShapeDtypeStruct(out, jnp.float32),
        ),
        scratch_shapes=[
            weights,
            weights,
            pltpu.VMEM((rows, hidden), jnp.bfloat16),
            pltpu.SemaphoreType.DMA((columns // width + 1,)),
        ],
        compiler_params=pltpu.CompilerParams(vmem_limit_bytes=46 * MIB),
        cost_estimate=pl.CostEstimate(
            flops=4 * rows * D * hidden, bytes_accessed=4 * D * hidden, transcendentals=0
        ),
        name="feed_forward",
    )(x, first, *late)


def body(
    states, mix_gain, w_value, w_gate, conv_kernel, chan_gain, w_mix_out, mlp_gain, w_up, w_down_t
):
    width = states.shape[1]
    early, late = packed(w_value, w_gate, w_mix_out, w_up, w_down_t)
    slab = lax.all_to_all(late, "y", 0, 0, tiled=True).reshape(-1, late.shape[2])
    run = lax.all_gather(early, "zl", axis=0)
    gates = over_y(run[:, :, : 2 * width])
    normed = normed_channels(states, mix_gain)
    ffn_first = over_y(run[:, :, 2 * width :])
    slabs = over_z(slab)
    filtered, sums = gated_filter(normed, conv_kernel, gates, width)
    sums = lax.all_to_all(sums, TP, 0, 0, tiled=True)
    theirs, mine = mixer(filtered, sums, chan_gain, slabs)
    mixed = over_group(mine, theirs)
    middle = (states.astype(jnp.float32) + mixed).astype(jnp.bfloat16)
    normed_mid = normed_channels(middle, mlp_gain)
    theirs, mine = feed_forward(normed_mid, ffn_first, slabs)
    fed = over_group(mine, theirs)
    return (middle.astype(jnp.float32) + fed).astype(jnp.bfloat16)


def solution(mesh):
    split = Mesh(mesh.devices.reshape(2, 4, 8, 4, 2), ("rep", "zl", "y", "x", "c"))
    fs = ("zl", "y")
    return jax.shard_map(
        body,
        mesh=split,
        in_specs=(
            P(("rep", *fs), TP),
            P(),
            P(fs, TP),
            P(fs, TP),
            P(),
            P(),
            P(fs, TP),
            P(),
            P(fs, TP),
            P(fs, TP),
        ),
        out_specs=P(("rep", *fs), TP),
        check_vma=False,
    )
```

profile of v0, /device:TPU:1, one launch (start us, length us, event | category | flops | bytes accessed | tf_op | source)
XLA Modules:
  0.0 183.7 jit_solution(3269468222398552146)
XLA Ops:
  6.5 2.0 %pack.1 = (bf16[64,1536]{1,0:T(8,128)(2,1)}, bf16[8,64,768]{2,1,0:T(8,128)(2,1)}) custom-call(bf16[64,256]{1,0:T(8,128)(2,1)} %value_ref.1, bf16[64,256]{1,0:T(8,128)(2,1)} %gate_ref.1, bf16[64,256]{1,0:T(8,128)(2,1)} %out_ref.1, bf16[64,768]{1,0:T(8,128)(2,1)} %up_ref.1, bf16[64,768]{1,0:T(8,128)(2,1)} %down_ref.1), custom_call_target="tpu_custom_call" | custom-call | bytes 1048576 | tf_op jit(solution)/shard_map/pack/pallas_call | solution.py:43
  8.5 20.8 %all-gather.1 = bf16[256,1536]{1,0:T(8,128)(2,1)S(1)} all-gather(bf16[64,1536]{1,0:T(8,128)(2,1)} %get-tuple-element.13), channel_id=3, replica_groups=mesh['rep'=2,'zl'=4,'y'=8,'x'=4,'c'=2] {'zl'}, dimensions={0}, use_global_device_ids=true | all-gather | bytes 983040 | tf_op jit(solution)/shard_map/all_gather | solution.py:307
  31.1 6.6 %all-to-all-start.1 = ((bf16[8,64,768]{2,1,0:T(8,128)(2,1)}), bf16[8,64,768]{2,1,0:T(8,128)(2,1)S(1)}, u32[]{:S(2)}, u32[]{:S(2)}) async-start(bf16[8,64,768]{2,1,0:T(8,128)(2,1)} %get-tuple-element.16), calls=%async_computation.1 | async-start | bytes 1572864 | tf_op jit(solution)/shard_map/all_to_all | solution.py:306
  37.7 11.4 %all-gather = bf16[1536,256]{1,0:T(8,128)(2,1)S(1)} all-gather(bf16[384,256]{1,0:T(8,128)(2,1)S(1)} %copy-done.6), channel_id=2, replica_groups=mesh['rep'=2,'zl'=4,'y'=8,'x'=4,'c'=2] {'x'}, dimensions={0}, use_global_device_ids=true | all-gather | bytes 983040 | tf_op jit(solution)/shard_map/all_gather | solution.py:200
  49.1 8.4 %collective-permute-start = (bf16[4,384,256]{2,1,0:T(8,128)(2,1)S(1)}, bf16[4,384,256]{2,1,0:T(8,128)(2,1)S(1)}, u32[]{:S(2)}, u32[]{:S(2)}) collective-permute-start(bf16[4,384,256]{2,1,0:T(8,128)(2,1)S(1)} %bitcast.13), channel_id=1, source_target_pairs={{0,1},{1,0},{2,3},{3,2},{4,5},{5,4},{6,7},{7,6},{8,9},{9,8},{10,11... | collective-permute-start | bytes 2359304 | tf_op jit(solution)/shard_map/ppermute | solution.py:201
  57.6 2.5 %all-to-all-done.1 = bf16[8,64,768]{2,1,0:T(8,128)(2,1)S(1)} async-done(((bf16[8,64,768]{2,1,0:T(8,128)(2,1)}), bf16[8,64,768]{2,1,0:T(8,128)(2,1)S(1)}, u32[]{:S(2)}, u32[]{:S(2)}) %all-to-all-start.1) | async-done | bytes 786464 | tf_op jit(solution)/shard_map/all_to_all | solution.py:306
  60.1 3.9 %collective-permute-start.4 = (bf16[512,768]{1,0:T(8,128)(2,1)S(1)}, bf16[512,768]{1,0:T(8,128)(2,1)}, u32[]{:S(2)}, u32[]{:S(2)}) collective-permute-start(bf16[512,768]{1,0:T(8,128)(2,1)S(1)} %bitcast.9), channel_id=1, source_target_pairs={{448,0},{0,64},{64,128},{128,192},{192,256},{256,320},{320,384},{3... | collective-permute-start | bytes 2359304 | tf_op jit(solution)/shard_map/ppermute | solution.py:63
  63.9 8.8 %collective-permute-start.1 = (bf16[512,768]{1,0:T(8,128)(2,1)S(1)}, bf16[512,768]{1,0:T(8,128)(2,1)}, u32[]{:S(2)}, u32[]{:S(2)}) collective-permute-start(bf16[512,768]{1,0:T(8,128)(2,1)S(1)} %bitcast.10), channel_id=1, source_target_pairs={{64,0},{128,64},{192,128},{256,192},{320,256},{384,320},{448,384},... | collective-permute-start | bytes 2359304 | tf_op jit(solution)/shard_map/ppermute | solution.py:63
  73.7 3.1 %collective-permute-start.2 = (bf16[256,768]{1,0:T(8,128)(2,1)}, bf16[256,768]{1,0:T(8,128)(2,1)S(1)}, u32[]{:S(2)}, u32[]{:S(2)}) collective-permute-start(bf16[256,768]{1,0:T(8,128)(2,1)} %bitcast.5), channel_id=1, source_target_pairs={{128,0},{192,64},{256,128},{320,192},{384,256},{448,320},{0,384},{... | collective-permute-start | bytes 1179656 | tf_op jit(solution)/shard_map/ppermute | solution.py:63
  76.8 3.1 %collective-permute-start.3 = (bf16[256,768]{1,0:T(8,128)(2,1)}, bf16[256,768]{1,0:T(8,128)(2,1)}, u32[]{:S(2)}, u32[]{:S(2)}) collective-permute-start(bf16[256,768]{1,0:T(8,128)(2,1)} %bitcast.6), channel_id=1, source_target_pairs={{384,0},{448,64},{0,128},{64,192},{128,256},{192,320},{256,384},{3... | collective-permute-start | bytes 1179656 | tf_op jit(solution)/shard_map/ppermute | solution.py:63
  84.2 5.3 %gated_filter.1 = (f32[384,256]{1,0:T(8,128)S(1)}, f32[8,1,768]{2,1,0:T(1,128)}) custom-call(bf16[384,2048]{1,0:T(8,128)(2,1)S(1)} %norm.2.x_ref, f32[31,2048]{1,0:T(8,128)S(1)} %copy-done.2, bf16[4,512,512]{2,1,0:T(8,128)(2,1)} %all-gather.6.cloned.1.call-done.weight_ref), custom_call_target="tpu_custom_call" | custom-call | flops 805306368 | bytes 2097152 | tf_op jit(solution)/shard_map/gated_filter/pallas_call | solution.py:120
  89.5 9.9 %all-to-all-start = ((f32[8,1,768]{2,1,0:T(1,128)}), f32[8,1,768]{2,1,0:T(1,128)S(1)}, u32[]{:S(2)}, u32[]{:S(2)}) async-start(f32[8,1,768]{2,1,0:T(1,128)} %get-tuple-element.15), calls=%async_computation | async-start | bytes 49152 | tf_op jit(solution)/shard_map/all_to_all | solution.py:313
  99.3 2.5 %collective-permute-done.2.refs_2_ = bf16[256,768]{1,0:T(8,128)(2,1)S(1)} collective-permute-done((bf16[256,768]{1,0:T(8,128)(2,1)}, bf16[256,768]{1,0:T(8,128)(2,1)S(1)}, u32[]{:S(2)}, u32[]{:S(2)}) %collective-permute-start.2) | collective-permute-done | bytes 393248 | tf_op jit(solution)/shard_map/ppermute | solution.py:63
  101.8 2.6 %all-to-all-done.sums_ref = f32[8,1,768]{2,1,0:T(1,128)S(1)} async-done(((f32[8,1,768]{2,1,0:T(1,128)}), f32[8,1,768]{2,1,0:T(1,128)S(1)}, u32[]{:S(2)}, u32[]{:S(2)}) %all-to-all-start) | async-done | bytes 24608 | tf_op jit(solution)/shard_map/all_to_all | solution.py:313
  104.4 2.2 %mixer.1 = (bf16[4,384,256]{2,1,0:T(8,128)(2,1)S(1)}, f32[4,384,256]{2,1,0:T(8,128)S(1)}) custom-call(f32[384,256]{1,0:T(8,128)S(1)} %get-tuple-element.14.filtered_ref, f32[8,1,768]{2,1,0:T(1,128)S(1)} %all-to-all-done.sums_ref, f32[1,2048]{1,0:T(1,128)S(1)} %bitcast.18, bf16[512,768]{1,0:T(8,128)(2,1)S(1)} %bitcast.11, ...), custom_call_target="tpu_custom_call" | custom-call | flops 402653184 | bytes 1048576 | tf_op jit(solution)/shard_map/mixer/pallas_call | solution.py:171
  106.6 4.9 %collective-permute-start.5 = (bf16[4,384,256]{2,1,0:T(8,128)(2,1)S(1)}, bf16[4,384,256]{2,1,0:T(8,128)(2,1)S(1)}, u32[]{:S(2)}, u32[]{:S(2)}) collective-permute-start(bf16[4,384,256]{2,1,0:T(8,128)(2,1)S(1)} %get-tuple-element.18), channel_id=1, source_target_pairs={{0,1},{1,0},{2,3},{3,2},{4,5},{5,4},{6,7},{7,6},{8,9},{9,8},{10,11... | collective-permute-start | bytes 2359304 | tf_op jit(solution)/shard_map/ppermute | solution.py:219
  111.5 1.9 %collective-permute-done.5 = bf16[4,384,256]{2,1,0:T(8,128)(2,1)S(1)} collective-permute-done((bf16[4,384,256]{2,1,0:T(8,128)(2,1)S(1)}, bf16[4,384,256]{2,1,0:T(8,128)(2,1)S(1)}, u32[]{:S(2)}, u32[]{:S(2)}) %collective-permute-start.5) | collective-permute-done | bytes 786464 | tf_op jit(solution)/shard_map/ppermute | solution.py:219
  113.6 15.4 %all_to_all.20 = bf16[4,384,256]{2,1,0:T(8,128)(2,1)S(1)} all-to-all(bf16[4,384,256]{2,1,0:T(8,128)(2,1)S(1)} %add_convert_fusion.1), channel_id=1, replica_groups=mesh['rep'=2,'zl'=4,'y'=8,'x'=4,'c'=2] {'x'}, dimensions={0} | all-to-all | bytes 1572864 | tf_op jit(solution)/shard_map/all_to_all | solution.py:221
  129.2 11.7 %all-gather.2 = bf16[1536,256]{1,0:T(8,128)(2,1)S(1)} all-gather(bf16[384,256]{1,0:T(8,128)(2,1)S(1)} %add_convert_fusion.3), channel_id=4, replica_groups=mesh['rep'=2,'zl'=4,'y'=8,'x'=4,'c'=2] {'x'}, dimensions={0}, use_global_device_ids=true | all-gather | bytes 983040 | tf_op jit(solution)/shard_map/all_gather | solution.py:200
  140.9 6.3 %collective-permute-start.6 = (bf16[4,384,256]{2,1,0:T(8,128)(2,1)S(1)}, bf16[4,384,256]{2,1,0:T(8,128)(2,1)S(1)}, u32[]{:S(2)}, u32[]{:S(2)}) collective-permute-start(bf16[4,384,256]{2,1,0:T(8,128)(2,1)S(1)} %bitcast.15), channel_id=1, source_target_pairs={{0,1},{1,0},{2,3},{3,2},{4,5},{5,4},{6,7},{7,6},{8,9},{9,8},{10,11... | collective-permute-start | bytes 2359304 | tf_op jit(solution)/shard_map/ppermute | solution.py:201
  147.2 1.9 %collective-permute-done.6.other_ref = bf16[4,384,256]{2,1,0:T(8,128)(2,1)S(1)} collective-permute-done((bf16[4,384,256]{2,1,0:T(8,128)(2,1)S(1)}, bf16[4,384,256]{2,1,0:T(8,128)(2,1)S(1)}, u32[]{:S(2)}, u32[]{:S(2)}) %collective-permute-start.6) | collective-permute-done | bytes 786464 | tf_op jit(solution)/shard_map/ppermute | solution.py:201
  150.4 7.0 %feed_forward.1 = (bf16[4,384,256]{2,1,0:T(8,128)(2,1)S(1)}, f32[4,384,256]{2,1,0:T(8,128)S(1)}) custom-call(bf16[384,2048]{1,0:T(8,128)(2,1)S(1)} %norm.3.x_ref, bf16[4,512,1024]{2,1,0:T(8,128)(2,1)} %all-gather.8.cloned.1.call-done.first_ref, bf16[512,768]{1,0:T(8,128)(2,1)S(1)} %bitcast.12, bf16[512,768]{1,0:T(8,128)(2,1)} %collective-permute-done.1.refs_1_, ...), custom_call_target="tpu_custom_call" | custom-call | flops 2415919104 | bytes 6291456 | tf_op jit(solution)/shard_map/feed_forward/pallas_call | solution.py:279
  157.3 2.3 %collective-permute-start.7 = (bf16[4,384,256]{2,1,0:T(8,128)(2,1)S(1)}, bf16[4,384,256]{2,1,0:T(8,128)(2,1)S(1)}, u32[]{:S(2)}, u32[]{:S(2)}) collective-permute-start(bf16[4,384,256]{2,1,0:T(8,128)(2,1)S(1)} %get-tuple-element.20), channel_id=1, source_target_pairs={{0,1},{1,0},{2,3},{3,2},{4,5},{5,4},{6,7},{7,6},{8,9},{9,8},{10,11... | collective-permute-start | bytes 2359304 | tf_op jit(solution)/shard_map/ppermute | solution.py:219
  161.7 14.3 %all_to_all.21 = bf16[4,384,256]{2,1,0:T(8,128)(2,1)S(1)} all-to-all(bf16[4,384,256]{2,1,0:T(8,128)(2,1)S(1)} %add_convert_fusion), channel_id=1, replica_groups=mesh['rep'=2,'zl'=4,'y'=8,'x'=4,'c'=2] {'x'}, dimensions={0} | all-to-all | bytes 1572864 | tf_op jit(solution)/shard_map/all_to_all | solution.py:221
  (38 shorter events, 11.5 us)
Async XLA Ops:
  6.5 76.7 %all-gather.6.cloned.1.call-start = ((), (), s32[]{:S(2)}) async-start(), calls=%async_computation.4 | async-start | bytes 2359296 | tf_op jit(solution)/shard_map/all_gather | solution.py:56
  30.1 7.6 %copy-start.6 = (bf16[384,256]{1,0:T(8,128)(2,1)S(1)}, bf16[384,256]{1,0:T(8,128)(2,1)}, u32[]{:S(2)}) copy-start(bf16[384,256]{1,0:T(8,128)(2,1)} %param.10) | copy-start | bytes 589828
  30.1 120.2 %all-gather.8.cloned.1.call-start = ((), (), s32[]{:S(2)}) async-start(), calls=%async_computation.5 | async-start | bytes 4718592 | tf_op jit(solution)/shard_map/all_gather | solution.py:56
  31.1 29.0 %all-to-all-start.1 = ((bf16[8,64,768]{2,1,0:T(8,128)(2,1)}), bf16[8,64,768]{2,1,0:T(8,128)(2,1)S(1)}, u32[]{:S(2)}, u32[]{:S(2)}) async-start(bf16[8,64,768]{2,1,0:T(8,128)(2,1)} %get-tuple-element.16), calls=%async_computation.1 | async-start | bytes 1572864 | tf_op jit(solution)/shard_map/all_to_all | solution.py:306
  37.7 43.1 %copy-start.3 = (f32[2048]{0:T(1024)S(1)}, f32[2048]{0:T(1024)}, u32[]{:S(2)}) copy-start(f32[2048]{0:T(1024)} %param.11) | copy-start | bytes 24580
  49.1 30.7 %collective-permute-start = (bf16[4,384,256]{2,1,0:T(8,128)(2,1)S(1)}, bf16[4,384,256]{2,1,0:T(8,128)(2,1)S(1)}, u32[]{:S(2)}, u32[]{:S(2)}) collective-permute-start(bf16[4,384,256]{2,1,0:T(8,128)(2,1)S(1)} %bitcast.13), channel_id=1, source_target_pairs={{0,1},{1,0},{2,3},{3,2},{4,5},{5,4},{6,7},{7,6},{8,9},{9,8},{10,11... | collective-permute-start | bytes 2359304 | tf_op jit(solution)/shard_map/ppermute | solution.py:201
  60.1 41.7 %collective-permute-start.4 = (bf16[512,768]{1,0:T(8,128)(2,1)S(1)}, bf16[512,768]{1,0:T(8,128)(2,1)}, u32[]{:S(2)}, u32[]{:S(2)}) collective-permute-start(bf16[512,768]{1,0:T(8,128)(2,1)S(1)} %bitcast.9), channel_id=1, source_target_pairs={{448,0},{0,64},{64,128},{128,192},{192,256},{256,320},{320,384},{3... | collective-permute-start | bytes 2359304 | tf_op jit(solution)/shard_map/ppermute | solution.py:63
  63.9 37.9 %collective-permute-start.1 = (bf16[512,768]{1,0:T(8,128)(2,1)S(1)}, bf16[512,768]{1,0:T(8,128)(2,1)}, u32[]{:S(2)}, u32[]{:S(2)}) collective-permute-start(bf16[512,768]{1,0:T(8,128)(2,1)S(1)} %bitcast.10), channel_id=1, source_target_pairs={{64,0},{128,64},{192,128},{256,192},{320,256},{384,320},{448,384},... | collective-permute-start | bytes 2359304 | tf_op jit(solution)/shard_map/ppermute | solution.py:63
  73.7 28.1 %collective-permute-start.2 = (bf16[256,768]{1,0:T(8,128)(2,1)}, bf16[256,768]{1,0:T(8,128)(2,1)S(1)}, u32[]{:S(2)}, u32[]{:S(2)}) collective-permute-start(bf16[256,768]{1,0:T(8,128)(2,1)} %bitcast.5), channel_id=1, source_target_pairs={{128,0},{192,64},{256,128},{320,192},{384,256},{448,320},{0,384},{... | collective-permute-start | bytes 1179656 | tf_op jit(solution)/shard_map/ppermute | solution.py:63
  76.8 25.0 %collective-permute-start.3 = (bf16[256,768]{1,0:T(8,128)(2,1)}, bf16[256,768]{1,0:T(8,128)(2,1)}, u32[]{:S(2)}, u32[]{:S(2)}) collective-permute-start(bf16[256,768]{1,0:T(8,128)(2,1)} %bitcast.6), channel_id=1, source_target_pairs={{384,0},{448,64},{0,128},{64,192},{128,256},{192,320},{256,384},{3... | collective-permute-start | bytes 1179656 | tf_op jit(solution)/shard_map/ppermute | solution.py:63
  79.9 1.0 copy-start
  80.8 1.1 copy-start.1
  83.2 1.0 copy-start.2
  84.2 20.3 %copy-start.4 = (f32[2048]{0:T(1024)S(1)}, f32[2048]{0:T(1024)}, u32[]{:S(2)}) copy-start(f32[2048]{0:T(1024)} %param.15) | copy-start | bytes 24580
  89.5 15.0 %all-to-all-start = ((f32[8,1,768]{2,1,0:T(1,128)}), f32[8,1,768]{2,1,0:T(1,128)S(1)}, u32[]{:S(2)}, u32[]{:S(2)}) async-start(f32[8,1,768]{2,1,0:T(1,128)} %get-tuple-element.15), calls=%async_computation | async-start | bytes 49152 | tf_op jit(solution)/shard_map/all_to_all | solution.py:313
  106.6 6.8 %collective-permute-start.5 = (bf16[4,384,256]{2,1,0:T(8,128)(2,1)S(1)}, bf16[4,384,256]{2,1,0:T(8,128)(2,1)S(1)}, u32[]{:S(2)}, u32[]{:S(2)}) collective-permute-start(bf16[4,384,256]{2,1,0:T(8,128)(2,1)S(1)} %get-tuple-element.18), channel_id=1, source_target_pairs={{0,1},{1,0},{2,3},{3,2},{4,5},{5,4},{6,7},{7,6},{8,9},{9,8},{10,11... | collective-permute-start | bytes 2359304 | tf_op jit(solution)/shard_map/ppermute | solution.py:219
  113.6 15.6 %copy-start.7 = (bf16[384,256]{1,0:T(8,128)(2,1)S(1)}, bf16[384,256]{1,0:T(8,128)(2,1)}, u32[]{:S(2)}) copy-start(bf16[384,256]{1,0:T(8,128)(2,1)} %param.10) | copy-start | bytes 589828
  129.0 20.1 %copy-start.5 = (f32[2048]{0:T(1024)S(1)}, f32[2048]{0:T(1024)}, u32[]{:S(2)}) copy-start(f32[2048]{0:T(1024)} %param.17) | copy-start | bytes 24580
  140.9 8.2 %collective-permute-start.6 = (bf16[4,384,256]{2,1,0:T(8,128)(2,1)S(1)}, bf16[4,384,256]{2,1,0:T(8,128)(2,1)S(1)}, u32[]{:S(2)}, u32[]{:S(2)}) collective-permute-start(bf16[4,384,256]{2,1,0:T(8,128)(2,1)S(1)} %bitcast.15), channel_id=1, source_target_pairs={{0,1},{1,0},{2,3},{3,2},{4,5},{5,4},{6,7},{7,6},{8,9},{9,8},{10,11... | collective-permute-start | bytes 2359304 | tf_op jit(solution)/shard_map/ppermute | solution.py:201
  157.3 4.2 %collective-permute-start.7 = (bf16[4,384,256]{2,1,0:T(8,128)(2,1)S(1)}, bf16[4,384,256]{2,1,0:T(8,128)(2,1)S(1)}, u32[]{:S(2)}, u32[]{:S(2)}) collective-permute-start(bf16[4,384,256]{2,1,0:T(8,128)(2,1)S(1)} %get-tuple-element.20), channel_id=1, source_target_pairs={{0,1},{1,0},{2,3},{3,2},{4,5},{5,4},{6,7},{7,6},{8,9},{9,8},{10,11... | collective-permute-start | bytes 2359304 | tf_op jit(solution)/shard_map/ppermute | solution.py:219
Sparse Core Ops, SparseCore 0:
  30.2 49.7 all-gather.5
  82.1 58.6 all-gather.7
where the time goes:
time: 184 us
  blocking collectives  73.7 us (40%)
  starting transfers between devices  57.2 us (31%)
  Pallas kernels  18.8 us (10%)
  between operations  13.6 us (7%)
  waiting for transfers between devices  13.3 us (7%)
  local copies, waits for them, and re-layouts  5.67 us (3%)
    all_to_all x2, blocking collectives, over_group(): lax.all_to_all(pair, 'x', 0, 0, tiled=True).astype(jnp.float32)  29.7 us
    all_gather x2, blocking collectives, normed_channels(): own = lax.all_gather(block, 'x', axis=0)  23.1 us
    all_gather x1, blocking collectives, body(): run = lax.all_gather(early, 'zl', axis=0)  20.8 us
    ppermute x4, starting transfers between devices, from_z(): lax.ppermute(piece, ('rep', 'zl'), [((i + step) % 8, i) for i in range(8)])  18.8 us
    ppermute x2, starting transfers between devices, normed_channels(): other = lax.ppermute(own, 'c', SWAP)  14.8 us
    all_to_all x1, starting transfers between devices, body(): sums = lax.all_to_all(sums, TP, 0, 0, tiled=True)  9.88 us
    ppermute x2, starting transfers between devices, over_group(): got = lax.ppermute(theirs, 'c', SWAP)  7.17 us
    pallas_call x1, Pallas kernels, feed_forward(): pl.pallas_call(feed_forward_kernel, in_specs=[vmem, pl.BlockSpec(memory_s...  6.98 us
  transfers between devices with their start and end apart: 12, of which 6 were waited for; matrix products, arithmetic and copies ran while one was open for 1% of the time, Pallas kernels for 5%

commit v1 on v0

--- a/solution.py
+++ b/solution.py
@@ -16,6 +16,7 @@
 
 MIB = 1 << 20
 LANES = 128
+ANY = pl.BlockSpec(memory_space=pl.ANY)
 LATE = 256
 
 
@@ -25,12 +26,12 @@
     )
 
 
-def pack_kernel(value_ref, gate_ref, out_ref, up_ref, down_ref, early_ref, late_ref):
+def pack_kernel(value_ref, gate_ref, out_ref, up_ref, down_ref, gates_ref, first_ref, late_ref):
     width, first = value_ref.shape[1], up_ref.shape[1] - LATE
-    at = 0
-    for ref, count in ((value_ref, width), (gate_ref, width), (up_ref, first), (down_ref, first)):
-        early_ref[:, at : at + count] = ref[:, :count]
-        at += count
+    gates_ref[:, :width] = value_ref[...]
+    gates_ref[:, width:] = gate_ref[...]
+    first_ref[:, :first] = up_ref[:, :first]
+    first_ref[:, first:] = down_ref[:, :first]
     for copy in range(late_ref.shape[0]):
         late_ref[copy, :, :width] = out_ref[...]
         late_ref[copy, :, width : width + LATE] = up_ref[:, first:]
@@ -43,7 +44,8 @@
     return pl.pallas_call(
         pack_kernel,
         out_shape=(
-            jax.ShapeDtypeStruct((rows, 2 * (width + first)), jnp.bfloat16),
+            jax.ShapeDtypeStruct((rows, 2 * width), jnp.bfloat16),
+            jax.ShapeDtypeStruct((rows, 2 * first), jnp.bfloat16),
             jax.ShapeDtypeStruct((lax.axis_size("y"), rows, width + 2 * LATE), jnp.bfloat16),
         ),
         compiler_params=pltpu.CompilerParams(vmem_limit_bytes=60 * MIB),
@@ -85,9 +87,8 @@
     for s in range(sequences):
         padded_ref[s, :pad] = jnp.zeros((pad, width), jnp.float32)
         padded_ref[s, pad:] = gated[s * LENGTH : (s + 1) * LENGTH]
-    first = lax.axis_index(TP) * width
     for lane in range(0, width, LANES):
-        taps = taps_ref[:, pl.ds(pl.multiple_of(first + lane, LANES), LANES)]
+        taps = taps_ref[:, lane : lane + LANES]
         for s in range(sequences):
             total = jnp.zeros((LENGTH, LANES), jnp.float32)
             for shift in range(8):
@@ -119,7 +120,7 @@
     vmem = pl.BlockSpec(memory_space=pltpu.VMEM)
     return pl.pallas_call(
         gate_kernel,
-        in_specs=[vmem, vmem, pl.BlockSpec(memory_space=pl.ANY)],
+        in_specs=[vmem, vmem, ANY],
         out_specs=(vmem, vmem),
         out_shape=(
             jax.ShapeDtypeStruct((rows, width), jnp.float32),
@@ -138,10 +139,22 @@
     )(x, taps, weights)
 
 
+def fetched(slab_refs, held_ref, columns, sems):
+    here, count = lax.axis_index("zl"), lax.axis_size("zl")
+    copies = []
+    for i, (ref, turn) in enumerate(zip(slab_refs, (0, 1, 2, 2, 3))):
+        low = ref.shape[0] if i == 3 else 0
+        to = held_ref.at[lax.rem(here + turn, count), low : low + ref.shape[0]]
+        copies.append(pltpu.make_async_copy(ref.at[:, columns], to, sems.at[i]))
+        copies[i].start()
+    return copies
+
+
 def mixer_kernel(filtered_ref, sums_ref, gain_ref, *refs):
-    *slab_refs, theirs_ref, mine_ref = refs
-    core, here, count = lax.axis_index("c"), lax.axis_index("zl"), lax.axis_size("zl")
+    *slab_refs, theirs_ref, mine_ref, held_ref, sems = refs
+    core = lax.axis_index("c")
     rows, width = filtered_ref.shape
+    copies = fetched(slab_refs, held_ref, slice(0, width), sems)
     sums = sum(sums_ref[d] for d in range(sums_ref.shape[0])) / D
     mean = sums[:, :rows]
     scale = lax.rsqrt(sums[:, rows:] - mean * mean + EPS)
@@ -153,15 +166,12 @@
     gain = gain_ref[:, pl.ds(pl.multiple_of(lax.axis_index(TP) * width, width), width)]
     values = (filtered_ref[...] - down_rows(mean)) * down_rows(scale) * gain
     activated = (values / (1.0 + jnp.exp(-values))).astype(jnp.bfloat16)
-    near, one, low, high, three = slab_refs
-    for turn, ref in ((0, near), (1, one), (2, None), (3, three)):
-        z = lax.rem(here + turn, count)
-        for out_ref, which in ((theirs_ref, 1 - core), (mine_ref, core)):
-            if ref is None:
-                weight = jnp.where(which == 0, low[:, :width], high[:, :width])
-            else:
-                weight = ref[pl.ds(pl.multiple_of(which * width, width), width), :width]
-            out_ref[z] = times_t(activated, weight).astype(out_ref.dtype)
+    for copy in copies:
+        copy.wait()
+    for out_ref, which in ((theirs_ref, 1 - core), (mine_ref, core)):
+        at = pl.ds(pl.multiple_of(which * width, width), width)
+        for z in range(held_ref.shape[0]):
+            out_ref[z] = times_t(activated, held_ref[z, at]).astype(out_ref.dtype)
 
 
 def mixer(filtered, sums, gain, slabs):
@@ -170,12 +180,16 @@
     out = (lax.axis_size("zl"), rows, width)
     return pl.pallas_call(
         mixer_kernel,
-        in_specs=[vmem] * (3 + len(slabs)),
+        in_specs=[vmem, vmem, vmem, *(ANY for _ in slabs)],
         out_specs=(vmem, vmem),
         out_shape=(
             jax.ShapeDtypeStruct(out, jnp.bfloat16),
             jax.ShapeDtypeStruct(out, jnp.float32),
         ),
+        scratch_shapes=[
+            pltpu.VMEM((out[0], 2 * width, width), jnp.bfloat16),
+            pltpu.SemaphoreType.DMA((len(slabs),)),
+        ],
         compiler_params=pltpu.CompilerParams(vmem_limit_bytes=24 * MIB),
         cost_estimate=pl.CostEstimate(
             flops=2 * rows * D * width, bytes_accessed=2 * D * width, transcendentals=rows * width
@@ -196,8 +210,7 @@
         out_ref[:, at] = (values * scale * gain_ref[:, at]).astype(jnp.bfloat16)
 
 
-def normed_channels(block, gain):
-    own = lax.all_gather(block, "x", axis=0)
+def normed_channels(own, gain):
     other = lax.ppermute(own, "c", SWAP)
     count, rows, width = own.shape
     part = pl.BlockSpec((count, LENGTH, width), lambda i: (0, i, 0))
@@ -222,49 +235,42 @@
 
 
 def feed_forward_kernel(x_ref, first_ref, *refs):
-    *slab_refs, theirs_ref, mine_ref, up_ref, down_ref, hidden_ref, sems = refs
-    core, here = lax.axis_index("c"), lax.axis_index("zl")
+    *slab_refs, theirs_ref, mine_ref, up_ref, down_ref, late_ref, hidden_ref, sems = refs
+    core = lax.axis_index("c")
     count, depth, columns = up_ref.shape
     width = depth // 2
-    up_at, down_at = slice(width, width + LATE), slice(width + LATE, width + 2 * LATE)
     steps = [slice(low, low + width) for low in range(0, columns, width)]
     copies = [
         pltpu.make_async_copy(first_ref.at[:, :, at], up_ref.at[:, :, at], sems.at[i])
         for i, at in enumerate(steps)
     ]
-    down = first_ref.at[:, :, columns:]
-    copies.append(pltpu.make_async_copy(down, down_ref, sems.at[len(steps)]))
     for copy in copies:
         copy.start()
-
-    def squared_relu(upward):
-        return jnp.square(jnp.maximum(upward, 0.0)).astype(jnp.bfloat16)
-
-    upward = 0.0
-    for ref, turn, low in zip(slab_refs, (0, 1, 2, 2, 3), (0, 0, 0, width, 0)):
-        start = lax.rem(here + turn, count) * depth + low
-        x = x_ref[:, pl.ds(pl.multiple_of(start, width), ref.shape[0])]
-        upward += jnp.dot(x, ref[:, up_at], preferred_element_type=jnp.float32)
-    hidden_ref[:, columns:] = squared_relu(upward)
-    for copy, at in zip(copies, steps):
-        copy.wait()
+    past = len(steps) + 1
+    late_copies = fetched(slab_refs, late_ref, slice(width, width + 2 * LATE), sems.at[past:])
+    down = pltpu.make_async_copy(first_ref.at[:, :, columns:], down_ref, sems.at[len(steps)])
+    down.start()
+
+    def hidden_of(weight_ref, at):
         upward = 0.0
         for z in range(count):
             x = x_ref[:, z * depth : (z + 1) * depth]
-            upward += jnp.dot(x, up_ref[z, :, at], preferred_element_type=jnp.float32)
-        hidden_ref[:, at] = squared_relu(upward)
-    copies[-1].wait()
-    near, one, low, high, three = slab_refs
+            upward += jnp.dot(x, weight_ref[z, :, at], preferred_element_type=jnp.float32)
+        return jnp.square(jnp.maximum(upward, 0.0)).astype(jnp.bfloat16)
+
+    for copy, at in zip(copies, steps):
+        copy.wait()
+        hidden_ref[:, at] = hidden_of(up_ref, at)
+    for copy in late_copies:
+        copy.wait()
+    hidden_ref[:, columns:] = hidden_of(late_ref, slice(0, LATE))
+    down.wait()
     for out_ref, which in ((theirs_ref, 1 - core), (mine_ref, core)):
         rows = pl.ds(pl.multiple_of(which * width, width), width)
-        for turn, ref in ((0, near), (1, one), (2, None), (3, three)):
-            z = lax.rem(here + turn, count)
-            if ref is None:
-                late = jnp.where(which == 0, low[:, down_at], high[:, down_at])
-            else:
-                late = ref[rows, down_at]
+        for z in range(count):
             part = times_t(hidden_ref[:, :columns], down_ref[z, rows])
-            out_ref[z] = (part + times_t(hidden_ref[:, columns:], late)).astype(out_ref.dtype)
+            part += times_t(hidden_ref[:, columns:], late_ref[z, rows, LATE:])
+            out_ref[z] = part.astype(out_ref.dtype)
 
 
 def feed_forward(x, first, late):
@@ -278,7 +284,7 @@
     hidden = columns + LATE
     return pl.pallas_call(
         feed_forward_kernel,
-        in_specs=[vmem, pl.BlockSpec(memory_space=pl.ANY), *(vmem for _ in late)],
+        in_specs=[vmem, ANY, *(ANY for _ in late)],
         out_specs=(vmem, vmem),
         out_shape=(
             jax.ShapeDtypeStruct(out, jnp.bfloat16),
@@ -287,8 +293,9 @@
         scratch_shapes=[
             weights,
             weights,
+            pltpu.VMEM((count, depth, 2 * LATE), jnp.bfloat16),
             pltpu.VMEM((rows, hidden), jnp.bfloat16),
-            pltpu.SemaphoreType.DMA((columns // width + 1,)),
+            pltpu.SemaphoreType.DMA((columns // width + 1 + len(late),)),
         ],
         compiler_params=pltpu.CompilerParams(vmem_limit_bytes=46 * MIB),
         cost_estimate=pl.CostEstimate(
@@ -302,20 +309,23 @@
     states, mix_gain, w_value, w_gate, conv_kernel, chan_gain, w_mix_out, mlp_gain, w_up, w_down_t
 ):
     width = states.shape[1]
-    early, late = packed(w_value, w_gate, w_mix_out, w_up, w_down_t)
+    gates, first, late = packed(w_value, w_gate, w_mix_out, w_up, w_down_t)
     slab = lax.all_to_all(late, "y", 0, 0, tiled=True).reshape(-1, late.shape[2])
-    run = lax.all_gather(early, "zl", axis=0)
-    gates = over_y(run[:, :, : 2 * width])
-    normed = normed_channels(states, mix_gain)
-    ffn_first = over_y(run[:, :, 2 * width :])
+    gates = lax.all_gather(gates, "zl", axis=0)
+    first = lax.all_gather(first, "zl", axis=0)
     slabs = over_z(slab)
-    filtered, sums = gated_filter(normed, conv_kernel, gates, width)
+    own = lax.all_gather(states, "x", axis=0)
+    taps = lax.dynamic_slice_in_dim(conv_kernel, lax.axis_index(TP) * width, width, 1)
+    own, taps = lax.optimization_barrier((own, taps))
+    gates, first = over_y(gates), over_y(first)
+    normed = normed_channels(own, mix_gain)
+    filtered, sums = gated_filter(normed, taps, gates, width)
     sums = lax.all_to_all(sums, TP, 0, 0, tiled=True)
     theirs, mine = mixer(filtered, sums, chan_gain, slabs)
     mixed = over_group(mine, theirs)
     middle = (states.astype(jnp.float32) + mixed).astype(jnp.bfloat16)
-    normed_mid = normed_channels(middle, mlp_gain)
-    theirs, mine = feed_forward(normed_mid, ffn_first, slabs)
+    normed_mid = normed_channels(lax.all_gather(middle, "x", axis=0), mlp_gain)
+    theirs, mine = feed_forward(normed_mid, first, slabs)
     fed = over_group(mine, theirs)
     return (middle.astype(jnp.float32) + fed).astype(jnp.bfloat16)
 

time: 184 us -> 195 us (1.060)
  blocking collectives: 73.7 us -> 83.6 us
  waiting for transfers between devices: 13.3 us -> 17.8 us
  local copies, waits for them, and re-layouts: 5.67 us -> 3.09 us
    all_gather x3 -> x4, blocking collectives: 43.9 us -> 53.9 us  [the longest x1 17.4 us: body(): gates = lax.all_gather(gates, 'zl', axis=0)]
    all_to_all x1, waiting for transfers between devices: 2.5 us -> 6.95 us  [body(): lax.all_to_all(late, 'y', 0, 0, tiled=True).reshape(-1, late.shape[2])]
    ppermute x4, starting transfers between devices: 18.8 us -> 15.7 us  [from_z(): lax.ppermute(piece, ('rep', 'zl'), [((i + step) % 8, i) for i in range(8)])]
    ppermute x4, waiting for transfers between devices: 2.46 us -> 0.01 us  [from_z(): lax.ppermute(piece, ('rep', 'zl'), [((i + step) % 8, i) for i in range(8)])]
    all_to_all x1, waiting for transfers between devices: 2.62 us -> 5.06 us  [body(): sums = lax.all_to_all(sums, TP, 0, 0, tiled=True)]
    ppermute x2, starting transfers between devices: 14.8 us -> 17.2 us  [normed_channels(): other = lax.ppermute(own, 'c', SWAP)]
  transfers between devices with their start and end apart: 12 -> 12, of which waited for: 6 -> 5; matrix products, arithmetic and copies ran while one was open for 1% -> 1% of each run, Pallas kernels for 5% -> 5%
where the time goes in v1:
time: 195 us; the launch traced here: 194 us
  blocking collectives  83.6 us (43%)
  starting transfers between devices  57.3 us (29%)
  waiting for transfers between devices  17.8 us (9%)
  Pallas kernels  17.5 us (9%)
  between operations  13.6 us (7%)
  local copies, waits for them, and re-layouts  3.09 us (2%)
    all_to_all x2, blocking collectives, over_group(): lax.all_to_all(pair, 'x', 0, 0, tiled=True).astype(jnp.float32)  29.7 us
    all_gather x1, blocking collectives, body(): gates = lax.all_gather(gates, 'zl', axis=0)  17.4 us
    ppermute x2, starting transfers between devices, normed_channels(): other = lax.ppermute(own, 'c', SWAP)  17.2 us
    ppermute x4, starting transfers between devices, from_z(): lax.ppermute(piece, ('rep', 'zl'), [((i + step) % 8, i) for i in range(8)])  15.7 us
    all_gather x1, blocking collectives, body(): first = lax.all_gather(first, 'zl', axis=0)  13.4 us
    all_gather x1, blocking collectives, body(): own = lax.all_gather(states, 'x', axis=0)  11.6 us
    all_gather x1, blocking collectives, body(): normed_mid = normed_channels(lax.all_gather(middle, 'x', axis=0), mlp_gain)  11.6 us
    all_to_all x1, starting transfers between devices, body(): sums = lax.all_to_all(sums, TP, 0, 0, tiled=True)  10.4 us
  transfers between devices with their start and end apart: 12, of which 5 were waited for; matrix products, arithmetic and copies ran while one was open for 1% of the time, Pallas kernels for 5%

profile of v1, /device:TPU:1, one launch (start us, length us, event | category | flops | bytes accessed | tf_op | source)
XLA Modules:
  0.0 194.3 jit_solution(18119902361740323736)
XLA Ops:
  6.5 2.0 %pack.1 = (bf16[64,512]{1,0:T(8,128)(2,1)}, bf16[64,1024]{1,0:T(8,128)(2,1)}, bf16[8,64,768]{2,1,0:T(8,128)(2,1)}) custom-call(bf16[64,256]{1,0:T(8,128)(2,1)} %value_ref.1, bf16[64,256]{1,0:T(8,128)(2,1)} %gate_ref.1, bf16[64,256]{1,0:T(8,128)(2,1)} %out_ref.1, bf16[64,768]{1,0:T(8,128)(2,1)} %up_ref.1, bf16[64,768]{1,0:T(8,128)(2,1)} %down_ref.1), custom_call_target="tpu_custom_call" | custom-call | bytes 1048576 | tf_op jit(solution)/shard_map/pack/pallas_call | solution.py:44
  8.5 17.4 %all-gather.1 = bf16[256,512]{1,0:T(8,128)(2,1)} all-gather(bf16[64,512]{1,0:T(8,128)(2,1)} %get-tuple-element.18), channel_id=3, replica_groups=mesh['rep'=2,'zl'=4,'y'=8,'x'=4,'c'=2] {'zl'}, dimensions={0}, use_global_device_ids=true | all-gather | bytes 327680 | tf_op jit(solution)/shard_map/all_gather | solution.py:314
  26.0 13.4 %all-gather.3 = bf16[256,1024]{1,0:T(8,128)(2,1)} all-gather(bf16[64,1024]{1,0:T(8,128)(2,1)} %get-tuple-element.24), channel_id=5, replica_groups=mesh['rep'=2,'zl'=4,'y'=8,'x'=4,'c'=2] {'zl'}, dimensions={0}, use_global_device_ids=true | all-gather | bytes 655360 | tf_op jit(solution)/shard_map/all_gather | solution.py:315
  39.5 6.2 %all-to-all-start.1 = ((bf16[8,64,768]{2,1,0:T(8,128)(2,1)}), bf16[8,64,768]{2,1,0:T(8,128)(2,1)S(1)}, u32[]{:S(2)}, u32[]{:S(2)}) async-start(bf16[8,64,768]{2,1,0:T(8,128)(2,1)} %get-tuple-element.21), calls=%async_computation.1 | async-start | bytes 1572864 | tf_op jit(solution)/shard_map/all_to_all | solution.py:313
  45.7 11.6 %all-gather = bf16[1536,256]{1,0:T(8,128)(2,1)S(1)} all-gather(bf16[384,256]{1,0:T(8,128)(2,1)S(1)} %copy-done.6), channel_id=2, replica_groups=mesh['rep'=2,'zl'=4,'y'=8,'x'=4,'c'=2] {'x'}, dimensions={0}, use_global_device_ids=true | all-gather | bytes 983040 | tf_op jit(solution)/shard_map/all_gather | solution.py:317
  57.3 10.8 %collective-permute-start = (bf16[4,384,256]{2,1,0:T(8,128)(2,1)S(1)}, bf16[4,384,256]{2,1,0:T(8,128)(2,1)S(1)}, u32[]{:S(2)}, u32[]{:S(2)}) collective-permute-start(bf16[4,384,256]{2,1,0:T(8,128)(2,1)S(1)} %bitcast.14), channel_id=1, source_target_pairs={{0,1},{1,0},{2,3},{3,2},{4,5},{5,4},{6,7},{7,6},{8,9},{9,8},{10,11... | collective-permute-start | bytes 2359304 | tf_op jit(solution)/shard_map/ppermute | solution.py:214
  68.1 7.0 %all-to-all-done.1 = bf16[8,64,768]{2,1,0:T(8,128)(2,1)S(1)} async-done(((bf16[8,64,768]{2,1,0:T(8,128)(2,1)}), bf16[8,64,768]{2,1,0:T(8,128)(2,1)S(1)}, u32[]{:S(2)}, u32[]{:S(2)}) %all-to-all-start.1) | async-done | bytes 786464 | tf_op jit(solution)/shard_map/all_to_all | solution.py:313
  75.1 3.0 %collective-permute-start.4 = (bf16[512,768]{1,0:T(8,128)(2,1)S(1)}, bf16[512,768]{1,0:T(8,128)(2,1)}, u32[]{:S(2)}, u32[]{:S(2)}) collective-permute-start(bf16[512,768]{1,0:T(8,128)(2,1)S(1)} %bitcast.10), channel_id=1, source_target_pairs={{448,0},{0,64},{64,128},{128,192},{192,256},{256,320},{320,384},{3... | collective-permute-start | bytes 2359304 | tf_op jit(solution)/shard_map/ppermute | solution.py:65
  78.1 6.6 %collective-permute-start.1 = (bf16[512,768]{1,0:T(8,128)(2,1)S(1)}, bf16[512,768]{1,0:T(8,128)(2,1)}, u32[]{:S(2)}, u32[]{:S(2)}) collective-permute-start(bf16[512,768]{1,0:T(8,128)(2,1)S(1)} %bitcast.11), channel_id=1, source_target_pairs={{64,0},{128,64},{192,128},{256,192},{320,256},{384,320},{448,384},... | collective-permute-start | bytes 2359304 | tf_op jit(solution)/shard_map/ppermute | solution.py:65
  85.6 3.1 %collective-permute-start.2 = (bf16[256,768]{1,0:T(8,128)(2,1)}, bf16[256,768]{1,0:T(8,128)(2,1)}, u32[]{:S(2)}, u32[]{:S(2)}) collective-permute-start(bf16[256,768]{1,0:T(8,128)(2,1)} %bitcast.5), channel_id=1, source_target_pairs={{128,0},{192,64},{256,128},{320,192},{384,256},{448,320},{0,384},{... | collective-permute-start | bytes 1179656 | tf_op jit(solution)/shard_map/ppermute | solution.py:65
  88.7 3.1 %collective-permute-start.3 = (bf16[256,768]{1,0:T(8,128)(2,1)}, bf16[256,768]{1,0:T(8,128)(2,1)}, u32[]{:S(2)}, u32[]{:S(2)}) collective-permute-start(bf16[256,768]{1,0:T(8,128)(2,1)} %bitcast.6), channel_id=1, source_target_pairs={{384,0},{448,64},{0,128},{64,192},{128,256},{192,320},{256,384},{3... | collective-permute-start | bytes 1179656 | tf_op jit(solution)/shard_map/ppermute | solution.py:65
  95.2 5.2 %gated_filter.1 = (f32[384,256]{1,0:T(8,128)S(1)}, f32[8,1,768]{2,1,0:T(1,128)}) custom-call(bf16[384,2048]{1,0:T(8,128)(2,1)S(1)} %norm.2.x_ref, f32[31,256]{1,0:T(8,128)S(1)} %constant_dynamic-slice_fusion.taps_ref, bf16[4,512,512]{2,1,0:T(8,128)(2,1)} %all-gather.7.cloned.1.call-done.weight_ref), custom_call_target="tpu_custom_call" | custom-call | flops 805306368 | bytes 2097152 | tf_op jit(solution)/shard_map/gated_filter/pallas_call | solution.py:121
  100.4 10.4 %all-to-all-start = ((f32[8,1,768]{2,1,0:T(1,128)}), f32[8,1,768]{2,1,0:T(1,128)S(1)}, u32[]{:S(2)}, u32[]{:S(2)}) async-start(f32[8,1,768]{2,1,0:T(1,128)} %get-tuple-element.20), calls=%async_computation | async-start | bytes 49152 | tf_op jit(solution)/shard_map/all_to_all | solution.py:323
  110.9 5.1 %all-to-all-done.sums_ref = f32[8,1,768]{2,1,0:T(1,128)S(1)} async-done(((f32[8,1,768]{2,1,0:T(1,128)}), f32[8,1,768]{2,1,0:T(1,128)S(1)}, u32[]{:S(2)}, u32[]{:S(2)}) %all-to-all-start) | async-done | bytes 24608 | tf_op jit(solution)/shard_map/all_to_all | solution.py:323
  115.9 2.0 %mixer.1 = (bf16[4,384,256]{2,1,0:T(8,128)(2,1)S(1)}, f32[4,384,256]{2,1,0:T(8,128)S(1)}) custom-call(f32[384,256]{1,0:T(8,128)S(1)} %get-tuple-element.19.filtered_ref, f32[8,1,768]{2,1,0:T(1,128)S(1)} %all-to-all-done.sums_ref, f32[1,2048]{1,0:T(1,128)S(1)} %bitcast.19, bf16[512,768]{1,0:T(8,128)(2,1)S(1)} %bitcast.12, ...), custom_call_target="tpu_custom_call" | custom-call | flops 402653184 | bytes 1048576 | tf_op jit(solution)/shard_map/mixer/pallas_call | solution.py:181
  117.9 5.4 %collective-permute-start.5 = (bf16[4,384,256]{2,1,0:T(8,128)(2,1)S(1)}, bf16[4,384,256]{2,1,0:T(8,128)(2,1)S(1)}, u32[]{:S(2)}, u32[]{:S(2)}) collective-permute-start(bf16[4,384,256]{2,1,0:T(8,128)(2,1)S(1)} %get-tuple-element.23), channel_id=1, source_target_pairs={{0,1},{1,0},{2,3},{3,2},{4,5},{5,4},{6,7},{7,6},{8,9},{9,8},{10,11... | collective-permute-start | bytes 2359304 | tf_op jit(solution)/shard_map/ppermute | solution.py:232
  123.3 1.9 collective-permute-done.5
  125.5 15.4 %all_to_all.20 = bf16[4,384,256]{2,1,0:T(8,128)(2,1)S(1)} all-to-all(bf16[4,384,256]{2,1,0:T(8,128)(2,1)S(1)} %add_convert_fusion.1), channel_id=1, replica_groups=mesh['rep'=2,'zl'=4,'y'=8,'x'=4,'c'=2] {'x'}, dimensions={0} | all-to-all | bytes 1572864 | tf_op jit(solution)/shard_map/all_to_all | solution.py:234
  141.1 11.6 %all-gather.2 = bf16[1536,256]{1,0:T(8,128)(2,1)S(1)} all-gather(bf16[384,256]{1,0:T(8,128)(2,1)S(1)} %add_convert_fusion.3), channel_id=4, replica_groups=mesh['rep'=2,'zl'=4,'y'=8,'x'=4,'c'=2] {'x'}, dimensions={0}, use_global_device_ids=true | all-gather | bytes 983040 | tf_op jit(solution)/shard_map/all_gather | solution.py:327
  152.6 6.4 %collective-permute-start.6 = (bf16[4,384,256]{2,1,0:T(8,128)(2,1)S(1)}, bf16[4,384,256]{2,1,0:T(8,128)(2,1)S(1)}, u32[]{:S(2)}, u32[]{:S(2)}) collective-permute-start(bf16[4,384,256]{2,1,0:T(8,128)(2,1)S(1)} %bitcast.16), channel_id=1, source_target_pairs={{0,1},{1,0},{2,3},{3,2},{4,5},{5,4},{6,7},{7,6},{8,9},{9,8},{10,11... | collective-permute-start | bytes 2359304 | tf_op jit(solution)/shard_map/ppermute | solution.py:214
  159.0 1.9 collective-permute-done.6.other_ref
  162.1 5.8 %feed_forward.1 = (bf16[4,384,256]{2,1,0:T(8,128)(2,1)S(1)}, f32[4,384,256]{2,1,0:T(8,128)S(1)}) custom-call(bf16[384,2048]{1,0:T(8,128)(2,1)S(1)} %norm.3.x_ref, bf16[4,512,1024]{2,1,0:T(8,128)(2,1)} %all-gather.9.cloned.1.call-done.first_ref, bf16[512,768]{1,0:T(8,128)(2,1)S(1)} %bitcast.13, bf16[512,768]{1,0:T(8,128)(2,1)} %collective-permute-done.1.refs_1_, ...), custom_call_target="tpu_custom_call" | custom-call | flops 2415919104 | bytes 6291456 | tf_op jit(solution)/shard_map/feed_forward/pallas_call | solution.py:285
  167.9 2.3 %collective-permute-start.7 = (bf16[4,384,256]{2,1,0:T(8,128)(2,1)S(1)}, bf16[4,384,256]{2,1,0:T(8,128)(2,1)S(1)}, u32[]{:S(2)}, u32[]{:S(2)}) collective-permute-start(bf16[4,384,256]{2,1,0:T(8,128)(2,1)S(1)} %get-tuple-element.26), channel_id=1, source_target_pairs={{0,1},{1,0},{2,3},{3,2},{4,5},{5,4},{6,7},{7,6},{8,9},{9,8},{10,11... | collective-permute-start | bytes 2359304 | tf_op jit(solution)/shard_map/ppermute | solution.py:232
  172.3 14.3 %all_to_all.21 = bf16[4,384,256]{2,1,0:T(8,128)(2,1)S(1)} all-to-all(bf16[4,384,256]{2,1,0:T(8,128)(2,1)S(1)} %add_convert_fusion), channel_id=1, replica_groups=mesh['rep'=2,'zl'=4,'y'=8,'x'=4,'c'=2] {'x'}, dimensions={0} | all-to-all | bytes 1572864 | tf_op jit(solution)/shard_map/all_to_all | solution.py:234
  (38 shorter events, 8.9 us)
Async XLA Ops:
  6.5 39.2 %copy-start = (f32[31,2048]{1,0:T(8,128)S(1)}, f32[31,2048]{1,0:T(8,128)}, u32[]{:S(2)}) copy-start(f32[31,2048]{1,0:T(8,128)} %param.14) | copy-start | bytes 761860
  6.5 88.6 %all-gather.7.cloned.1.call-start = ((), (), s32[]{:S(2)}) async-start(), calls=%async_computation.4 | async-start | bytes 2359296 | tf_op jit(solution)/shard_map/all_gather | solution.py:58
  25.9 19.8 %copy-start.6 = (bf16[384,256]{1,0:T(8,128)(2,1)S(1)}, bf16[384,256]{1,0:T(8,128)(2,1)}, u32[]{:S(2)}) copy-start(bf16[384,256]{1,0:T(8,128)(2,1)} %param.10) | copy-start | bytes 589828
  26.0 136.1 %all-gather.9.cloned.1.call-start = ((), (), s32[]{:S(2)}) async-start(), calls=%async_computation.5 | async-start | bytes 4718592 | tf_op jit(solution)/shard_map/all_gather | solution.py:58
  39.5 35.7 %all-to-all-start.1 = ((bf16[8,64,768]{2,1,0:T(8,128)(2,1)}), bf16[8,64,768]{2,1,0:T(8,128)(2,1)S(1)}, u32[]{:S(2)}, u32[]{:S(2)}) async-start(bf16[8,64,768]{2,1,0:T(8,128)(2,1)} %get-tuple-element.21), calls=%async_computation.1 | async-start | bytes 1572864 | tf_op jit(solution)/shard_map/all_to_all | solution.py:313
  45.7 47.1 %copy-start.3 = (f32[2048]{0:T(1024)S(1)}, f32[2048]{0:T(1024)}, u32[]{:S(2)}) copy-start(f32[2048]{0:T(1024)} %param.11) | copy-start | bytes 24580
  57.3 34.5 %collective-permute-start = (bf16[4,384,256]{2,1,0:T(8,128)(2,1)S(1)}, bf16[4,384,256]{2,1,0:T(8,128)(2,1)S(1)}, u32[]{:S(2)}, u32[]{:S(2)}) collective-permute-start(bf16[4,384,256]{2,1,0:T(8,128)(2,1)S(1)} %bitcast.14), channel_id=1, source_target_pairs={{0,1},{1,0},{2,3},{3,2},{4,5},{5,4},{6,7},{7,6},{8,9},{9,8},{10,11... | collective-permute-start | bytes 2359304 | tf_op jit(solution)/shard_map/ppermute | solution.py:214
  75.1 35.8 %collective-permute-start.4 = (bf16[512,768]{1,0:T(8,128)(2,1)S(1)}, bf16[512,768]{1,0:T(8,128)(2,1)}, u32[]{:S(2)}, u32[]{:S(2)}) collective-permute-start(bf16[512,768]{1,0:T(8,128)(2,1)S(1)} %bitcast.10), channel_id=1, source_target_pairs={{448,0},{0,64},{64,128},{128,192},{192,256},{256,320},{320,384},{3... | collective-permute-start | bytes 2359304 | tf_op jit(solution)/shard_map/ppermute | solution.py:65
  78.1 32.8 %collective-permute-start.1 = (bf16[512,768]{1,0:T(8,128)(2,1)S(1)}, bf16[512,768]{1,0:T(8,128)(2,1)}, u32[]{:S(2)}, u32[]{:S(2)}) collective-permute-start(bf16[512,768]{1,0:T(8,128)(2,1)S(1)} %bitcast.11), channel_id=1, source_target_pairs={{64,0},{128,64},{192,128},{256,192},{320,256},{384,320},{448,384},... | collective-permute-start | bytes 2359304 | tf_op jit(solution)/shard_map/ppermute | solution.py:65
  85.6 25.2 %collective-permute-start.2 = (bf16[256,768]{1,0:T(8,128)(2,1)}, bf16[256,768]{1,0:T(8,128)(2,1)}, u32[]{:S(2)}, u32[]{:S(2)}) collective-permute-start(bf16[256,768]{1,0:T(8,128)(2,1)} %bitcast.5), channel_id=1, source_target_pairs={{128,0},{192,64},{256,128},{320,192},{384,256},{448,320},{0,384},{... | collective-permute-start | bytes 1179656 | tf_op jit(solution)/shard_map/ppermute | solution.py:65
  88.7 22.1 %collective-permute-start.3 = (bf16[256,768]{1,0:T(8,128)(2,1)}, bf16[256,768]{1,0:T(8,128)(2,1)}, u32[]{:S(2)}, u32[]{:S(2)}) collective-permute-start(bf16[256,768]{1,0:T(8,128)(2,1)} %bitcast.6), channel_id=1, source_target_pairs={{384,0},{448,64},{0,128},{64,192},{128,256},{192,320},{256,384},{3... | collective-permute-start | bytes 1179656 | tf_op jit(solution)/shard_map/ppermute | solution.py:65
  91.8 1.0 copy-start.1
  92.8 1.1 copy-start.2
  95.2 20.8 %copy-start.4 = (f32[2048]{0:T(1024)S(1)}, f32[2048]{0:T(1024)}, u32[]{:S(2)}) copy-start(f32[2048]{0:T(1024)} %param.15) | copy-start | bytes 24580
  100.4 15.5 %all-to-all-start = ((f32[8,1,768]{2,1,0:T(1,128)}), f32[8,1,768]{2,1,0:T(1,128)S(1)}, u32[]{:S(2)}, u32[]{:S(2)}) async-start(f32[8,1,768]{2,1,0:T(1,128)} %get-tuple-element.20), calls=%async_computation | async-start | bytes 49152 | tf_op jit(solution)/shard_map/all_to_all | solution.py:323
  117.9 7.3 %collective-permute-start.5 = (bf16[4,384,256]{2,1,0:T(8,128)(2,1)S(1)}, bf16[4,384,256]{2,1,0:T(8,128)(2,1)S(1)}, u32[]{:S(2)}, u32[]{:S(2)}) collective-permute-start(bf16[4,384,256]{2,1,0:T(8,128)(2,1)S(1)} %get-tuple-element.23), channel_id=1, source_target_pairs={{0,1},{1,0},{2,3},{3,2},{4,5},{5,4},{6,7},{7,6},{8,9},{9,8},{10,11... | collective-permute-start | bytes 2359304 | tf_op jit(solution)/shard_map/ppermute | solution.py:232
  125.5 15.5 %copy-start.7 = (bf16[384,256]{1,0:T(8,128)(2,1)S(1)}, bf16[384,256]{1,0:T(8,128)(2,1)}, u32[]{:S(2)}) copy-start(bf16[384,256]{1,0:T(8,128)(2,1)} %param.10) | copy-start | bytes 589828
  140.9 20.0 %copy-start.5 = (f32[2048]{0:T(1024)S(1)}, f32[2048]{0:T(1024)}, u32[]{:S(2)}) copy-start(f32[2048]{0:T(1024)} %param.17) | copy-start | bytes 24580
  152.6 8.3 %collective-permute-start.6 = (bf16[4,384,256]{2,1,0:T(8,128)(2,1)S(1)}, bf16[4,384,256]{2,1,0:T(8,128)(2,1)S(1)}, u32[]{:S(2)}, u32[]{:S(2)}) collective-permute-start(bf16[4,384,256]{2,1,0:T(8,128)(2,1)S(1)} %bitcast.16), channel_id=1, source_target_pairs={{0,1},{1,0},{2,3},{3,2},{4,5},{5,4},{6,7},{7,6},{8,9},{9,8},{10,11... | collective-permute-start | bytes 2359304 | tf_op jit(solution)/shard_map/ppermute | solution.py:214
  167.9 4.2 %collective-permute-start.7 = (bf16[4,384,256]{2,1,0:T(8,128)(2,1)S(1)}, bf16[4,384,256]{2,1,0:T(8,128)(2,1)S(1)}, u32[]{:S(2)}, u32[]{:S(2)}) collective-permute-start(bf16[4,384,256]{2,1,0:T(8,128)(2,1)S(1)} %get-tuple-element.26), channel_id=1, source_target_pairs={{0,1},{1,0},{2,3},{3,2},{4,5},{5,4},{6,7},{7,6},{8,9},{9,8},{10,11... | collective-permute-start | bytes 2359304 | tf_op jit(solution)/shard_map/ppermute | solution.py:232
Sparse Core Ops, SparseCore 0:
  26.1 58.3 all-gather.6
  86.6 57.6 all-gather.8

commit v2 on v1

--- a/solution.py
+++ b/solution.py
@@ -59,12 +59,12 @@
 
 
 def over_z(slab):
-    half = slab.shape[0] // 2
-
-    def from_z(piece, step):
-        return lax.ppermute(piece, ("rep", "zl"), [((i + step) % 8, i) for i in range(8)])
-
-    return [slab, from_z(slab, 1), from_z(slab[:half], 2), from_z(slab[half:], -2), from_z(slab, -1)]
+    def from_z(step):
+        pairs = [((i + step(i)) % 8, i) for i in range(8)]
+        return lax.ppermute(slab, ("rep", "zl"), pairs)
+
+    two = from_z(lambda i: 2 if i % 2 == 0 else -2)
+    return [slab, from_z(lambda i: 1), two, from_z(lambda i: -1)]
 
 
 def gate_kernel(x_ref, taps_ref, weight_ref, filtered_ref, sums_ref, padded_ref, held_ref, sems):
@@ -131,7 +131,7 @@
             pltpu.VMEM((count, depth, 2 * width), jnp.bfloat16),
             pltpu.SemaphoreType.DMA((count,)),
         ],
-        compiler_params=pltpu.CompilerParams(vmem_limit_bytes=51 * MIB),
+        compiler_params=pltpu.CompilerParams(vmem_limit_bytes=52 * MIB),
         cost_estimate=pl.CostEstimate(
             flops=4 * rows * D * width, bytes_accessed=4 * D * width, transcendentals=rows * width
         ),
@@ -142,11 +142,10 @@
 def fetched(slab_refs, held_ref, columns, sems):
     here, count = lax.axis_index("zl"), lax.axis_size("zl")
     copies = []
-    for i, (ref, turn) in enumerate(zip(slab_refs, (0, 1, 2, 2, 3))):
-        low = ref.shape[0] if i == 3 else 0
-        to = held_ref.at[lax.rem(here + turn, count), low : low + ref.shape[0]]
-        copies.append(pltpu.make_async_copy(ref.at[:, columns], to, sems.at[i]))
-        copies[i].start()
+    for turn, ref in enumerate(slab_refs):
+        to = held_ref.at[lax.rem(here + turn, count)]
+        copies.append(pltpu.make_async_copy(ref.at[:, columns], to, sems.at[turn]))
+        copies[turn].start()
     return copies
 
 
@@ -184,13 +183,13 @@
         out_specs=(vmem, vmem),
         out_shape=(
             jax.ShapeDtypeStruct(out, jnp.bfloat16),
-            jax.ShapeDtypeStruct(out, jnp.float32),
+            jax.ShapeDtypeStruct(out, jnp.bfloat16),
         ),
         scratch_shapes=[
             pltpu.VMEM((out[0], 2 * width, width), jnp.bfloat16),
             pltpu.SemaphoreType.DMA((len(slabs),)),
         ],
-        compiler_params=pltpu.CompilerParams(vmem_limit_bytes=24 * MIB),
+        compiler_params=pltpu.CompilerParams(vmem_limit_bytes=52 * MIB),
         cost_estimate=pl.CostEstimate(
             flops=2 * rows * D * width, bytes_accessed=2 * D * width, transcendentals=rows * width
         ),
@@ -230,7 +229,7 @@
 
 def over_group(mine, theirs):
     got = lax.ppermute(theirs, "c", SWAP)
-    pair = (mine + got.astype(jnp.float32)).astype(jnp.bfloat16)
+    pair = (mine.astype(jnp.float32) + got.astype(jnp.float32)).astype(jnp.bfloat16)
     return jnp.sum(lax.all_to_all(pair, "x", 0, 0, tiled=True).astype(jnp.float32), axis=0)
 
 
@@ -288,7 +287,7 @@
         out_specs=(vmem, vmem),
         out_shape=(
             jax.ShapeDtypeStruct(out, jnp.bfloat16),
-            jax.ShapeDtypeStruct(out, jnp.float32),
+            jax.ShapeDtypeStruct(out, jnp.bfloat16),
         ),
         scratch_shapes=[
             weights,
@@ -297,7 +296,7 @@
             pltpu.VMEM((rows, hidden), jnp.bfloat16),
             pltpu.SemaphoreType.DMA((columns // width + 1 + len(late),)),
         ],
-        compiler_params=pltpu.CompilerParams(vmem_limit_bytes=46 * MIB),
+        compiler_params=pltpu.CompilerParams(vmem_limit_bytes=52 * MIB),
         cost_estimate=pl.CostEstimate(
             flops=4 * rows * D * hidden, bytes_accessed=4 * D * hidden, transcendentals=0
         ),

time: 195 us -> 199 us (1.021)
  waiting for transfers between devices: 17.8 us -> 25.7 us
  starting transfers between devices: 57.3 us -> 54.1 us
    ppermute x4 -> x3, waiting for transfers between devices: 0.01 us -> 12.9 us  [from_z(): return lax.ppermute(slab, ('rep', 'zl'), pairs)]
    all_to_all x1, waiting for transfers between devices: 5.06 us -> 0.01 us  [body(): sums = lax.all_to_all(sums, TP, 0, 0, tiled=True)]
    ppermute x4 -> x3, starting transfers between devices: 15.7 us -> 12.9 us  [from_z(): return lax.ppermute(slab, ('rep', 'zl'), pairs)]
  transfers between devices with their start and end apart: 12 -> 11, of which waited for: 5 -> 5; matrix products, arithmetic and copies ran while one was open for 1% -> 0% of each run, Pallas kernels for 5% -> 5%
where the time goes in v2:
time: 199 us; the launch traced here: 198 us
  blocking collectives  83.6 us (42%)
  starting transfers between devices  54.1 us (27%)
  waiting for transfers between devices  25.7 us (13%)
  Pallas kernels  18.9 us (9%)
  between operations  13.6 us (7%)
    all_to_all x2, blocking collectives, over_group(): lax.all_to_all(pair, 'x', 0, 0, tiled=True).astype(jnp.float32)  29.6 us
    all_gather x1, blocking collectives, body(): gates = lax.all_gather(gates, 'zl', axis=0)  17.4 us
    ppermute x2, starting transfers between devices, normed_channels(): other = lax.ppermute(own, 'c', SWAP)  17.2 us
    all_gather x1, blocking collectives, body(): first = lax.all_gather(first, 'zl', axis=0)  13.4 us
    ppermute x3, waiting for transfers between devices, from_z(): return lax.ppermute(slab, ('rep', 'zl'), pairs)  12.9 us
    ppermute x3, starting transfers between devices, from_z(): return lax.ppermute(slab, ('rep', 'zl'), pairs)  12.9 us
    all_gather x1, blocking collectives, body(): own = lax.all_gather(states, 'x', axis=0)  11.6 us
    all_gather x1, blocking collectives, body(): normed_mid = normed_channels(lax.all_gather(middle, 'x', axis=0), mlp_gain)  11.6 us
  transfers between devices with their start and end apart: 11, of which 5 were waited for; matrix products, arithmetic and copies ran while one was open for 0% of the time, Pallas kernels for 5%

profile of v2, /device:TPU:1, one launch (start us, length us, event | category | flops | bytes accessed | tf_op | source)
XLA Modules:
  0.0 198.4 jit_solution(1683444527575517240)
XLA Ops:
  6.5 2.0 %pack.1 = (bf16[64,512]{1,0:T(8,128)(2,1)}, bf16[64,1024]{1,0:T(8,128)(2,1)}, bf16[8,64,768]{2,1,0:T(8,128)(2,1)}) custom-call(bf16[64,256]{1,0:T(8,128)(2,1)} %value_ref.1, bf16[64,256]{1,0:T(8,128)(2,1)} %gate_ref.1, bf16[64,256]{1,0:T(8,128)(2,1)} %out_ref.1, bf16[64,768]{1,0:T(8,128)(2,1)} %up_ref.1, bf16[64,768]{1,0:T(8,128)(2,1)} %down_ref.1), custom_call_target="tpu_custom_call" | custom-call | bytes 1048576 | tf_op jit(solution)/shard_map/pack/pallas_call | solution.py:44
  8.5 17.4 %all-gather.1 = bf16[256,512]{1,0:T(8,128)(2,1)} all-gather(bf16[64,512]{1,0:T(8,128)(2,1)} %get-tuple-element.18), channel_id=3, replica_groups=mesh['rep'=2,'zl'=4,'y'=8,'x'=4,'c'=2] {'zl'}, dimensions={0}, use_global_device_ids=true | all-gather | bytes 327680 | tf_op jit(solution)/shard_map/all_gather | solution.py:313
  26.0 13.4 %all-gather.3 = bf16[256,1024]{1,0:T(8,128)(2,1)} all-gather(bf16[64,1024]{1,0:T(8,128)(2,1)} %get-tuple-element.24), channel_id=5, replica_groups=mesh['rep'=2,'zl'=4,'y'=8,'x'=4,'c'=2] {'zl'}, dimensions={0}, use_global_device_ids=true | all-gather | bytes 655360 | tf_op jit(solution)/shard_map/all_gather | solution.py:314
  39.4 6.2 %all-to-all-start.1 = ((bf16[8,64,768]{2,1,0:T(8,128)(2,1)}), bf16[8,64,768]{2,1,0:T(8,128)(2,1)}, u32[]{:S(2)}, u32[]{:S(2)}) async-start(bf16[8,64,768]{2,1,0:T(8,128)(2,1)} %get-tuple-element.21), calls=%async_computation.1 | async-start | bytes 1572864 | tf_op jit(solution)/shard_map/all_to_all | solution.py:312
  45.7 11.6 %all-gather = bf16[1536,256]{1,0:T(8,128)(2,1)S(1)} all-gather(bf16[384,256]{1,0:T(8,128)(2,1)S(1)} %copy-done.5), channel_id=2, replica_groups=mesh['rep'=2,'zl'=4,'y'=8,'x'=4,'c'=2] {'x'}, dimensions={0}, use_global_device_ids=true | all-gather | bytes 983040 | tf_op jit(solution)/shard_map/all_gather | solution.py:316
  57.3 10.8 %collective-permute-start = (bf16[4,384,256]{2,1,0:T(8,128)(2,1)S(1)}, bf16[4,384,256]{2,1,0:T(8,128)(2,1)S(1)}, u32[]{:S(2)}, u32[]{:S(2)}) collective-permute-start(bf16[4,384,256]{2,1,0:T(8,128)(2,1)S(1)} %bitcast.8), channel_id=1, source_target_pairs={{0,1},{1,0},{2,3},{3,2},{4,5},{5,4},{6,7},{7,6},{8,9},{9,8},{10,11... | collective-permute-start | bytes 2359304 | tf_op jit(solution)/shard_map/ppermute | solution.py:213
  68.1 7.1 %all-to-all-done.1 = bf16[8,64,768]{2,1,0:T(8,128)(2,1)} async-done(((bf16[8,64,768]{2,1,0:T(8,128)(2,1)}), bf16[8,64,768]{2,1,0:T(8,128)(2,1)}, u32[]{:S(2)}, u32[]{:S(2)}) %all-to-all-start.1) | async-done | bytes 786464 | tf_op jit(solution)/shard_map/all_to_all | solution.py:312
  75.2 3.0 %collective-permute-start.3 = (bf16[512,768]{1,0:T(8,128)(2,1)}, bf16[512,768]{1,0:T(8,128)(2,1)}, u32[]{:S(2)}, u32[]{:S(2)}) collective-permute-start(bf16[512,768]{1,0:T(8,128)(2,1)} %bitcast.4.refs_0_), channel_id=1, source_target_pairs={{448,0},{0,64},{64,128},{128,192},{192,256},{256,320},{320,384},{3... | collective-permute-start | bytes 2359304 | tf_op jit(solution)/shard_map/ppermute | solution.py:64
  78.2 7.9 %collective-permute-start.2 = (bf16[512,768]{1,0:T(8,128)(2,1)}, bf16[512,768]{1,0:T(8,128)(2,1)}, u32[]{:S(2)}, u32[]{:S(2)}) collective-permute-start(bf16[512,768]{1,0:T(8,128)(2,1)} %bitcast.4.refs_0_), channel_id=1, source_target_pairs={{128,0},{448,64},{256,128},{64,192},{384,256},{192,320},{0,384},{3... | collective-permute-start | bytes 2359304 | tf_op jit(solution)/shard_map/ppermute | solution.py:64
  86.2 1.9 collective-permute-start.1
  89.4 5.2 %gated_filter.1 = (f32[384,256]{1,0:T(8,128)S(1)}, f32[8,1,768]{2,1,0:T(1,128)}) custom-call(bf16[384,2048]{1,0:T(8,128)(2,1)S(1)} %norm.2.x_ref, f32[31,256]{1,0:T(8,128)S(1)} %constant_dynamic-slice_fusion.taps_ref, bf16[4,512,512]{2,1,0:T(8,128)(2,1)} %all-gather.7.cloned.1.call-done.weight_ref), custom_call_target="tpu_custom_call" | custom-call | flops 805306368 | bytes 2097152 | tf_op jit(solution)/shard_map/gated_filter/pallas_call | solution.py:121
  94.6 9.5 %all-to-all-start = ((f32[8,1,768]{2,1,0:T(1,128)}), f32[8,1,768]{2,1,0:T(1,128)S(1)}, u32[]{:S(2)}, u32[]{:S(2)}) async-start(f32[8,1,768]{2,1,0:T(1,128)} %get-tuple-element.20), calls=%async_computation | async-start | bytes 49152 | tf_op jit(solution)/shard_map/all_to_all | solution.py:322
  104.1 12.9 %collective-permute-done.1.refs_1_ = bf16[512,768]{1,0:T(8,128)(2,1)} collective-permute-done((bf16[512,768]{1,0:T(8,128)(2,1)}, bf16[512,768]{1,0:T(8,128)(2,1)}, u32[]{:S(2)}, u32[]{:S(2)}) %collective-permute-start.1) | collective-permute-done | bytes 786464 | tf_op jit(solution)/shard_map/ppermute | solution.py:64
  117.0 2.0 %mixer.1 = (bf16[4,384,256]{2,1,0:T(8,128)(2,1)S(1)}, bf16[4,384,256]{2,1,0:T(8,128)(2,1)S(1)}) custom-call(f32[384,256]{1,0:T(8,128)S(1)} %get-tuple-element.19.filtered_ref, f32[8,1,768]{2,1,0:T(1,128)S(1)} %all-to-all-done.sums_ref, f32[1,2048]{1,0:T(1,128)S(1)} %bitcast.13, bf16[512,768]{1,0:T(8,128)(2,1)} %bitcast.4.refs_0_, ...), custom_call_target="tpu_custom_call" | custom-call | flops 402653184 | bytes 1048576 | tf_op jit(solution)/shard_map/mixer/pallas_call | solution.py:180
  119.0 6.0 %collective-permute-start.4 = (bf16[4,384,256]{2,1,0:T(8,128)(2,1)S(1)}, bf16[4,384,256]{2,1,0:T(8,128)(2,1)S(1)}, u32[]{:S(2)}, u32[]{:S(2)}) collective-permute-start(bf16[4,384,256]{2,1,0:T(8,128)(2,1)S(1)} %get-tuple-element.23), channel_id=1, source_target_pairs={{0,1},{1,0},{2,3},{3,2},{4,5},{5,4},{6,7},{7,6},{8,9},{9,8},{10,11... | collective-permute-start | bytes 2359304 | tf_op jit(solution)/shard_map/ppermute | solution.py:231
  125.0 1.9 collective-permute-done.4
  127.1 15.3 %all_to_all.20 = bf16[4,384,256]{2,1,0:T(8,128)(2,1)S(1)} all-to-all(bf16[4,384,256]{2,1,0:T(8,128)(2,1)S(1)} %add_convert_fusion.1), channel_id=1, replica_groups=mesh['rep'=2,'zl'=4,'y'=8,'x'=4,'c'=2] {'x'}, dimensions={0} | all-to-all | bytes 1572864 | tf_op jit(solution)/shard_map/all_to_all | solution.py:233
  142.6 11.6 %all-gather.2 = bf16[1536,256]{1,0:T(8,128)(2,1)S(1)} all-gather(bf16[384,256]{1,0:T(8,128)(2,1)S(1)} %add_convert_fusion.3), channel_id=4, replica_groups=mesh['rep'=2,'zl'=4,'y'=8,'x'=4,'c'=2] {'x'}, dimensions={0}, use_global_device_ids=true | all-gather | bytes 983040 | tf_op jit(solution)/shard_map/all_gather | solution.py:326
  154.2 6.3 %collective-permute-start.5 = (bf16[4,384,256]{2,1,0:T(8,128)(2,1)S(1)}, bf16[4,384,256]{2,1,0:T(8,128)(2,1)S(1)}, u32[]{:S(2)}, u32[]{:S(2)}) collective-permute-start(bf16[4,384,256]{2,1,0:T(8,128)(2,1)S(1)} %bitcast.10), channel_id=1, source_target_pairs={{0,1},{1,0},{2,3},{3,2},{4,5},{5,4},{6,7},{7,6},{8,9},{9,8},{10,11... | collective-permute-start | bytes 2359304 | tf_op jit(solution)/shard_map/ppermute | solution.py:213
  160.6 1.9 collective-permute-done.5.other_ref
  164.9 7.2 %feed_forward.1 = (bf16[4,384,256]{2,1,0:T(8,128)(2,1)S(1)}, bf16[4,384,256]{2,1,0:T(8,128)(2,1)S(1)}) custom-call(bf16[384,2048]{1,0:T(8,128)(2,1)} %copy-done.1, bf16[4,512,1024]{2,1,0:T(8,128)(2,1)} %all-gather.9.cloned.1.call-done.first_ref, bf16[512,768]{1,0:T(8,128)(2,1)} %bitcast.4.refs_0_, bf16[512,768]{1,0:T(8,128)(2,1)} %collective-permute-done.1.refs_1_, ...), custom_call_target="tpu_custom_call" | custom-call | flops 2415919104 | bytes 6291456 | tf_op jit(solution)/shard_map/feed_forward/pallas_call | solution.py:284
  172.1 2.3 %collective-permute-start.6 = (bf16[4,384,256]{2,1,0:T(8,128)(2,1)S(1)}, bf16[4,384,256]{2,1,0:T(8,128)(2,1)S(1)}, u32[]{:S(2)}, u32[]{:S(2)}) collective-permute-start(bf16[4,384,256]{2,1,0:T(8,128)(2,1)S(1)} %get-tuple-element.26), channel_id=1, source_target_pairs={{0,1},{1,0},{2,3},{3,2},{4,5},{5,4},{6,7},{7,6},{8,9},{9,8},{10,11... | collective-permute-start | bytes 2359304 | tf_op jit(solution)/shard_map/ppermute | solution.py:231
  174.4 1.9 collective-permute-done.6
  176.4 14.3 %all_to_all.21 = bf16[4,384,256]{2,1,0:T(8,128)(2,1)S(1)} all-to-all(bf16[4,384,256]{2,1,0:T(8,128)(2,1)S(1)} %add_convert_fusion), channel_id=1, replica_groups=mesh['rep'=2,'zl'=4,'y'=8,'x'=4,'c'=2] {'x'}, dimensions={0} | all-to-all | bytes 1572864 | tf_op jit(solution)/shard_map/all_to_all | solution.py:233
  (33 shorter events, 5.1 us)
Async XLA Ops:
  6.5 39.2 %copy-start = (f32[31,2048]{1,0:T(8,128)S(1)}, f32[31,2048]{1,0:T(8,128)}, u32[]{:S(2)}) copy-start(f32[31,2048]{1,0:T(8,128)} %param.14) | copy-start | bytes 761860
  6.5 82.8 %all-gather.7.cloned.1.call-start = ((), (), s32[]{:S(2)}) async-start(), calls=%async_computation.4 | async-start | bytes 2359296 | tf_op jit(solution)/shard_map/all_gather | solution.py:58
  25.9 19.8 %copy-start.5 = (bf16[384,256]{1,0:T(8,128)(2,1)S(1)}, bf16[384,256]{1,0:T(8,128)(2,1)}, u32[]{:S(2)}) copy-start(bf16[384,256]{1,0:T(8,128)(2,1)} %param.10) | copy-start | bytes 589828
  25.9 138.9 %all-gather.9.cloned.1.call-start = ((), (), s32[]{:S(2)}) async-start(), calls=%async_computation.5 | async-start | bytes 4718592 | tf_op jit(solution)/shard_map/all_gather | solution.py:58
  39.4 48.7 %copy-start.2 = (f32[2048]{0:T(1024)S(1)}, f32[2048]{0:T(1024)}, u32[]{:S(2)}) copy-start(f32[2048]{0:T(1024)} %param.11) | copy-start | bytes 24580
  39.4 35.8 %all-to-all-start.1 = ((bf16[8,64,768]{2,1,0:T(8,128)(2,1)}), bf16[8,64,768]{2,1,0:T(8,128)(2,1)}, u32[]{:S(2)}, u32[]{:S(2)}) async-start(bf16[8,64,768]{2,1,0:T(8,128)(2,1)} %get-tuple-element.21), calls=%async_computation.1 | async-start | bytes 1572864 | tf_op jit(solution)/shard_map/all_to_all | solution.py:312
  57.3 30.8 %collective-permute-start = (bf16[4,384,256]{2,1,0:T(8,128)(2,1)S(1)}, bf16[4,384,256]{2,1,0:T(8,128)(2,1)S(1)}, u32[]{:S(2)}, u32[]{:S(2)}) collective-permute-start(bf16[4,384,256]{2,1,0:T(8,128)(2,1)S(1)} %bitcast.8), channel_id=1, source_target_pairs={{0,1},{1,0},{2,3},{3,2},{4,5},{5,4},{6,7},{7,6},{8,9},{9,8},{10,11... | collective-permute-start | bytes 2359304 | tf_op jit(solution)/shard_map/ppermute | solution.py:213
  75.2 28.9 %collective-permute-start.3 = (bf16[512,768]{1,0:T(8,128)(2,1)}, bf16[512,768]{1,0:T(8,128)(2,1)}, u32[]{:S(2)}, u32[]{:S(2)}) collective-permute-start(bf16[512,768]{1,0:T(8,128)(2,1)} %bitcast.4.refs_0_), channel_id=1, source_target_pairs={{448,0},{0,64},{64,128},{128,192},{192,256},{256,320},{320,384},{3... | collective-permute-start | bytes 2359304 | tf_op jit(solution)/shard_map/ppermute | solution.py:64
  78.2 25.9 %collective-permute-start.2 = (bf16[512,768]{1,0:T(8,128)(2,1)}, bf16[512,768]{1,0:T(8,128)(2,1)}, u32[]{:S(2)}, u32[]{:S(2)}) collective-permute-start(bf16[512,768]{1,0:T(8,128)(2,1)} %bitcast.4.refs_0_), channel_id=1, source_target_pairs={{128,0},{448,64},{256,128},{64,192},{384,256},{192,320},{0,384},{3... | collective-permute-start | bytes 2359304 | tf_op jit(solution)/shard_map/ppermute | solution.py:64
  86.2 30.8 %collective-permute-start.1 = (bf16[512,768]{1,0:T(8,128)(2,1)}, bf16[512,768]{1,0:T(8,128)(2,1)}, u32[]{:S(2)}, u32[]{:S(2)}) collective-permute-start(bf16[512,768]{1,0:T(8,128)(2,1)} %bitcast.4.refs_0_), channel_id=1, source_target_pairs={{64,0},{128,64},{192,128},{256,192},{320,256},{384,320},{448,384},... | collective-permute-start | bytes 2359304 | tf_op jit(solution)/shard_map/ppermute | solution.py:64
  89.3 27.7 %copy-start.3 = (f32[2048]{0:T(1024)S(1)}, f32[2048]{0:T(1024)}, u32[]{:S(2)}) copy-start(f32[2048]{0:T(1024)} %param.15) | copy-start | bytes 24580
  94.6 22.4 %all-to-all-start = ((f32[8,1,768]{2,1,0:T(1,128)}), f32[8,1,768]{2,1,0:T(1,128)S(1)}, u32[]{:S(2)}, u32[]{:S(2)}) async-start(f32[8,1,768]{2,1,0:T(1,128)} %get-tuple-element.20), calls=%async_computation | async-start | bytes 49152 | tf_op jit(solution)/shard_map/all_to_all | solution.py:322
  119.0 7.9 %collective-permute-start.4 = (bf16[4,384,256]{2,1,0:T(8,128)(2,1)S(1)}, bf16[4,384,256]{2,1,0:T(8,128)(2,1)S(1)}, u32[]{:S(2)}, u32[]{:S(2)}) collective-permute-start(bf16[4,384,256]{2,1,0:T(8,128)(2,1)S(1)} %get-tuple-element.23), channel_id=1, source_target_pairs={{0,1},{1,0},{2,3},{3,2},{4,5},{5,4},{6,7},{7,6},{8,9},{9,8},{10,11... | collective-permute-start | bytes 2359304 | tf_op jit(solution)/shard_map/ppermute | solution.py:231
  127.1 15.5 %copy-start.6 = (bf16[384,256]{1,0:T(8,128)(2,1)S(1)}, bf16[384,256]{1,0:T(8,128)(2,1)}, u32[]{:S(2)}) copy-start(bf16[384,256]{1,0:T(8,128)(2,1)} %param.10) | copy-start | bytes 589828
  142.5 20.0 %copy-start.4 = (f32[2048]{0:T(1024)S(1)}, f32[2048]{0:T(1024)}, u32[]{:S(2)}) copy-start(f32[2048]{0:T(1024)} %param.17) | copy-start | bytes 24580
  154.2 8.2 %collective-permute-start.5 = (bf16[4,384,256]{2,1,0:T(8,128)(2,1)S(1)}, bf16[4,384,256]{2,1,0:T(8,128)(2,1)S(1)}, u32[]{:S(2)}, u32[]{:S(2)}) collective-permute-start(bf16[4,384,256]{2,1,0:T(8,128)(2,1)S(1)} %bitcast.10), channel_id=1, source_target_pairs={{0,1},{1,0},{2,3},{3,2},{4,5},{5,4},{6,7},{7,6},{8,9},{9,8},{10,11... | collective-permute-start | bytes 2359304 | tf_op jit(solution)/shard_map/ppermute | solution.py:213
  163.7 1.2 copy-start.1
  172.1 4.2 %collective-permute-start.6 = (bf16[4,384,256]{2,1,0:T(8,128)(2,1)S(1)}, bf16[4,384,256]{2,1,0:T(8,128)(2,1)S(1)}, u32[]{:S(2)}, u32[]{:S(2)}) collective-permute-start(bf16[4,384,256]{2,1,0:T(8,128)(2,1)S(1)} %get-tuple-element.26), channel_id=1, source_target_pairs={{0,1},{1,0},{2,3},{3,2},{4,5},{5,4},{6,7},{7,6},{8,9},{9,8},{10,11... | collective-permute-start | bytes 2359304 | tf_op jit(solution)/shard_map/ppermute | solution.py:231
Sparse Core Ops, SparseCore 0:
  26.1 58.3 all-gather.6
  86.6 57.6 all-gather.8

commit v3 on v2

--- a/solution.py
+++ b/solution.py
@@ -63,24 +63,29 @@
         pairs = [((i + step(i)) % 8, i) for i in range(8)]
         return lax.ppermute(slab, ("rep", "zl"), pairs)
 
+    one, three = from_z(lambda i: 1), from_z(lambda i: -1)
     two = from_z(lambda i: 2 if i % 2 == 0 else -2)
-    return [slab, from_z(lambda i: 1), two, from_z(lambda i: -1)]
+    return [slab, one, two, three]
 
 
 def gate_kernel(x_ref, taps_ref, weight_ref, filtered_ref, sums_ref, padded_ref, held_ref, sems):
-    count, depth, width = held_ref.shape[0], held_ref.shape[1], held_ref.shape[2] // 2
+    count, depth, columns = weight_ref.shape
+    width = columns // 2
     copies = [
-        pltpu.make_async_copy(weight_ref.at[z, :, : 2 * width], held_ref.at[z], sems.at[z])
+        pltpu.make_async_copy(
+            weight_ref.at[z], held_ref.at[z * depth : (z + 1) * depth], sems.at[z]
+        )
         for z in range(count)
     ]
     for copy in copies:
         copy.start()
-    value, gate = 0.0, 0.0
-    for z, copy in enumerate(copies):
-        copy.wait()
-        x = x_ref[:, z * depth : (z + 1) * depth]
-        value += jnp.dot(x, held_ref[z, :, :width], preferred_element_type=jnp.float32)
-        gate += jnp.dot(x, held_ref[z, :, width:], preferred_element_type=jnp.float32)
+    both = 0.0
+    for half in range(2):
+        for copy in copies[half * count // 2 : (half + 1) * count // 2]:
+            copy.wait()
+        at = slice(half * D // 2, (half + 1) * D // 2)
+        both += jnp.dot(x_ref[:, at], held_ref[at], preferred_element_type=jnp.float32)
+    value, gate = both[:, :width], both[:, width:]
     gated = value * jax.nn.sigmoid(gate)
     pad = padded_ref.shape[1] - LENGTH
     sequences = padded_ref.shape[0]
@@ -116,7 +121,7 @@
 
 def gated_filter(x, taps, weights, width):
     rows = x.shape[0]
-    count, depth, _ = weights.shape
+    count, _, _ = weights.shape
     vmem = pl.BlockSpec(memory_space=pltpu.VMEM)
     return pl.pallas_call(
         gate_kernel,
@@ -128,7 +133,7 @@
         ),
         scratch_shapes=[
             pltpu.VMEM((rows // LENGTH, LENGTH + 32, width), jnp.float32),
-            pltpu.VMEM((count, depth, 2 * width), jnp.bfloat16),
+            pltpu.VMEM((D, 2 * width), jnp.bfloat16),
             pltpu.SemaphoreType.DMA((count,)),
         ],
         compiler_params=pltpu.CompilerParams(vmem_limit_bytes=52 * MIB),
@@ -139,11 +144,13 @@
     )(x, taps, weights)
 
 
-def fetched(slab_refs, held_ref, columns, sems):
+def fetched(slab_refs, held_ref, columns, at, sems):
     here, count = lax.axis_index("zl"), lax.axis_size("zl")
     copies = []
     for turn, ref in enumerate(slab_refs):
-        to = held_ref.at[lax.rem(here + turn, count)]
+        depth = ref.shape[0]
+        start = pl.multiple_of(lax.rem(here + turn, count) * depth, depth)
+        to = held_ref.at[pl.ds(start, depth), at]
         copies.append(pltpu.make_async_copy(ref.at[:, columns], to, sems.at[turn]))
         copies[turn].start()
     return copies
@@ -153,7 +160,8 @@
     *slab_refs, theirs_ref, mine_ref, held_ref, sems = refs
     core = lax.axis_index("c")
     rows, width = filtered_ref.shape
-    copies = fetched(slab_refs, held_ref, slice(0, width), sems)
+    own = slice(0, width)
+    copies = fetched(slab_refs, held_ref, own, own, sems)
     sums = sum(sums_ref[d] for d in range(sums_ref.shape[0])) / D
     mean = sums[:, :rows]
     scale = lax.rsqrt(sums[:, rows:] - mean * mean + EPS)
@@ -168,9 +176,9 @@
     for copy in copies:
         copy.wait()
     for out_ref, which in ((theirs_ref, 1 - core), (mine_ref, core)):
-        at = pl.ds(pl.multiple_of(which * width, width), width)
-        for z in range(held_ref.shape[0]):
-            out_ref[z] = times_t(activated, held_ref[z, at]).astype(out_ref.dtype)
+        for x in range(out_ref.shape[0]):
+            at = pl.ds(pl.multiple_of((2 * x + which) * width, width), width)
+            out_ref[x] = times_t(activated, held_ref[at]).astype(out_ref.dtype)
 
 
 def mixer(filtered, sums, gain, slabs):
@@ -186,7 +194,7 @@
             jax.ShapeDtypeStruct(out, jnp.bfloat16),
         ),
         scratch_shapes=[
-            pltpu.VMEM((out[0], 2 * width, width), jnp.bfloat16),
+            pltpu.VMEM((D, width), jnp.bfloat16),
             pltpu.SemaphoreType.DMA((len(slabs),)),
         ],
         compiler_params=pltpu.CompilerParams(vmem_limit_bytes=52 * MIB),
@@ -234,42 +242,52 @@
 
 
 def feed_forward_kernel(x_ref, first_ref, *refs):
-    *slab_refs, theirs_ref, mine_ref, up_ref, down_ref, late_ref, hidden_ref, sems = refs
+    *slab_refs, theirs_ref, mine_ref, up_ref, down_ref, hidden_ref, sems = refs
     core = lax.axis_index("c")
-    count, depth, columns = up_ref.shape
+    count, depth, columns = first_ref.shape
+    columns //= 2
     width = depth // 2
     steps = [slice(low, low + width) for low in range(0, columns, width)]
-    copies = [
-        pltpu.make_async_copy(first_ref.at[:, :, at], up_ref.at[:, :, at], sems.at[i])
-        for i, at in enumerate(steps)
-    ]
-    for copy in copies:
-        copy.start()
-    past = len(steps) + 1
-    late_copies = fetched(slab_refs, late_ref, slice(width, width + 2 * LATE), sems.at[past:])
-    down = pltpu.make_async_copy(first_ref.at[:, :, columns:], down_ref, sems.at[len(steps)])
-    down.start()
-
-    def hidden_of(weight_ref, at):
-        upward = 0.0
-        for z in range(count):
-            x = x_ref[:, z * depth : (z + 1) * depth]
-            upward += jnp.dot(x, weight_ref[z, :, at], preferred_element_type=jnp.float32)
-        return jnp.square(jnp.maximum(upward, 0.0)).astype(jnp.bfloat16)
-
-    for copy, at in zip(copies, steps):
-        copy.wait()
-        hidden_ref[:, at] = hidden_of(up_ref, at)
-    for copy in late_copies:
-        copy.wait()
-    hidden_ref[:, columns:] = hidden_of(late_ref, slice(0, LATE))
-    down.wait()
+    late = slice(columns, columns + LATE)
+
+    def fetch(low, ref, at, sem):
+        copies = [
+            pltpu.make_async_copy(
+                first_ref.at[z, :, low : low + at.stop - at.start],
+                ref.at[z * depth : (z + 1) * depth, at],
+                sem.at[z],
+            )
+            for z in range(count)
+        ]
+        for copy in copies:
+            copy.start()
+        return copies
+
+    def wait(copies):
+        for copy in copies:
+            copy.wait()
+
+    def hidden_of(at):
+        upward = jnp.dot(x_ref[...], up_ref[:, at], preferred_element_type=jnp.float32)
+        hidden_ref[:, at] = jnp.square(jnp.maximum(upward, 0.0)).astype(jnp.bfloat16)
+
+    early = [fetch(at.start, up_ref, at, sems.at[i]) for i, at in enumerate(steps)]
+    past = len(steps)
+    late_up = fetched(slab_refs, up_ref, slice(width, width + LATE), late, sems.at[past])
+    down = fetch(columns, down_ref, slice(0, columns), sems.at[past + 1])
+    down += fetched(
+        slab_refs, down_ref, slice(width + LATE, width + 2 * LATE), late, sems.at[past + 2]
+    )
+    for copies, at in zip(early, steps):
+        wait(copies)
+        hidden_of(at)
+    wait(late_up)
+    hidden_of(late)
+    wait(down)
     for out_ref, which in ((theirs_ref, 1 - core), (mine_ref, core)):
-        rows = pl.ds(pl.multiple_of(which * width, width), width)
-        for z in range(count):
-            part = times_t(hidden_ref[:, :columns], down_ref[z, rows])
-            part += times_t(hidden_ref[:, columns:], late_ref[z, rows, LATE:])
-            out_ref[z] = part.astype(out_ref.dtype)
+        for x in range(count):
+            rows = pl.ds(pl.multiple_of((2 * x + which) * width, width), width)
+            out_ref[x] = times_t(hidden_ref[...], down_ref[rows]).astype(out_ref.dtype)
 
 
 def feed_forward(x, first, late):
@@ -279,8 +297,8 @@
     width = depth // 2
     out = (count, rows, width)
     vmem = pl.BlockSpec(memory_space=pltpu.VMEM)
-    weights = pltpu.VMEM((count, depth, columns), jnp.bfloat16)
     hidden = columns + LATE
+    weights = pltpu.VMEM((D, hidden), jnp.bfloat16)
     return pl.pallas_call(
         feed_forward_kernel,
         in_specs=[vmem, ANY, *(ANY for _ in late)],
@@ -292,9 +310,8 @@
         scratch_shapes=[
             weights,
             weights,
-            pltpu.VMEM((count, depth, 2 * LATE), jnp.bfloat16),
             pltpu.VMEM((rows, hidden), jnp.bfloat16),
-            pltpu.SemaphoreType.DMA((columns // width + 1 + len(late),)),
+            pltpu.SemaphoreType.DMA((columns // width + 3, count)),
         ],
         compiler_params=pltpu.CompilerParams(vmem_limit_bytes=52 * MIB),
         cost_estimate=pl.CostEstimate(

time: 199 us -> 199 us (level)
  no operation moved by 1% of the time
where the time goes in v3:
time: 199 us
  blocking collectives  83.6 us (42%)
  starting transfers between devices  54.1 us (27%)
  waiting for transfers between devices  25.5 us (13%)
  Pallas kernels  19.2 us (10%)
  between operations  13.6 us (7%)
    all_to_all x2, blocking collectives, over_group(): lax.all_to_all(pair, 'x', 0, 0, tiled=True).astype(jnp.float32)  29.6 us
    all_gather x1, blocking collectives, body(): gates = lax.all_gather(gates, 'zl', axis=0)  17.4 us
    ppermute x2, starting transfers between devices, normed_channels(): other = lax.ppermute(own, 'c', SWAP)  17.2 us
    all_gather x1, blocking collectives, body(): first = lax.all_gather(first, 'zl', axis=0)  13.4 us
    ppermute x3, starting transfers between devices, from_z(): return lax.ppermute(slab, ('rep', 'zl'), pairs)  12.9 us
    ppermute x3, waiting for transfers between devices, from_z(): return lax.ppermute(slab, ('rep', 'zl'), pairs)  12.7 us
    all_gather x1, blocking collectives, body(): own = lax.all_gather(states, 'x', axis=0)  11.6 us
    all_gather x1, blocking collectives, body(): normed_mid = normed_channels(lax.all_gather(middle, 'x', axis=0), mlp_gain)  11.6 us
  transfers between devices with their start and end apart: 11, of which 5 were waited for; matrix products, arithmetic and copies ran while one was open for 0% of the time, Pallas kernels for 5%

profile of v3, /device:TPU:1, one launch (start us, length us, event | category | flops | bytes accessed | tf_op | source)
XLA Modules:
  0.0 198.5 jit_solution(5173681917683512966)
XLA Ops:
  6.5 2.0 %pack.1 = (bf16[64,512]{1,0:T(8,128)(2,1)}, bf16[64,1024]{1,0:T(8,128)(2,1)}, bf16[8,64,768]{2,1,0:T(8,128)(2,1)}) custom-call(bf16[64,256]{1,0:T(8,128)(2,1)} %value_ref.1, bf16[64,256]{1,0:T(8,128)(2,1)} %gate_ref.1, bf16[64,256]{1,0:T(8,128)(2,1)} %out_ref.1, bf16[64,768]{1,0:T(8,128)(2,1)} %up_ref.1, bf16[64,768]{1,0:T(8,128)(2,1)} %down_ref.1), custom_call_target="tpu_custom_call" | custom-call | bytes 1048576 | tf_op jit(solution)/shard_map/pack/pallas_call | solution.py:44
  8.5 17.4 %all-gather.1 = bf16[256,512]{1,0:T(8,128)(2,1)} all-gather(bf16[64,512]{1,0:T(8,128)(2,1)} %get-tuple-element.18), channel_id=3, replica_groups=mesh['rep'=2,'zl'=4,'y'=8,'x'=4,'c'=2] {'zl'}, dimensions={0}, use_global_device_ids=true | all-gather | bytes 327680 | tf_op jit(solution)/shard_map/all_gather | solution.py:330
  26.0 13.4 %all-gather.3 = bf16[256,1024]{1,0:T(8,128)(2,1)} all-gather(bf16[64,1024]{1,0:T(8,128)(2,1)} %get-tuple-element.24), channel_id=5, replica_groups=mesh['rep'=2,'zl'=4,'y'=8,'x'=4,'c'=2] {'zl'}, dimensions={0}, use_global_device_ids=true | all-gather | bytes 655360 | tf_op jit(solution)/shard_map/all_gather | solution.py:331
  39.4 6.2 %all-to-all-start.1 = ((bf16[8,64,768]{2,1,0:T(8,128)(2,1)}), bf16[8,64,768]{2,1,0:T(8,128)(2,1)}, u32[]{:S(2)}, u32[]{:S(2)}) async-start(bf16[8,64,768]{2,1,0:T(8,128)(2,1)} %get-tuple-element.21), calls=%async_computation.1 | async-start | bytes 1572864 | tf_op jit(solution)/shard_map/all_to_all | solution.py:329
  45.7 11.6 %all-gather = bf16[1536,256]{1,0:T(8,128)(2,1)S(1)} all-gather(bf16[384,256]{1,0:T(8,128)(2,1)S(1)} %copy-done.5), channel_id=2, replica_groups=mesh['rep'=2,'zl'=4,'y'=8,'x'=4,'c'=2] {'x'}, dimensions={0}, use_global_device_ids=true | all-gather | bytes 983040 | tf_op jit(solution)/shard_map/all_gather | solution.py:333
  57.3 10.8 %collective-permute-start = (bf16[4,384,256]{2,1,0:T(8,128)(2,1)S(1)}, bf16[4,384,256]{2,1,0:T(8,128)(2,1)S(1)}, u32[]{:S(2)}, u32[]{:S(2)}) collective-permute-start(bf16[4,384,256]{2,1,0:T(8,128)(2,1)S(1)} %bitcast.8), channel_id=1, source_target_pairs={{0,1},{1,0},{2,3},{3,2},{4,5},{5,4},{6,7},{7,6},{8,9},{9,8},{10,11... | collective-permute-start | bytes 2359304 | tf_op jit(solution)/shard_map/ppermute | solution.py:221
  68.1 7.1 %all-to-all-done.1 = bf16[8,64,768]{2,1,0:T(8,128)(2,1)} async-done(((bf16[8,64,768]{2,1,0:T(8,128)(2,1)}), bf16[8,64,768]{2,1,0:T(8,128)(2,1)}, u32[]{:S(2)}, u32[]{:S(2)}) %all-to-all-start.1) | async-done | bytes 786464 | tf_op jit(solution)/shard_map/all_to_all | solution.py:329
  75.2 3.0 %collective-permute-start.3 = (bf16[512,768]{1,0:T(8,128)(2,1)}, bf16[512,768]{1,0:T(8,128)(2,1)}, u32[]{:S(2)}, u32[]{:S(2)}) collective-permute-start(bf16[512,768]{1,0:T(8,128)(2,1)} %bitcast.4.refs_0_), channel_id=1, source_target_pairs={{448,0},{0,64},{64,128},{128,192},{192,256},{256,320},{320,384},{3... | collective-permute-start | bytes 2359304 | tf_op jit(solution)/shard_map/ppermute | solution.py:64
  78.2 7.9 %collective-permute-start.2 = (bf16[512,768]{1,0:T(8,128)(2,1)}, bf16[512,768]{1,0:T(8,128)(2,1)}, u32[]{:S(2)}, u32[]{:S(2)}) collective-permute-start(bf16[512,768]{1,0:T(8,128)(2,1)} %bitcast.4.refs_0_), channel_id=1, source_target_pairs={{128,0},{448,64},{256,128},{64,192},{384,256},{192,320},{0,384},{3... | collective-permute-start | bytes 2359304 | tf_op jit(solution)/shard_map/ppermute | solution.py:64
  86.2 1.9 collective-permute-start.1
  89.4 5.5 %gated_filter.1 = (f32[384,256]{1,0:T(8,128)S(1)}, f32[8,1,768]{2,1,0:T(1,128)}) custom-call(bf16[384,2048]{1,0:T(8,128)(2,1)S(1)} %norm.2.x_ref, f32[31,256]{1,0:T(8,128)S(1)} %constant_dynamic-slice_fusion.taps_ref, bf16[4,512,512]{2,1,0:T(8,128)(2,1)} %all-gather.7.cloned.1.call-done.weight_ref), custom_call_target="tpu_custom_call" | custom-call | flops 805306368 | bytes 2097152 | tf_op jit(solution)/shard_map/gated_filter/pallas_call | solution.py:126
  94.8 9.5 %all-to-all-start = ((f32[8,1,768]{2,1,0:T(1,128)}), f32[8,1,768]{2,1,0:T(1,128)S(1)}, u32[]{:S(2)}, u32[]{:S(2)}) async-start(f32[8,1,768]{2,1,0:T(1,128)} %get-tuple-element.20), calls=%async_computation | async-start | bytes 49152 | tf_op jit(solution)/shard_map/all_to_all | solution.py:339
  104.3 12.7 %collective-permute-done.1.refs_1_ = bf16[512,768]{1,0:T(8,128)(2,1)} collective-permute-done((bf16[512,768]{1,0:T(8,128)(2,1)}, bf16[512,768]{1,0:T(8,128)(2,1)}, u32[]{:S(2)}, u32[]{:S(2)}) %collective-permute-start.1) | collective-permute-done | bytes 786464 | tf_op jit(solution)/shard_map/ppermute | solution.py:64
  117.0 2.0 %mixer.1 = (bf16[4,384,256]{2,1,0:T(8,128)(2,1)S(1)}, bf16[4,384,256]{2,1,0:T(8,128)(2,1)S(1)}) custom-call(f32[384,256]{1,0:T(8,128)S(1)} %get-tuple-element.19.filtered_ref, f32[8,1,768]{2,1,0:T(1,128)S(1)} %all-to-all-done.sums_ref, f32[1,2048]{1,0:T(1,128)S(1)} %bitcast.13, bf16[512,768]{1,0:T(8,128)(2,1)} %bitcast.4.refs_0_, ...), custom_call_target="tpu_custom_call" | custom-call | flops 402653184 | bytes 1048576 | tf_op jit(solution)/shard_map/mixer/pallas_call | solution.py:188
  119.0 6.0 %collective-permute-start.4 = (bf16[4,384,256]{2,1,0:T(8,128)(2,1)S(1)}, bf16[4,384,256]{2,1,0:T(8,128)(2,1)S(1)}, u32[]{:S(2)}, u32[]{:S(2)}) collective-permute-start(bf16[4,384,256]{2,1,0:T(8,128)(2,1)S(1)} %get-tuple-element.23), channel_id=1, source_target_pairs={{0,1},{1,0},{2,3},{3,2},{4,5},{5,4},{6,7},{7,6},{8,9},{9,8},{10,11... | collective-permute-start | bytes 2359304 | tf_op jit(solution)/shard_map/ppermute | solution.py:239
  125.0 1.9 collective-permute-done.4
  127.1 15.3 %all_to_all.20 = bf16[4,384,256]{2,1,0:T(8,128)(2,1)S(1)} all-to-all(bf16[4,384,256]{2,1,0:T(8,128)(2,1)S(1)} %add_convert_fusion.1), channel_id=1, replica_groups=mesh['rep'=2,'zl'=4,'y'=8,'x'=4,'c'=2] {'x'}, dimensions={0} | all-to-all | bytes 1572864 | tf_op jit(solution)/shard_map/all_to_all | solution.py:241
  142.6 11.6 %all-gather.2 = bf16[1536,256]{1,0:T(8,128)(2,1)S(1)} all-gather(bf16[384,256]{1,0:T(8,128)(2,1)S(1)} %add_convert_fusion.3), channel_id=4, replica_groups=mesh['rep'=2,'zl'=4,'y'=8,'x'=4,'c'=2] {'x'}, dimensions={0}, use_global_device_ids=true | all-gather | bytes 983040 | tf_op jit(solution)/shard_map/all_gather | solution.py:343
  154.2 6.3 %collective-permute-start.5 = (bf16[4,384,256]{2,1,0:T(8,128)(2,1)S(1)}, bf16[4,384,256]{2,1,0:T(8,128)(2,1)S(1)}, u32[]{:S(2)}, u32[]{:S(2)}) collective-permute-start(bf16[4,384,256]{2,1,0:T(8,128)(2,1)S(1)} %bitcast.10), channel_id=1, source_target_pairs={{0,1},{1,0},{2,3},{3,2},{4,5},{5,4},{6,7},{7,6},{8,9},{9,8},{10,11... | collective-permute-start | bytes 2359304 | tf_op jit(solution)/shard_map/ppermute | solution.py:221
  160.6 1.9 collective-permute-done.5.other_ref
  164.9 7.3 %feed_forward.1 = (bf16[4,384,256]{2,1,0:T(8,128)(2,1)S(1)}, bf16[4,384,256]{2,1,0:T(8,128)(2,1)S(1)}) custom-call(bf16[384,2048]{1,0:T(8,128)(2,1)} %copy-done.1, bf16[4,512,1024]{2,1,0:T(8,128)(2,1)} %all-gather.9.cloned.1.call-done.first_ref, bf16[512,768]{1,0:T(8,128)(2,1)} %bitcast.4.refs_0_, bf16[512,768]{1,0:T(8,128)(2,1)} %collective-permute-done.1.refs_1_, ...), custom_call_target="tpu_custom_call" | custom-call | flops 2415919104 | bytes 6291456 | tf_op jit(solution)/shard_map/feed_forward/pallas_call | solution.py:302
  172.2 2.3 %collective-permute-start.6 = (bf16[4,384,256]{2,1,0:T(8,128)(2,1)S(1)}, bf16[4,384,256]{2,1,0:T(8,128)(2,1)S(1)}, u32[]{:S(2)}, u32[]{:S(2)}) collective-permute-start(bf16[4,384,256]{2,1,0:T(8,128)(2,1)S(1)} %get-tuple-element.26), channel_id=1, source_target_pairs={{0,1},{1,0},{2,3},{3,2},{4,5},{5,4},{6,7},{7,6},{8,9},{9,8},{10,11... | collective-permute-start | bytes 2359304 | tf_op jit(solution)/shard_map/ppermute | solution.py:239
  174.5 1.9 collective-permute-done.6
  176.5 14.3 %all_to_all.21 = bf16[4,384,256]{2,1,0:T(8,128)(2,1)S(1)} all-to-all(bf16[4,384,256]{2,1,0:T(8,128)(2,1)S(1)} %add_convert_fusion), channel_id=1, replica_groups=mesh['rep'=2,'zl'=4,'y'=8,'x'=4,'c'=2] {'x'}, dimensions={0} | all-to-all | bytes 1572864 | tf_op jit(solution)/shard_map/all_to_all | solution.py:241
  (33 shorter events, 5.1 us)
Async XLA Ops:
  6.5 39.2 %copy-start = (f32[31,2048]{1,0:T(8,128)S(1)}, f32[31,2048]{1,0:T(8,128)}, u32[]{:S(2)}) copy-start(f32[31,2048]{1,0:T(8,128)} %param.14) | copy-start | bytes 761860
  6.5 82.8 %all-gather.7.cloned.1.call-start = ((), (), s32[]{:S(2)}) async-start(), calls=%async_computation.4 | async-start | bytes 2359296 | tf_op jit(solution)/shard_map/all_gather | solution.py:58
  25.9 19.8 %copy-start.5 = (bf16[384,256]{1,0:T(8,128)(2,1)S(1)}, bf16[384,256]{1,0:T(8,128)(2,1)}, u32[]{:S(2)}) copy-start(bf16[384,256]{1,0:T(8,128)(2,1)} %param.10) | copy-start | bytes 589828
  25.9 138.9 %all-gather.9.cloned.1.call-start = ((), (), s32[]{:S(2)}) async-start(), calls=%async_computation.5 | async-start | bytes 4718592 | tf_op jit(solution)/shard_map/all_gather | solution.py:58
  39.4 48.7 %copy-start.2 = (f32[2048]{0:T(1024)S(1)}, f32[2048]{0:T(1024)}, u32[]{:S(2)}) copy-start(f32[2048]{0:T(1024)} %param.11) | copy-start | bytes 24580
  39.4 35.8 %all-to-all-start.1 = ((bf16[8,64,768]{2,1,0:T(8,128)(2,1)}), bf16[8,64,768]{2,1,0:T(8,128)(2,1)}, u32[]{:S(2)}, u32[]{:S(2)}) async-start(bf16[8,64,768]{2,1,0:T(8,128)(2,1)} %get-tuple-element.21), calls=%async_computation.1 | async-start | bytes 1572864 | tf_op jit(solution)/shard_map/all_to_all | solution.py:329
  57.3 30.8 %collective-permute-start = (bf16[4,384,256]{2,1,0:T(8,128)(2,1)S(1)}, bf16[4,384,256]{2,1,0:T(8,128)(2,1)S(1)}, u32[]{:S(2)}, u32[]{:S(2)}) collective-permute-start(bf16[4,384,256]{2,1,0:T(8,128)(2,1)S(1)} %bitcast.8), channel_id=1, source_target_pairs={{0,1},{1,0},{2,3},{3,2},{4,5},{5,4},{6,7},{7,6},{8,9},{9,8},{10,11... | collective-permute-start | bytes 2359304 | tf_op jit(solution)/shard_map/ppermute | solution.py:221
  75.2 29.1 %collective-permute-start.3 = (bf16[512,768]{1,0:T(8,128)(2,1)}, bf16[512,768]{1,0:T(8,128)(2,1)}, u32[]{:S(2)}, u32[]{:S(2)}) collective-permute-start(bf16[512,768]{1,0:T(8,128)(2,1)} %bitcast.4.refs_0_), channel_id=1, source_target_pairs={{448,0},{0,64},{64,128},{128,192},{192,256},{256,320},{320,384},{3... | collective-permute-start | bytes 2359304 | tf_op jit(solution)/shard_map/ppermute | solution.py:64
  78.2 26.1 %collective-permute-start.2 = (bf16[512,768]{1,0:T(8,128)(2,1)}, bf16[512,768]{1,0:T(8,128)(2,1)}, u32[]{:S(2)}, u32[]{:S(2)}) collective-permute-start(bf16[512,768]{1,0:T(8,128)(2,1)} %bitcast.4.refs_0_), channel_id=1, source_target_pairs={{128,0},{448,64},{256,128},{64,192},{384,256},{192,320},{0,384},{3... | collective-permute-start | bytes 2359304 | tf_op jit(solution)/shard_map/ppermute | solution.py:64
  86.2 30.8 %collective-permute-start.1 = (bf16[512,768]{1,0:T(8,128)(2,1)}, bf16[512,768]{1,0:T(8,128)(2,1)}, u32[]{:S(2)}, u32[]{:S(2)}) collective-permute-start(bf16[512,768]{1,0:T(8,128)(2,1)} %bitcast.4.refs_0_), channel_id=1, source_target_pairs={{64,0},{128,64},{192,128},{256,192},{320,256},{384,320},{448,384},... | collective-permute-start | bytes 2359304 | tf_op jit(solution)/shard_map/ppermute | solution.py:64
  89.3 27.7 %copy-start.3 = (f32[2048]{0:T(1024)S(1)}, f32[2048]{0:T(1024)}, u32[]{:S(2)}) copy-start(f32[2048]{0:T(1024)} %param.15) | copy-start | bytes 24580
  94.8 22.1 %all-to-all-start = ((f32[8,1,768]{2,1,0:T(1,128)}), f32[8,1,768]{2,1,0:T(1,128)S(1)}, u32[]{:S(2)}, u32[]{:S(2)}) async-start(f32[8,1,768]{2,1,0:T(1,128)} %get-tuple-element.20), calls=%async_computation | async-start | bytes 49152 | tf_op jit(solution)/shard_map/all_to_all | solution.py:339
  119.0 7.9 %collective-permute-start.4 = (bf16[4,384,256]{2,1,0:T(8,128)(2,1)S(1)}, bf16[4,384,256]{2,1,0:T(8,128)(2,1)S(1)}, u32[]{:S(2)}, u32[]{:S(2)}) collective-permute-start(bf16[4,384,256]{2,1,0:T(8,128)(2,1)S(1)} %get-tuple-element.23), channel_id=1, source_target_pairs={{0,1},{1,0},{2,3},{3,2},{4,5},{5,4},{6,7},{7,6},{8,9},{9,8},{10,11... | collective-permute-start | bytes 2359304 | tf_op jit(solution)/shard_map/ppermute | solution.py:239
  127.1 15.5 %copy-start.6 = (bf16[384,256]{1,0:T(8,128)(2,1)S(1)}, bf16[384,256]{1,0:T(8,128)(2,1)}, u32[]{:S(2)}) copy-start(bf16[384,256]{1,0:T(8,128)(2,1)} %param.10) | copy-start | bytes 589828
  142.5 20.0 %copy-start.4 = (f32[2048]{0:T(1024)S(1)}, f32[2048]{0:T(1024)}, u32[]{:S(2)}) copy-start(f32[2048]{0:T(1024)} %param.17) | copy-start | bytes 24580
  154.2 8.2 %collective-permute-start.5 = (bf16[4,384,256]{2,1,0:T(8,128)(2,1)S(1)}, bf16[4,384,256]{2,1,0:T(8,128)(2,1)S(1)}, u32[]{:S(2)}, u32[]{:S(2)}) collective-permute-start(bf16[4,384,256]{2,1,0:T(8,128)(2,1)S(1)} %bitcast.10), channel_id=1, source_target_pairs={{0,1},{1,0},{2,3},{3,2},{4,5},{5,4},{6,7},{7,6},{8,9},{9,8},{10,11... | collective-permute-start | bytes 2359304 | tf_op jit(solution)/shard_map/ppermute | solution.py:221
  163.7 1.2 copy-start.1
  172.2 4.2 %collective-permute-start.6 = (bf16[4,384,256]{2,1,0:T(8,128)(2,1)S(1)}, bf16[4,384,256]{2,1,0:T(8,128)(2,1)S(1)}, u32[]{:S(2)}, u32[]{:S(2)}) collective-permute-start(bf16[4,384,256]{2,1,0:T(8,128)(2,1)S(1)} %get-tuple-element.26), channel_id=1, source_target_pairs={{0,1},{1,0},{2,3},{3,2},{4,5},{5,4},{6,7},{7,6},{8,9},{9,8},{10,11... | collective-permute-start | bytes 2359304 | tf_op jit(solution)/shard_map/ppermute | solution.py:239
Sparse Core Ops, SparseCore 0:
  26.1 58.3 all-gather.6
  86.6 57.6 all-gather.8

commit v4 on v2

--- a/solution.py
+++ b/solution.py
@@ -233,8 +233,8 @@
     return jnp.sum(lax.all_to_all(pair, "x", 0, 0, tiled=True).astype(jnp.float32), axis=0)
 
 
-def feed_forward_kernel(x_ref, first_ref, *refs):
-    *slab_refs, theirs_ref, mine_ref, up_ref, down_ref, late_ref, hidden_ref, sems = refs
+def feed_forward_kernel(rows_ref, first_ref, *refs):
+    *slab_refs, theirs_ref, mine_ref, x_ref, up_ref, down_ref, late_ref, hidden_ref, sems = refs
     core = lax.axis_index("c")
     count, depth, columns = up_ref.shape
     width = depth // 2
@@ -243,12 +243,12 @@
         pltpu.make_async_copy(first_ref.at[:, :, at], up_ref.at[:, :, at], sems.at[i])
         for i, at in enumerate(steps)
     ]
+    past = len(steps) + 2
+    whole_x = pltpu.make_async_copy(rows_ref, x_ref, sems.at[past - 1])
+    down = pltpu.make_async_copy(first_ref.at[:, :, columns:], down_ref, sems.at[len(steps)])
+    whole_x.start()
     for copy in copies:
         copy.start()
-    past = len(steps) + 1
-    late_copies = fetched(slab_refs, late_ref, slice(width, width + 2 * LATE), sems.at[past:])
-    down = pltpu.make_async_copy(first_ref.at[:, :, columns:], down_ref, sems.at[len(steps)])
-    down.start()
 
     def hidden_of(weight_ref, at):
         upward = 0.0
@@ -257,7 +257,12 @@
             upward += jnp.dot(x, weight_ref[z, :, at], preferred_element_type=jnp.float32)
         return jnp.square(jnp.maximum(upward, 0.0)).astype(jnp.bfloat16)
 
-    for copy, at in zip(copies, steps):
+    whole_x.wait()
+    copies[0].wait()
+    late_copies = fetched(slab_refs, late_ref, slice(width, width + 2 * LATE), sems.at[past:])
+    down.start()
+    hidden_ref[:, steps[0]] = hidden_of(up_ref, steps[0])
+    for copy, at in zip(copies[1:], steps[1:]):
         copy.wait()
         hidden_ref[:, at] = hidden_of(up_ref, at)
     for copy in late_copies:
@@ -283,18 +288,19 @@
     hidden = columns + LATE
     return pl.pallas_call(
         feed_forward_kernel,
-        in_specs=[vmem, ANY, *(ANY for _ in late)],
+        in_specs=[ANY, ANY, *(ANY for _ in late)],
         out_specs=(vmem, vmem),
         out_shape=(
             jax.ShapeDtypeStruct(out, jnp.bfloat16),
             jax.ShapeDtypeStruct(out, jnp.bfloat16),
         ),
         scratch_shapes=[
+            pltpu.VMEM(x.shape, jnp.bfloat16),
             weights,
             weights,
             pltpu.VMEM((count, depth, 2 * LATE), jnp.bfloat16),
             pltpu.VMEM((rows, hidden), jnp.bfloat16),
-            pltpu.SemaphoreType.DMA((columns // width + 1 + len(late),)),
+            pltpu.SemaphoreType.DMA((columns // width + 2 + len(late),)),
         ],
         compiler_params=pltpu.CompilerParams(vmem_limit_bytes=52 * MIB),
         cost_estimate=pl.CostEstimate(

time: 199 us -> 198 us (level)
  no operation moved by 1% of the time
where the time goes in v4:
time: 198 us; the launch traced here: 197 us
  blocking collectives  83.6 us (42%)
  starting transfers between devices  54.1 us (27%)
  waiting for transfers between devices  25.7 us (13%)
  Pallas kernels  18 us (9%)
  between operations  13.6 us (7%)
    all_to_all x2, blocking collectives, over_group(): lax.all_to_all(pair, 'x', 0, 0, tiled=True).astype(jnp.float32)  29.6 us
    all_gather x1, blocking collectives, body(): gates = lax.all_gather(gates, 'zl', axis=0)  17.4 us
    ppermute x2, starting transfers between devices, normed_channels(): other = lax.ppermute(own, 'c', SWAP)  17.2 us
    all_gather x1, blocking collectives, body(): first = lax.all_gather(first, 'zl', axis=0)  13.4 us
    ppermute x3, waiting for transfers between devices, from_z(): return lax.ppermute(slab, ('rep', 'zl'), pairs)  12.9 us
    ppermute x3, starting transfers between devices, from_z(): return lax.ppermute(slab, ('rep', 'zl'), pairs)  12.9 us
    all_gather x1, blocking collectives, body(): own = lax.all_gather(states, 'x', axis=0)  11.6 us
    all_gather x1, blocking collectives, body(): normed_mid = normed_channels(lax.all_gather(middle, 'x', axis=0), mlp_gain)  11.6 us
  transfers between devices with their start and end apart: 11, of which 5 were waited for; matrix products, arithmetic and copies ran while one was open for 0% of the time, Pallas kernels for 5%

profile of v4, /device:TPU:1, one launch (start us, length us, event | category | flops | bytes accessed | tf_op | source)
XLA Modules:
  0.0 197.5 jit_solution(2430296149882964284)
XLA Ops:
  6.5 2.0 %pack.1 = (bf16[64,512]{1,0:T(8,128)(2,1)}, bf16[64,1024]{1,0:T(8,128)(2,1)}, bf16[8,64,768]{2,1,0:T(8,128)(2,1)}) custom-call(bf16[64,256]{1,0:T(8,128)(2,1)} %value_ref.1, bf16[64,256]{1,0:T(8,128)(2,1)} %gate_ref.1, bf16[64,256]{1,0:T(8,128)(2,1)} %out_ref.1, bf16[64,768]{1,0:T(8,128)(2,1)} %up_ref.1, bf16[64,768]{1,0:T(8,128)(2,1)} %down_ref.1), custom_call_target="tpu_custom_call" | custom-call | bytes 1048576 | tf_op jit(solution)/shard_map/pack/pallas_call | solution.py:44
  8.5 17.4 %all-gather.1 = bf16[256,512]{1,0:T(8,128)(2,1)} all-gather(bf16[64,512]{1,0:T(8,128)(2,1)} %get-tuple-element.18), channel_id=3, replica_groups=mesh['rep'=2,'zl'=4,'y'=8,'x'=4,'c'=2] {'zl'}, dimensions={0}, use_global_device_ids=true | all-gather | bytes 327680 | tf_op jit(solution)/shard_map/all_gather | solution.py:319
  26.0 13.4 %all-gather.3 = bf16[256,1024]{1,0:T(8,128)(2,1)} all-gather(bf16[64,1024]{1,0:T(8,128)(2,1)} %get-tuple-element.24), channel_id=5, replica_groups=mesh['rep'=2,'zl'=4,'y'=8,'x'=4,'c'=2] {'zl'}, dimensions={0}, use_global_device_ids=true | all-gather | bytes 655360 | tf_op jit(solution)/shard_map/all_gather | solution.py:320
  39.4 6.2 %all-to-all-start.1 = ((bf16[8,64,768]{2,1,0:T(8,128)(2,1)}), bf16[8,64,768]{2,1,0:T(8,128)(2,1)}, u32[]{:S(2)}, u32[]{:S(2)}) async-start(bf16[8,64,768]{2,1,0:T(8,128)(2,1)} %get-tuple-element.21), calls=%async_computation.1 | async-start | bytes 1572864 | tf_op jit(solution)/shard_map/all_to_all | solution.py:318
  45.7 11.6 %all-gather = bf16[1536,256]{1,0:T(8,128)(2,1)S(1)} all-gather(bf16[384,256]{1,0:T(8,128)(2,1)S(1)} %copy-done.5), channel_id=2, replica_groups=mesh['rep'=2,'zl'=4,'y'=8,'x'=4,'c'=2] {'x'}, dimensions={0}, use_global_device_ids=true | all-gather | bytes 983040 | tf_op jit(solution)/shard_map/all_gather | solution.py:322
  57.3 10.8 %collective-permute-start = (bf16[4,384,256]{2,1,0:T(8,128)(2,1)S(1)}, bf16[4,384,256]{2,1,0:T(8,128)(2,1)S(1)}, u32[]{:S(2)}, u32[]{:S(2)}) collective-permute-start(bf16[4,384,256]{2,1,0:T(8,128)(2,1)S(1)} %bitcast.8), channel_id=1, source_target_pairs={{0,1},{1,0},{2,3},{3,2},{4,5},{5,4},{6,7},{7,6},{8,9},{9,8},{10,11... | collective-permute-start | bytes 2359304 | tf_op jit(solution)/shard_map/ppermute | solution.py:213
  68.1 7.1 %all-to-all-done.1 = bf16[8,64,768]{2,1,0:T(8,128)(2,1)} async-done(((bf16[8,64,768]{2,1,0:T(8,128)(2,1)}), bf16[8,64,768]{2,1,0:T(8,128)(2,1)}, u32[]{:S(2)}, u32[]{:S(2)}) %all-to-all-start.1) | async-done | bytes 786464 | tf_op jit(solution)/shard_map/all_to_all | solution.py:318
  75.2 3.0 %collective-permute-start.3 = (bf16[512,768]{1,0:T(8,128)(2,1)}, bf16[512,768]{1,0:T(8,128)(2,1)}, u32[]{:S(2)}, u32[]{:S(2)}) collective-permute-start(bf16[512,768]{1,0:T(8,128)(2,1)} %bitcast.4.refs_0_), channel_id=1, source_target_pairs={{448,0},{0,64},{64,128},{128,192},{192,256},{256,320},{320,384},{3... | collective-permute-start | bytes 2359304 | tf_op jit(solution)/shard_map/ppermute | solution.py:64
  78.2 7.9 %collective-permute-start.2 = (bf16[512,768]{1,0:T(8,128)(2,1)}, bf16[512,768]{1,0:T(8,128)(2,1)}, u32[]{:S(2)}, u32[]{:S(2)}) collective-permute-start(bf16[512,768]{1,0:T(8,128)(2,1)} %bitcast.4.refs_0_), channel_id=1, source_target_pairs={{128,0},{448,64},{256,128},{64,192},{384,256},{192,320},{0,384},{3... | collective-permute-start | bytes 2359304 | tf_op jit(solution)/shard_map/ppermute | solution.py:64
  86.2 1.9 collective-permute-start.1
  89.4 5.2 %gated_filter.1 = (f32[384,256]{1,0:T(8,128)S(1)}, f32[8,1,768]{2,1,0:T(1,128)}) custom-call(bf16[384,2048]{1,0:T(8,128)(2,1)S(1)} %norm.2.x_ref, f32[31,256]{1,0:T(8,128)S(1)} %constant_dynamic-slice_fusion.taps_ref, bf16[4,512,512]{2,1,0:T(8,128)(2,1)} %all-gather.7.cloned.1.call-done.weight_ref), custom_call_target="tpu_custom_call" | custom-call | flops 805306368 | bytes 2097152 | tf_op jit(solution)/shard_map/gated_filter/pallas_call | solution.py:121
  94.6 9.5 %all-to-all-start = ((f32[8,1,768]{2,1,0:T(1,128)}), f32[8,1,768]{2,1,0:T(1,128)S(1)}, u32[]{:S(2)}, u32[]{:S(2)}) async-start(f32[8,1,768]{2,1,0:T(1,128)} %get-tuple-element.20), calls=%async_computation | async-start | bytes 49152 | tf_op jit(solution)/shard_map/all_to_all | solution.py:328
  104.1 12.9 %collective-permute-done.1.refs_1_ = bf16[512,768]{1,0:T(8,128)(2,1)} collective-permute-done((bf16[512,768]{1,0:T(8,128)(2,1)}, bf16[512,768]{1,0:T(8,128)(2,1)}, u32[]{:S(2)}, u32[]{:S(2)}) %collective-permute-start.1) | collective-permute-done | bytes 786464 | tf_op jit(solution)/shard_map/ppermute | solution.py:64
  117.0 2.0 %mixer.1 = (bf16[4,384,256]{2,1,0:T(8,128)(2,1)S(1)}, bf16[4,384,256]{2,1,0:T(8,128)(2,1)S(1)}) custom-call(f32[384,256]{1,0:T(8,128)S(1)} %get-tuple-element.19.filtered_ref, f32[8,1,768]{2,1,0:T(1,128)S(1)} %all-to-all-done.sums_ref, f32[1,2048]{1,0:T(1,128)S(1)} %bitcast.13, bf16[512,768]{1,0:T(8,128)(2,1)} %bitcast.4.refs_0_, ...), custom_call_target="tpu_custom_call" | custom-call | flops 402653184 | bytes 1048576 | tf_op jit(solution)/shard_map/mixer/pallas_call | solution.py:180
  119.0 6.0 %collective-permute-start.4 = (bf16[4,384,256]{2,1,0:T(8,128)(2,1)S(1)}, bf16[4,384,256]{2,1,0:T(8,128)(2,1)S(1)}, u32[]{:S(2)}, u32[]{:S(2)}) collective-permute-start(bf16[4,384,256]{2,1,0:T(8,128)(2,1)S(1)} %get-tuple-element.23), channel_id=1, source_target_pairs={{0,1},{1,0},{2,3},{3,2},{4,5},{5,4},{6,7},{7,6},{8,9},{9,8},{10,11... | collective-permute-start | bytes 2359304 | tf_op jit(solution)/shard_map/ppermute | solution.py:231
  125.0 1.9 collective-permute-done.4
  127.1 15.3 %all_to_all.20 = bf16[4,384,256]{2,1,0:T(8,128)(2,1)S(1)} all-to-all(bf16[4,384,256]{2,1,0:T(8,128)(2,1)S(1)} %add_convert_fusion.1), channel_id=1, replica_groups=mesh['rep'=2,'zl'=4,'y'=8,'x'=4,'c'=2] {'x'}, dimensions={0} | all-to-all | bytes 1572864 | tf_op jit(solution)/shard_map/all_to_all | solution.py:233
  142.6 11.6 %all-gather.2 = bf16[1536,256]{1,0:T(8,128)(2,1)S(1)} all-gather(bf16[384,256]{1,0:T(8,128)(2,1)S(1)} %add_convert_fusion.3), channel_id=4, replica_groups=mesh['rep'=2,'zl'=4,'y'=8,'x'=4,'c'=2] {'x'}, dimensions={0}, use_global_device_ids=true | all-gather | bytes 983040 | tf_op jit(solution)/shard_map/all_gather | solution.py:332
  154.2 6.3 %collective-permute-start.5 = (bf16[4,384,256]{2,1,0:T(8,128)(2,1)S(1)}, bf16[4,384,256]{2,1,0:T(8,128)(2,1)S(1)}, u32[]{:S(2)}, u32[]{:S(2)}) collective-permute-start(bf16[4,384,256]{2,1,0:T(8,128)(2,1)S(1)} %bitcast.10), channel_id=1, source_target_pairs={{0,1},{1,0},{2,3},{3,2},{4,5},{5,4},{6,7},{7,6},{8,9},{9,8},{10,11... | collective-permute-start | bytes 2359304 | tf_op jit(solution)/shard_map/ppermute | solution.py:213
  160.6 1.9 collective-permute-done.5.other_ref
  164.9 6.3 %feed_forward.1 = (bf16[4,384,256]{2,1,0:T(8,128)(2,1)S(1)}, bf16[4,384,256]{2,1,0:T(8,128)(2,1)S(1)}) custom-call(bf16[384,2048]{1,0:T(8,128)(2,1)} %copy-done.1, bf16[4,512,1024]{2,1,0:T(8,128)(2,1)} %all-gather.9.cloned.1.call-done.first_ref, bf16[512,768]{1,0:T(8,128)(2,1)} %bitcast.4.refs_0_, bf16[512,768]{1,0:T(8,128)(2,1)} %collective-permute-done.1.refs_1_, ...), custom_call_target="tpu_custom_call" | custom-call | flops 2415919104 | bytes 6291456 | tf_op jit(solution)/shard_map/feed_forward/pallas_call | solution.py:289
  171.1 2.3 %collective-permute-start.6 = (bf16[4,384,256]{2,1,0:T(8,128)(2,1)S(1)}, bf16[4,384,256]{2,1,0:T(8,128)(2,1)S(1)}, u32[]{:S(2)}, u32[]{:S(2)}) collective-permute-start(bf16[4,384,256]{2,1,0:T(8,128)(2,1)S(1)} %get-tuple-element.26), channel_id=1, source_target_pairs={{0,1},{1,0},{2,3},{3,2},{4,5},{5,4},{6,7},{7,6},{8,9},{9,8},{10,11... | collective-permute-start | bytes 2359304 | tf_op jit(solution)/shard_map/ppermute | solution.py:231
  173.4 1.9 collective-permute-done.6
  175.5 14.3 %all_to_all.21 = bf16[4,384,256]{2,1,0:T(8,128)(2,1)S(1)} all-to-all(bf16[4,384,256]{2,1,0:T(8,128)(2,1)S(1)} %add_convert_fusion), channel_id=1, replica_groups=mesh['rep'=2,'zl'=4,'y'=8,'x'=4,'c'=2] {'x'}, dimensions={0} | all-to-all | bytes 1572864 | tf_op jit(solution)/shard_map/all_to_all | solution.py:233
  (33 shorter events, 5.1 us)
Async XLA Ops:
  6.5 39.2 %copy-start = (f32[31,2048]{1,0:T(8,128)S(1)}, f32[31,2048]{1,0:T(8,128)}, u32[]{:S(2)}) copy-start(f32[31,2048]{1,0:T(8,128)} %param.14) | copy-start | bytes 761860
  6.5 82.8 %all-gather.7.cloned.1.call-start = ((), (), s32[]{:S(2)}) async-start(), calls=%async_computation.4 | async-start | bytes 2359296 | tf_op jit(solution)/shard_map/all_gather | solution.py:58
  25.9 19.8 %copy-start.5 = (bf16[384,256]{1,0:T(8,128)(2,1)S(1)}, bf16[384,256]{1,0:T(8,128)(2,1)}, u32[]{:S(2)}) copy-start(bf16[384,256]{1,0:T(8,128)(2,1)} %param.10) | copy-start | bytes 589828
  25.9 138.9 %all-gather.9.cloned.1.call-start = ((), (), s32[]{:S(2)}) async-start(), calls=%async_computation.5 | async-start | bytes 4718592 | tf_op jit(solution)/shard_map/all_gather | solution.py:58
  39.4 48.7 %copy-start.2 = (f32[2048]{0:T(1024)S(1)}, f32[2048]{0:T(1024)}, u32[]{:S(2)}) copy-start(f32[2048]{0:T(1024)} %param.11) | copy-start | bytes 24580
  39.4 35.8 %all-to-all-start.1 = ((bf16[8,64,768]{2,1,0:T(8,128)(2,1)}), bf16[8,64,768]{2,1,0:T(8,128)(2,1)}, u32[]{:S(2)}, u32[]{:S(2)}) async-start(bf16[8,64,768]{2,1,0:T(8,128)(2,1)} %get-tuple-element.21), calls=%async_computation.1 | async-start | bytes 1572864 | tf_op jit(solution)/shard_map/all_to_all | solution.py:318
  57.3 30.8 %collective-permute-start = (bf16[4,384,256]{2,1,0:T(8,128)(2,1)S(1)}, bf16[4,384,256]{2,1,0:T(8,128)(2,1)S(1)}, u32[]{:S(2)}, u32[]{:S(2)}) collective-permute-start(bf16[4,384,256]{2,1,0:T(8,128)(2,1)S(1)} %bitcast.8), channel_id=1, source_target_pairs={{0,1},{1,0},{2,3},{3,2},{4,5},{5,4},{6,7},{7,6},{8,9},{9,8},{10,11... | collective-permute-start | bytes 2359304 | tf_op jit(solution)/shard_map/ppermute | solution.py:213
  75.2 28.9 %collective-permute-start.3 = (bf16[512,768]{1,0:T(8,128)(2,1)}, bf16[512,768]{1,0:T(8,128)(2,1)}, u32[]{:S(2)}, u32[]{:S(2)}) collective-permute-start(bf16[512,768]{1,0:T(8,128)(2,1)} %bitcast.4.refs_0_), channel_id=1, source_target_pairs={{448,0},{0,64},{64,128},{128,192},{192,256},{256,320},{320,384},{3... | collective-permute-start | bytes 2359304 | tf_op jit(solution)/shard_map/ppermute | solution.py:64
  78.2 25.9 %collective-permute-start.2 = (bf16[512,768]{1,0:T(8,128)(2,1)}, bf16[512,768]{1,0:T(8,128)(2,1)}, u32[]{:S(2)}, u32[]{:S(2)}) collective-permute-start(bf16[512,768]{1,0:T(8,128)(2,1)} %bitcast.4.refs_0_), channel_id=1, source_target_pairs={{128,0},{448,64},{256,128},{64,192},{384,256},{192,320},{0,384},{3... | collective-permute-start | bytes 2359304 | tf_op jit(solution)/shard_map/ppermute | solution.py:64
  86.2 30.8 %collective-permute-start.1 = (bf16[512,768]{1,0:T(8,128)(2,1)}, bf16[512,768]{1,0:T(8,128)(2,1)}, u32[]{:S(2)}, u32[]{:S(2)}) collective-permute-start(bf16[512,768]{1,0:T(8,128)(2,1)} %bitcast.4.refs_0_), channel_id=1, source_target_pairs={{64,0},{128,64},{192,128},{256,192},{320,256},{384,320},{448,384},... | collective-permute-start | bytes 2359304 | tf_op jit(solution)/shard_map/ppermute | solution.py:64
  89.3 27.7 %copy-start.3 = (f32[2048]{0:T(1024)S(1)}, f32[2048]{0:T(1024)}, u32[]{:S(2)}) copy-start(f32[2048]{0:T(1024)} %param.15) | copy-start | bytes 24580
  94.6 22.4 %all-to-all-start = ((f32[8,1,768]{2,1,0:T(1,128)}), f32[8,1,768]{2,1,0:T(1,128)S(1)}, u32[]{:S(2)}, u32[]{:S(2)}) async-start(f32[8,1,768]{2,1,0:T(1,128)} %get-tuple-element.20), calls=%async_computation | async-start | bytes 49152 | tf_op jit(solution)/shard_map/all_to_all | solution.py:328
  119.0 7.9 %collective-permute-start.4 = (bf16[4,384,256]{2,1,0:T(8,128)(2,1)S(1)}, bf16[4,384,256]{2,1,0:T(8,128)(2,1)S(1)}, u32[]{:S(2)}, u32[]{:S(2)}) collective-permute-start(bf16[4,384,256]{2,1,0:T(8,128)(2,1)S(1)} %get-tuple-element.23), channel_id=1, source_target_pairs={{0,1},{1,0},{2,3},{3,2},{4,5},{5,4},{6,7},{7,6},{8,9},{9,8},{10,11... | collective-permute-start | bytes 2359304 | tf_op jit(solution)/shard_map/ppermute | solution.py:231
  127.1 15.5 %copy-start.6 = (bf16[384,256]{1,0:T(8,128)(2,1)S(1)}, bf16[384,256]{1,0:T(8,128)(2,1)}, u32[]{:S(2)}) copy-start(bf16[384,256]{1,0:T(8,128)(2,1)} %param.10) | copy-start | bytes 589828
  142.5 20.0 %copy-start.4 = (f32[2048]{0:T(1024)S(1)}, f32[2048]{0:T(1024)}, u32[]{:S(2)}) copy-start(f32[2048]{0:T(1024)} %param.17) | copy-start | bytes 24580
  154.2 8.2 %collective-permute-start.5 = (bf16[4,384,256]{2,1,0:T(8,128)(2,1)S(1)}, bf16[4,384,256]{2,1,0:T(8,128)(2,1)S(1)}, u32[]{:S(2)}, u32[]{:S(2)}) collective-permute-start(bf16[4,384,256]{2,1,0:T(8,128)(2,1)S(1)} %bitcast.10), channel_id=1, source_target_pairs={{0,1},{1,0},{2,3},{3,2},{4,5},{5,4},{6,7},{7,6},{8,9},{9,8},{10,11... | collective-permute-start | bytes 2359304 | tf_op jit(solution)/shard_map/ppermute | solution.py:213
  163.7 1.2 copy-start.1
  171.1 4.2 %collective-permute-start.6 = (bf16[4,384,256]{2,1,0:T(8,128)(2,1)S(1)}, bf16[4,384,256]{2,1,0:T(8,128)(2,1)S(1)}, u32[]{:S(2)}, u32[]{:S(2)}) collective-permute-start(bf16[4,384,256]{2,1,0:T(8,128)(2,1)S(1)} %get-tuple-element.26), channel_id=1, source_target_pairs={{0,1},{1,0},{2,3},{3,2},{4,5},{5,4},{6,7},{7,6},{8,9},{9,8},{10,11... | collective-permute-start | bytes 2359304 | tf_op jit(solution)/shard_map/ppermute | solution.py:231
Sparse Core Ops, SparseCore 0:
  26.1 58.3 all-gather.6
  86.6 57.6 all-gather.8

commit v5 on v4

--- a/solution.py
+++ b/solution.py
@@ -165,11 +165,12 @@
     gain = gain_ref[:, pl.ds(pl.multiple_of(lax.axis_index(TP) * width, width), width)]
     values = (filtered_ref[...] - down_rows(mean)) * down_rows(scale) * gain
     activated = (values / (1.0 + jnp.exp(-values))).astype(jnp.bfloat16)
-    for copy in copies:
+    here, count = lax.axis_index("zl"), lax.axis_size("zl")
+    for turn, copy in enumerate(copies):
+        z = lax.rem(here + turn, count)
         copy.wait()
-    for out_ref, which in ((theirs_ref, 1 - core), (mine_ref, core)):
-        at = pl.ds(pl.multiple_of(which * width, width), width)
-        for z in range(held_ref.shape[0]):
+        for out_ref, which in ((theirs_ref, 1 - core), (mine_ref, core)):
+            at = pl.ds(pl.multiple_of(which * width, width), width)
             out_ref[z] = times_t(activated, held_ref[z, at]).astype(out_ref.dtype)
 
 
@@ -209,7 +210,7 @@
         out_ref[:, at] = (values * scale * gain_ref[:, at]).astype(jnp.bfloat16)
 
 
-def normed_channels(own, gain):
+def normed_channels(own, gain, vmem_mib):
     other = lax.ppermute(own, "c", SWAP)
     count, rows, width = own.shape
     part = pl.BlockSpec((count, LENGTH, width), lambda i: (0, i, 0))
@@ -222,7 +223,7 @@
         cost_estimate=pl.CostEstimate(
             flops=6 * rows * D, bytes_accessed=4 * rows * D, transcendentals=rows
         ),
-        compiler_params=pltpu.CompilerParams(vmem_limit_bytes=12 * MIB),
+        compiler_params=pltpu.CompilerParams(vmem_limit_bytes=vmem_mib * MIB),
         name="norm",
     )(own, other, gain[None])
 
@@ -323,13 +324,13 @@
     taps = lax.dynamic_slice_in_dim(conv_kernel, lax.axis_index(TP) * width, width, 1)
     own, taps = lax.optimization_barrier((own, taps))
     gates, first = over_y(gates), over_y(first)
-    normed = normed_channels(own, mix_gain)
+    normed = normed_channels(own, mix_gain, 12)
     filtered, sums = gated_filter(normed, taps, gates, width)
     sums = lax.all_to_all(sums, TP, 0, 0, tiled=True)
     theirs, mine = mixer(filtered, sums, chan_gain, slabs)
     mixed = over_group(mine, theirs)
     middle = (states.astype(jnp.float32) + mixed).astype(jnp.bfloat16)
-    normed_mid = normed_channels(lax.all_gather(middle, "x", axis=0), mlp_gain)
+    normed_mid = normed_channels(lax.all_gather(middle, "x", axis=0), mlp_gain, 56)
     theirs, mine = feed_forward(normed_mid, first, slabs)
     fed = over_group(mine, theirs)
     return (middle.astype(jnp.float32) + fed).astype(jnp.bfloat16)

time: 198 us -> 201 us (1.015)
  Pallas kernels: 18 us -> 20.8 us
    pallas_call x2, Pallas kernels: 2.44 us -> 4.94 us  [normed_channels(): pl.pallas_call(norm_kernel, grid=(rows // LENGTH,), in_specs=[part, part,...]
  transfers between devices with their start and end apart: 11 -> 11, of which waited for: 5 -> 5; matrix products, arithmetic and copies ran while one was open for 0% -> 0% of each run, Pallas kernels for 5% -> 6%
where the time goes in v5:
time: 201 us; the launch traced here: 200 us
  blocking collectives  83.6 us (42%)
  starting transfers between devices  54.2 us (27%)
  waiting for transfers between devices  25.6 us (13%)
  Pallas kernels  20.8 us (10%)
  between operations  13.6 us (7%)
    all_to_all x2, blocking collectives, over_group(): lax.all_to_all(pair, 'x', 0, 0, tiled=True).astype(jnp.float32)  29.7 us
    all_gather x1, blocking collectives, body(): gates = lax.all_gather(gates, 'zl', axis=0)  17.4 us
    ppermute x2, starting transfers between devices, normed_channels(): other = lax.ppermute(own, 'c', SWAP)  17.2 us
    all_gather x1, blocking collectives, body(): first = lax.all_gather(first, 'zl', axis=0)  13.4 us
    ppermute x3, starting transfers between devices, from_z(): return lax.ppermute(slab, ('rep', 'zl'), pairs)  12.9 us
    ppermute x3, waiting for transfers between devices, from_z(): return lax.ppermute(slab, ('rep', 'zl'), pairs)  12.8 us
    all_gather x1, blocking collectives, body(): own = lax.all_gather(states, 'x', axis=0)  11.6 us
    all_gather x1, blocking collectives, body(): lax.all_gather(middle, 'x', axis=0)  11.6 us
  transfers between devices with their start and end apart: 11, of which 5 were waited for; matrix products, arithmetic and copies ran while one was open for 0% of the time, Pallas kernels for 6%

profile of v5, /device:TPU:1, one launch (start us, length us, event | category | flops | bytes accessed | tf_op | source)
XLA Modules:
  0.0 200.1 jit_solution(1370547612798628883)
XLA Ops:
  6.5 2.0 pack.1
  8.5 17.4 %all-gather.1 = bf16[256,512]{1,0:T(8,128)(2,1)} all-gather(bf16[64,512]{1,0:T(8,128)(2,1)} %get-tuple-element.18), channel_id=3, replica_groups=mesh['rep'=2,'zl'=4,'y'=8,'x'=4,'c'=2] {'zl'}, dimensions={0}, use_global_device_ids=true | all-gather | bytes 327680 | tf_op jit(solution)/shard_map/all_gather | solution.py:320
  26.0 13.4 %all-gather.3 = bf16[256,1024]{1,0:T(8,128)(2,1)} all-gather(bf16[64,1024]{1,0:T(8,128)(2,1)} %get-tuple-element.24), channel_id=5, replica_groups=mesh['rep'=2,'zl'=4,'y'=8,'x'=4,'c'=2] {'zl'}, dimensions={0}, use_global_device_ids=true | all-gather | bytes 655360 | tf_op jit(solution)/shard_map/all_gather | solution.py:321
  39.5 6.2 %all-to-all-start.1 = ((bf16[8,64,768]{2,1,0:T(8,128)(2,1)}), bf16[8,64,768]{2,1,0:T(8,128)(2,1)}, u32[]{:S(2)}, u32[]{:S(2)}) async-start(bf16[8,64,768]{2,1,0:T(8,128)(2,1)} %get-tuple-element.21), calls=%async_computation.1 | async-start | bytes 1572864 | tf_op jit(solution)/shard_map/all_to_all | solution.py:319
  45.7 11.6 %all-gather = bf16[1536,256]{1,0:T(8,128)(2,1)S(1)} all-gather(bf16[384,256]{1,0:T(8,128)(2,1)S(1)} %copy-done.5), channel_id=2, replica_groups=mesh['rep'=2,'zl'=4,'y'=8,'x'=4,'c'=2] {'x'}, dimensions={0}, use_global_device_ids=true | all-gather | bytes 983040 | tf_op jit(solution)/shard_map/all_gather | solution.py:323
  57.3 10.8 %collective-permute-start = (bf16[4,384,256]{2,1,0:T(8,128)(2,1)S(1)}, bf16[4,384,256]{2,1,0:T(8,128)(2,1)S(1)}, u32[]{:S(2)}, u32[]{:S(2)}) collective-permute-start(bf16[4,384,256]{2,1,0:T(8,128)(2,1)S(1)} %bitcast.8), channel_id=1, source_target_pairs={{0,1},{1,0},{2,3},{3,2},{4,5},{5,4},{6,7},{7,6},{8,9},{9,8},{10,11... | collective-permute-start | bytes 2359304 | tf_op jit(solution)/shard_map/ppermute | solution.py:214
  68.1 7.1 %all-to-all-done.1 = bf16[8,64,768]{2,1,0:T(8,128)(2,1)} async-done(((bf16[8,64,768]{2,1,0:T(8,128)(2,1)}), bf16[8,64,768]{2,1,0:T(8,128)(2,1)}, u32[]{:S(2)}, u32[]{:S(2)}) %all-to-all-start.1) | async-done | bytes 786464 | tf_op jit(solution)/shard_map/all_to_all | solution.py:319
  75.2 3.0 %collective-permute-start.3 = (bf16[512,768]{1,0:T(8,128)(2,1)}, bf16[512,768]{1,0:T(8,128)(2,1)}, u32[]{:S(2)}, u32[]{:S(2)}) collective-permute-start(bf16[512,768]{1,0:T(8,128)(2,1)} %bitcast.4.refs_0_), channel_id=1, source_target_pairs={{448,0},{0,64},{64,128},{128,192},{192,256},{256,320},{320,384},{3... | collective-permute-start | bytes 2359304 | tf_op jit(solution)/shard_map/ppermute | solution.py:64
  78.2 8.0 %collective-permute-start.2 = (bf16[512,768]{1,0:T(8,128)(2,1)}, bf16[512,768]{1,0:T(8,128)(2,1)}, u32[]{:S(2)}, u32[]{:S(2)}) collective-permute-start(bf16[512,768]{1,0:T(8,128)(2,1)} %bitcast.4.refs_0_), channel_id=1, source_target_pairs={{128,0},{448,64},{256,128},{64,192},{384,256},{192,320},{0,384},{3... | collective-permute-start | bytes 2359304 | tf_op jit(solution)/shard_map/ppermute | solution.py:64
  86.2 1.9 collective-permute-start.1
  89.4 5.2 %gated_filter.1 = (f32[384,256]{1,0:T(8,128)S(1)}, f32[8,1,768]{2,1,0:T(1,128)}) custom-call(bf16[384,2048]{1,0:T(8,128)(2,1)S(1)} %norm.2.x_ref, f32[31,256]{1,0:T(8,128)S(1)} %constant_dynamic-slice_fusion.taps_ref, bf16[4,512,512]{2,1,0:T(8,128)(2,1)} %all-gather.7.cloned.1.call-done.weight_ref), custom_call_target="tpu_custom_call" | custom-call | flops 805306368 | bytes 2097152 | tf_op jit(solution)/shard_map/gated_filter/pallas_call | solution.py:121
  94.7 9.4 %all-to-all-start = ((f32[8,1,768]{2,1,0:T(1,128)}), f32[8,1,768]{2,1,0:T(1,128)S(1)}, u32[]{:S(2)}, u32[]{:S(2)}) async-start(f32[8,1,768]{2,1,0:T(1,128)} %get-tuple-element.20), calls=%async_computation | async-start | bytes 49152 | tf_op jit(solution)/shard_map/all_to_all | solution.py:329
  104.1 12.8 %collective-permute-done.1.refs_1_ = bf16[512,768]{1,0:T(8,128)(2,1)} collective-permute-done((bf16[512,768]{1,0:T(8,128)(2,1)}, bf16[512,768]{1,0:T(8,128)(2,1)}, u32[]{:S(2)}, u32[]{:S(2)}) %collective-permute-start.1) | collective-permute-done | bytes 786464 | tf_op jit(solution)/shard_map/ppermute | solution.py:64
  116.9 2.3 %mixer.1 = (bf16[4,384,256]{2,1,0:T(8,128)(2,1)S(1)}, bf16[4,384,256]{2,1,0:T(8,128)(2,1)S(1)}) custom-call(f32[384,256]{1,0:T(8,128)S(1)} %get-tuple-element.19.filtered_ref, f32[8,1,768]{2,1,0:T(1,128)S(1)} %all-to-all-done.sums_ref, f32[1,2048]{1,0:T(1,128)S(1)} %bitcast.11, bf16[512,768]{1,0:T(8,128)(2,1)} %bitcast.4.refs_0_, ...), custom_call_target="tpu_custom_call" | custom-call | flops 402653184 | bytes 1048576 | tf_op jit(solution)/shard_map/mixer/pallas_call | solution.py:181
  119.2 6.2 %collective-permute-start.4 = (bf16[4,384,256]{2,1,0:T(8,128)(2,1)S(1)}, bf16[4,384,256]{2,1,0:T(8,128)(2,1)S(1)}, u32[]{:S(2)}, u32[]{:S(2)}) collective-permute-start(bf16[4,384,256]{2,1,0:T(8,128)(2,1)S(1)} %get-tuple-element.23), channel_id=1, source_target_pairs={{0,1},{1,0},{2,3},{3,2},{4,5},{5,4},{6,7},{7,6},{8,9},{9,8},{10,11... | collective-permute-start | bytes 2359304 | tf_op jit(solution)/shard_map/ppermute | solution.py:232
  125.4 1.9 collective-permute-done.4
  127.5 15.4 %all_to_all.20 = bf16[4,384,256]{2,1,0:T(8,128)(2,1)S(1)} all-to-all(bf16[4,384,256]{2,1,0:T(8,128)(2,1)S(1)} %add_convert_fusion.1), channel_id=1, replica_groups=mesh['rep'=2,'zl'=4,'y'=8,'x'=4,'c'=2] {'x'}, dimensions={0} | all-to-all | bytes 1572864 | tf_op jit(solution)/shard_map/all_to_all | solution.py:234
  143.0 11.6 %all-gather.2 = bf16[1536,256]{1,0:T(8,128)(2,1)S(1)} all-gather(bf16[384,256]{1,0:T(8,128)(2,1)S(1)} %add_convert_fusion.3), channel_id=4, replica_groups=mesh['rep'=2,'zl'=4,'y'=8,'x'=4,'c'=2] {'x'}, dimensions={0}, use_global_device_ids=true | all-gather | bytes 983040 | tf_op jit(solution)/shard_map/all_gather | solution.py:333
  154.6 6.3 %collective-permute-start.5 = (bf16[4,384,256]{2,1,0:T(8,128)(2,1)S(1)}, bf16[4,384,256]{2,1,0:T(8,128)(2,1)S(1)}, u32[]{:S(2)}, u32[]{:S(2)}) collective-permute-start(bf16[4,384,256]{2,1,0:T(8,128)(2,1)S(1)} %bitcast.12), channel_id=1, source_target_pairs={{0,1},{1,0},{2,3},{3,2},{4,5},{5,4},{6,7},{7,6},{8,9},{9,8},{10,11... | collective-permute-start | bytes 2359304 | tf_op jit(solution)/shard_map/ppermute | solution.py:214
  163.7 3.7 %norm.3.rows_ref = bf16[384,2048]{1,0:T(8,128)(2,1)} custom-call(bf16[4,384,256]{2,1,0:T(8,128)(2,1)} %bitcast.13, bf16[4,384,256]{2,1,0:T(8,128)(2,1)} %copy-done.4, f32[1,2048]{1,0:T(1,128)} %bitcast.16), custom_call_target="tpu_custom_call" | custom-call | flops 4718592 | bytes 3145728 | tf_op jit(solution)/shard_map/norm/pallas_call | solution.py:217
  167.4 6.3 %feed_forward.1 = (bf16[4,384,256]{2,1,0:T(8,128)(2,1)S(1)}, bf16[4,384,256]{2,1,0:T(8,128)(2,1)S(1)}) custom-call(bf16[384,2048]{1,0:T(8,128)(2,1)} %norm.3.rows_ref, bf16[4,512,1024]{2,1,0:T(8,128)(2,1)} %all-gather.9.cloned.1.call-done.first_ref, bf16[512,768]{1,0:T(8,128)(2,1)} %bitcast.4.refs_0_, bf16[512,768]{1,0:T(8,128)(2,1)} %collective-permute-done.1.refs_1_, ...), custom_call_target="tpu_custom_call" | custom-call | flops 2415919104 | bytes 6291456 | tf_op jit(solution)/shard_map/feed_forward/pallas_call | solution.py:290
  173.7 2.3 %collective-permute-start.6 = (bf16[4,384,256]{2,1,0:T(8,128)(2,1)S(1)}, bf16[4,384,256]{2,1,0:T(8,128)(2,1)S(1)}, u32[]{:S(2)}, u32[]{:S(2)}) collective-permute-start(bf16[4,384,256]{2,1,0:T(8,128)(2,1)S(1)} %get-tuple-element.26), channel_id=1, source_target_pairs={{0,1},{1,0},{2,3},{3,2},{4,5},{5,4},{6,7},{7,6},{8,9},{9,8},{10,11... | collective-permute-start | bytes 2359304 | tf_op jit(solution)/shard_map/ppermute | solution.py:232
  176.0 1.9 collective-permute-done.6
  178.1 14.3 %all_to_all.21 = bf16[4,384,256]{2,1,0:T(8,128)(2,1)S(1)} all-to-all(bf16[4,384,256]{2,1,0:T(8,128)(2,1)S(1)} %add_convert_fusion), channel_id=1, replica_groups=mesh['rep'=2,'zl'=4,'y'=8,'x'=4,'c'=2] {'x'}, dimensions={0} | all-to-all | bytes 1572864 | tf_op jit(solution)/shard_map/all_to_all | solution.py:234
  (33 shorter events, 5.5 us)
Async XLA Ops:
  6.5 39.2 %copy-start = (f32[31,2048]{1,0:T(8,128)S(1)}, f32[31,2048]{1,0:T(8,128)}, u32[]{:S(2)}) copy-start(f32[31,2048]{1,0:T(8,128)} %param.14) | copy-start | bytes 761860
  6.5 82.9 %all-gather.7.cloned.1.call-start = ((), (), s32[]{:S(2)}) async-start(), calls=%async_computation.4 | async-start | bytes 2359296 | tf_op jit(solution)/shard_map/all_gather | solution.py:58
  25.9 19.8 %copy-start.5 = (bf16[384,256]{1,0:T(8,128)(2,1)S(1)}, bf16[384,256]{1,0:T(8,128)(2,1)}, u32[]{:S(2)}) copy-start(bf16[384,256]{1,0:T(8,128)(2,1)} %param.10) | copy-start | bytes 589828
  25.9 141.5 %all-gather.9.cloned.1.call-start = ((), (), s32[]{:S(2)}) async-start(), calls=%async_computation.5 | async-start | bytes 4718592 | tf_op jit(solution)/shard_map/all_gather | solution.py:58
  39.4 48.7 %copy-start.1 = (f32[2048]{0:T(1024)S(1)}, f32[2048]{0:T(1024)}, u32[]{:S(2)}) copy-start(f32[2048]{0:T(1024)} %param.11) | copy-start | bytes 24580
  39.5 35.7 %all-to-all-start.1 = ((bf16[8,64,768]{2,1,0:T(8,128)(2,1)}), bf16[8,64,768]{2,1,0:T(8,128)(2,1)}, u32[]{:S(2)}, u32[]{:S(2)}) async-start(bf16[8,64,768]{2,1,0:T(8,128)(2,1)} %get-tuple-element.21), calls=%async_computation.1 | async-start | bytes 1572864 | tf_op jit(solution)/shard_map/all_to_all | solution.py:319
  57.3 30.8 %collective-permute-start = (bf16[4,384,256]{2,1,0:T(8,128)(2,1)S(1)}, bf16[4,384,256]{2,1,0:T(8,128)(2,1)S(1)}, u32[]{:S(2)}, u32[]{:S(2)}) collective-permute-start(bf16[4,384,256]{2,1,0:T(8,128)(2,1)S(1)} %bitcast.8), channel_id=1, source_target_pairs={{0,1},{1,0},{2,3},{3,2},{4,5},{5,4},{6,7},{7,6},{8,9},{9,8},{10,11... | collective-permute-start | bytes 2359304 | tf_op jit(solution)/shard_map/ppermute | solution.py:214
  75.2 28.9 %collective-permute-start.3 = (bf16[512,768]{1,0:T(8,128)(2,1)}, bf16[512,768]{1,0:T(8,128)(2,1)}, u32[]{:S(2)}, u32[]{:S(2)}) collective-permute-start(bf16[512,768]{1,0:T(8,128)(2,1)} %bitcast.4.refs_0_), channel_id=1, source_target_pairs={{448,0},{0,64},{64,128},{128,192},{192,256},{256,320},{320,384},{3... | collective-permute-start | bytes 2359304 | tf_op jit(solution)/shard_map/ppermute | solution.py:64
  78.2 25.9 %collective-permute-start.2 = (bf16[512,768]{1,0:T(8,128)(2,1)}, bf16[512,768]{1,0:T(8,128)(2,1)}, u32[]{:S(2)}, u32[]{:S(2)}) collective-permute-start(bf16[512,768]{1,0:T(8,128)(2,1)} %bitcast.4.refs_0_), channel_id=1, source_target_pairs={{128,0},{448,64},{256,128},{64,192},{384,256},{192,320},{0,384},{3... | collective-permute-start | bytes 2359304 | tf_op jit(solution)/shard_map/ppermute | solution.py:64
  86.2 30.7 %collective-permute-start.1 = (bf16[512,768]{1,0:T(8,128)(2,1)}, bf16[512,768]{1,0:T(8,128)(2,1)}, u32[]{:S(2)}, u32[]{:S(2)}) collective-permute-start(bf16[512,768]{1,0:T(8,128)(2,1)} %bitcast.4.refs_0_), channel_id=1, source_target_pairs={{64,0},{128,64},{192,128},{256,192},{320,256},{384,320},{448,384},... | collective-permute-start | bytes 2359304 | tf_op jit(solution)/shard_map/ppermute | solution.py:64
  89.4 27.5 %copy-start.2 = (f32[2048]{0:T(1024)S(1)}, f32[2048]{0:T(1024)}, u32[]{:S(2)}) copy-start(f32[2048]{0:T(1024)} %param.15) | copy-start | bytes 24580
  94.7 22.2 %all-to-all-start = ((f32[8,1,768]{2,1,0:T(1,128)}), f32[8,1,768]{2,1,0:T(1,128)S(1)}, u32[]{:S(2)}, u32[]{:S(2)}) async-start(f32[8,1,768]{2,1,0:T(1,128)} %get-tuple-element.20), calls=%async_computation | async-start | bytes 49152 | tf_op jit(solution)/shard_map/all_to_all | solution.py:329
  119.2 8.1 %collective-permute-start.4 = (bf16[4,384,256]{2,1,0:T(8,128)(2,1)S(1)}, bf16[4,384,256]{2,1,0:T(8,128)(2,1)S(1)}, u32[]{:S(2)}, u32[]{:S(2)}) collective-permute-start(bf16[4,384,256]{2,1,0:T(8,128)(2,1)S(1)} %get-tuple-element.23), channel_id=1, source_target_pairs={{0,1},{1,0},{2,3},{3,2},{4,5},{5,4},{6,7},{7,6},{8,9},{9,8},{10,11... | collective-permute-start | bytes 2359304 | tf_op jit(solution)/shard_map/ppermute | solution.py:232
  127.5 15.5 %copy-start.6 = (bf16[384,256]{1,0:T(8,128)(2,1)S(1)}, bf16[384,256]{1,0:T(8,128)(2,1)}, u32[]{:S(2)}) copy-start(bf16[384,256]{1,0:T(8,128)(2,1)} %param.10) | copy-start | bytes 589828
  154.6 8.2 %copy-start.3 = (bf16[1536,256]{1,0:T(8,128)(2,1)}, bf16[1536,256]{1,0:T(8,128)(2,1)S(1)}, u32[]{:S(2)}) copy-start(bf16[1536,256]{1,0:T(8,128)(2,1)S(1)} %all-gather.2) | copy-start | bytes 2359300
  154.6 8.2 %collective-permute-start.5 = (bf16[4,384,256]{2,1,0:T(8,128)(2,1)S(1)}, bf16[4,384,256]{2,1,0:T(8,128)(2,1)S(1)}, u32[]{:S(2)}, u32[]{:S(2)}) collective-permute-start(bf16[4,384,256]{2,1,0:T(8,128)(2,1)S(1)} %bitcast.12), channel_id=1, source_target_pairs={{0,1},{1,0},{2,3},{3,2},{4,5},{5,4},{6,7},{7,6},{8,9},{9,8},{10,11... | collective-permute-start | bytes 2359304 | tf_op jit(solution)/shard_map/ppermute | solution.py:214
  162.8 0.9 copy-start.4
  173.7 4.2 %collective-permute-start.6 = (bf16[4,384,256]{2,1,0:T(8,128)(2,1)S(1)}, bf16[4,384,256]{2,1,0:T(8,128)(2,1)S(1)}, u32[]{:S(2)}, u32[]{:S(2)}) collective-permute-start(bf16[4,384,256]{2,1,0:T(8,128)(2,1)S(1)} %get-tuple-element.26), channel_id=1, source_target_pairs={{0,1},{1,0},{2,3},{3,2},{4,5},{5,4},{6,7},{7,6},{8,9},{9,8},{10,11... | collective-permute-start | bytes 2359304 | tf_op jit(solution)/shard_map/ppermute | solution.py:232
Sparse Core Ops, SparseCore 0:
  26.1 58.3 all-gather.6
  86.6 57.5 all-gather.8

commit v6 on v5

--- a/solution.py
+++ b/solution.py
@@ -210,7 +210,7 @@
         out_ref[:, at] = (values * scale * gain_ref[:, at]).astype(jnp.bfloat16)
 
 
-def normed_channels(own, gain, vmem_mib):
+def normed_channels(own, gain):
     other = lax.ppermute(own, "c", SWAP)
     count, rows, width = own.shape
     part = pl.BlockSpec((count, LENGTH, width), lambda i: (0, i, 0))
@@ -223,7 +223,7 @@
         cost_estimate=pl.CostEstimate(
             flops=6 * rows * D, bytes_accessed=4 * rows * D, transcendentals=rows
         ),
-        compiler_params=pltpu.CompilerParams(vmem_limit_bytes=vmem_mib * MIB),
+        compiler_params=pltpu.CompilerParams(vmem_limit_bytes=12 * MIB),
         name="norm",
     )(own, other, gain[None])
 
@@ -324,13 +324,13 @@
     taps = lax.dynamic_slice_in_dim(conv_kernel, lax.axis_index(TP) * width, width, 1)
     own, taps = lax.optimization_barrier((own, taps))
     gates, first = over_y(gates), over_y(first)
-    normed = normed_channels(own, mix_gain, 12)
+    normed = normed_channels(own, mix_gain)
     filtered, sums = gated_filter(normed, taps, gates, width)
     sums = lax.all_to_all(sums, TP, 0, 0, tiled=True)
     theirs, mine = mixer(filtered, sums, chan_gain, slabs)
     mixed = over_group(mine, theirs)
     middle = (states.astype(jnp.float32) + mixed).astype(jnp.bfloat16)
-    normed_mid = normed_channels(lax.all_gather(middle, "x", axis=0), mlp_gain, 56)
+    normed_mid = normed_channels(lax.all_gather(middle, "x", axis=0), mlp_gain)
     theirs, mine = feed_forward(normed_mid, first, slabs)
     fed = over_group(mine, theirs)
     return (middle.astype(jnp.float32) + fed).astype(jnp.bfloat16)

time: 201 us -> 199 us (0.990)
  Pallas kernels: 20.8 us -> 18.3 us
    pallas_call x2, Pallas kernels: 4.94 us -> 2.44 us  [normed_channels(): pl.pallas_call(norm_kernel, grid=(rows // LENGTH,), in_specs=[part, part,...]
  transfers between devices with their start and end apart: 11 -> 11, of which waited for: 5 -> 5; matrix products, arithmetic and copies ran while one was open for 0% -> 0% of each run, Pallas kernels for 6% -> 5%
where the time goes in v6:
time: 199 us; the launch traced here: 198 us
  blocking collectives  83.6 us (42%)
  starting transfers between devices  54.1 us (27%)
  waiting for transfers between devices  25.7 us (13%)
  Pallas kernels  18.3 us (9%)
  between operations  13.6 us (7%)
    all_to_all x2, blocking collectives, over_group(): lax.all_to_all(pair, 'x', 0, 0, tiled=True).astype(jnp.float32)  29.6 us
    all_gather x1, blocking collectives, body(): gates = lax.all_gather(gates, 'zl', axis=0)  17.4 us
    ppermute x2, starting transfers between devices, normed_channels(): other = lax.ppermute(own, 'c', SWAP)  17.2 us
    all_gather x1, blocking collectives, body(): first = lax.all_gather(first, 'zl', axis=0)  13.4 us
    ppermute x3, waiting for transfers between devices, from_z(): return lax.ppermute(slab, ('rep', 'zl'), pairs)  12.9 us
    ppermute x3, starting transfers between devices, from_z(): return lax.ppermute(slab, ('rep', 'zl'), pairs)  12.9 us
    all_gather x1, blocking collectives, body(): own = lax.all_gather(states, 'x', axis=0)  11.6 us
    all_gather x1, blocking collectives, body(): normed_mid = normed_channels(lax.all_gather(middle, 'x', axis=0), mlp_gain)  11.6 us
  transfers between devices with their start and end apart: 11, of which 5 were waited for; matrix products, arithmetic and copies ran while one was open for 0% of the time, Pallas kernels for 5%

profile of v6, /device:TPU:1, one launch (start us, length us, event | category | flops | bytes accessed | tf_op | source)
XLA Modules:
  0.0 197.8 jit_solution(7658062078457226768)
XLA Ops:
  6.5 2.0 %pack.1 = (bf16[64,512]{1,0:T(8,128)(2,1)}, bf16[64,1024]{1,0:T(8,128)(2,1)}, bf16[8,64,768]{2,1,0:T(8,128)(2,1)}) custom-call(bf16[64,256]{1,0:T(8,128)(2,1)} %value_ref.1, bf16[64,256]{1,0:T(8,128)(2,1)} %gate_ref.1, bf16[64,256]{1,0:T(8,128)(2,1)} %out_ref.1, bf16[64,768]{1,0:T(8,128)(2,1)} %up_ref.1, bf16[64,768]{1,0:T(8,128)(2,1)} %down_ref.1), custom_call_target="tpu_custom_call" | custom-call | bytes 1048576 | tf_op jit(solution)/shard_map/pack/pallas_call | solution.py:44
  8.5 17.4 %all-gather.1 = bf16[256,512]{1,0:T(8,128)(2,1)} all-gather(bf16[64,512]{1,0:T(8,128)(2,1)} %get-tuple-element.18), channel_id=3, replica_groups=mesh['rep'=2,'zl'=4,'y'=8,'x'=4,'c'=2] {'zl'}, dimensions={0}, use_global_device_ids=true | all-gather | bytes 327680 | tf_op jit(solution)/shard_map/all_gather | solution.py:320
  26.0 13.4 %all-gather.3 = bf16[256,1024]{1,0:T(8,128)(2,1)} all-gather(bf16[64,1024]{1,0:T(8,128)(2,1)} %get-tuple-element.24), channel_id=5, replica_groups=mesh['rep'=2,'zl'=4,'y'=8,'x'=4,'c'=2] {'zl'}, dimensions={0}, use_global_device_ids=true | all-gather | bytes 655360 | tf_op jit(solution)/shard_map/all_gather | solution.py:321
  39.4 6.2 %all-to-all-start.1 = ((bf16[8,64,768]{2,1,0:T(8,128)(2,1)}), bf16[8,64,768]{2,1,0:T(8,128)(2,1)}, u32[]{:S(2)}, u32[]{:S(2)}) async-start(bf16[8,64,768]{2,1,0:T(8,128)(2,1)} %get-tuple-element.21), calls=%async_computation.1 | async-start | bytes 1572864 | tf_op jit(solution)/shard_map/all_to_all | solution.py:319
  45.7 11.6 %all-gather = bf16[1536,256]{1,0:T(8,128)(2,1)S(1)} all-gather(bf16[384,256]{1,0:T(8,128)(2,1)S(1)} %copy-done.5), channel_id=2, replica_groups=mesh['rep'=2,'zl'=4,'y'=8,'x'=4,'c'=2] {'x'}, dimensions={0}, use_global_device_ids=true | all-gather | bytes 983040 | tf_op jit(solution)/shard_map/all_gather | solution.py:323
  57.3 10.8 %collective-permute-start = (bf16[4,384,256]{2,1,0:T(8,128)(2,1)S(1)}, bf16[4,384,256]{2,1,0:T(8,128)(2,1)S(1)}, u32[]{:S(2)}, u32[]{:S(2)}) collective-permute-start(bf16[4,384,256]{2,1,0:T(8,128)(2,1)S(1)} %bitcast.8), channel_id=1, source_target_pairs={{0,1},{1,0},{2,3},{3,2},{4,5},{5,4},{6,7},{7,6},{8,9},{9,8},{10,11... | collective-permute-start | bytes 2359304 | tf_op jit(solution)/shard_map/ppermute | solution.py:214
  68.1 7.1 %all-to-all-done.1 = bf16[8,64,768]{2,1,0:T(8,128)(2,1)} async-done(((bf16[8,64,768]{2,1,0:T(8,128)(2,1)}), bf16[8,64,768]{2,1,0:T(8,128)(2,1)}, u32[]{:S(2)}, u32[]{:S(2)}) %all-to-all-start.1) | async-done | bytes 786464 | tf_op jit(solution)/shard_map/all_to_all | solution.py:319
  75.2 3.0 %collective-permute-start.3 = (bf16[512,768]{1,0:T(8,128)(2,1)}, bf16[512,768]{1,0:T(8,128)(2,1)}, u32[]{:S(2)}, u32[]{:S(2)}) collective-permute-start(bf16[512,768]{1,0:T(8,128)(2,1)} %bitcast.4.refs_0_), channel_id=1, source_target_pairs={{448,0},{0,64},{64,128},{128,192},{192,256},{256,320},{320,384},{3... | collective-permute-start | bytes 2359304 | tf_op jit(solution)/shard_map/ppermute | solution.py:64
  78.2 7.9 %collective-permute-start.2 = (bf16[512,768]{1,0:T(8,128)(2,1)}, bf16[512,768]{1,0:T(8,128)(2,1)}, u32[]{:S(2)}, u32[]{:S(2)}) collective-permute-start(bf16[512,768]{1,0:T(8,128)(2,1)} %bitcast.4.refs_0_), channel_id=1, source_target_pairs={{128,0},{448,64},{256,128},{64,192},{384,256},{192,320},{0,384},{3... | collective-permute-start | bytes 2359304 | tf_op jit(solution)/shard_map/ppermute | solution.py:64
  86.2 1.9 collective-permute-start.1
  89.4 5.2 %gated_filter.1 = (f32[384,256]{1,0:T(8,128)S(1)}, f32[8,1,768]{2,1,0:T(1,128)}) custom-call(bf16[384,2048]{1,0:T(8,128)(2,1)S(1)} %norm.2.x_ref, f32[31,256]{1,0:T(8,128)S(1)} %constant_dynamic-slice_fusion.taps_ref, bf16[4,512,512]{2,1,0:T(8,128)(2,1)} %all-gather.7.cloned.1.call-done.weight_ref), custom_call_target="tpu_custom_call" | custom-call | flops 805306368 | bytes 2097152 | tf_op jit(solution)/shard_map/gated_filter/pallas_call | solution.py:121
  94.6 9.5 %all-to-all-start = ((f32[8,1,768]{2,1,0:T(1,128)}), f32[8,1,768]{2,1,0:T(1,128)S(1)}, u32[]{:S(2)}, u32[]{:S(2)}) async-start(f32[8,1,768]{2,1,0:T(1,128)} %get-tuple-element.20), calls=%async_computation | async-start | bytes 49152 | tf_op jit(solution)/shard_map/all_to_all | solution.py:329
  104.1 12.9 %collective-permute-done.1.refs_1_ = bf16[512,768]{1,0:T(8,128)(2,1)} collective-permute-done((bf16[512,768]{1,0:T(8,128)(2,1)}, bf16[512,768]{1,0:T(8,128)(2,1)}, u32[]{:S(2)}, u32[]{:S(2)}) %collective-permute-start.1) | collective-permute-done | bytes 786464 | tf_op jit(solution)/shard_map/ppermute | solution.py:64
  117.0 2.3 %mixer.1 = (bf16[4,384,256]{2,1,0:T(8,128)(2,1)S(1)}, bf16[4,384,256]{2,1,0:T(8,128)(2,1)S(1)}) custom-call(f32[384,256]{1,0:T(8,128)S(1)} %get-tuple-element.19.filtered_ref, f32[8,1,768]{2,1,0:T(1,128)S(1)} %all-to-all-done.sums_ref, f32[1,2048]{1,0:T(1,128)S(1)} %bitcast.13, bf16[512,768]{1,0:T(8,128)(2,1)} %bitcast.4.refs_0_, ...), custom_call_target="tpu_custom_call" | custom-call | flops 402653184 | bytes 1048576 | tf_op jit(solution)/shard_map/mixer/pallas_call | solution.py:181
  119.3 6.0 %collective-permute-start.4 = (bf16[4,384,256]{2,1,0:T(8,128)(2,1)S(1)}, bf16[4,384,256]{2,1,0:T(8,128)(2,1)S(1)}, u32[]{:S(2)}, u32[]{:S(2)}) collective-permute-start(bf16[4,384,256]{2,1,0:T(8,128)(2,1)S(1)} %get-tuple-element.23), channel_id=1, source_target_pairs={{0,1},{1,0},{2,3},{3,2},{4,5},{5,4},{6,7},{7,6},{8,9},{9,8},{10,11... | collective-permute-start | bytes 2359304 | tf_op jit(solution)/shard_map/ppermute | solution.py:232
  125.4 1.9 collective-permute-done.4
  127.4 15.3 %all_to_all.20 = bf16[4,384,256]{2,1,0:T(8,128)(2,1)S(1)} all-to-all(bf16[4,384,256]{2,1,0:T(8,128)(2,1)S(1)} %add_convert_fusion.1), channel_id=1, replica_groups=mesh['rep'=2,'zl'=4,'y'=8,'x'=4,'c'=2] {'x'}, dimensions={0} | all-to-all | bytes 1572864 | tf_op jit(solution)/shard_map/all_to_all | solution.py:234
  143.0 11.6 %all-gather.2 = bf16[1536,256]{1,0:T(8,128)(2,1)S(1)} all-gather(bf16[384,256]{1,0:T(8,128)(2,1)S(1)} %add_convert_fusion.3), channel_id=4, replica_groups=mesh['rep'=2,'zl'=4,'y'=8,'x'=4,'c'=2] {'x'}, dimensions={0}, use_global_device_ids=true | all-gather | bytes 983040 | tf_op jit(solution)/shard_map/all_gather | solution.py:333
  154.5 6.3 %collective-permute-start.5 = (bf16[4,384,256]{2,1,0:T(8,128)(2,1)S(1)}, bf16[4,384,256]{2,1,0:T(8,128)(2,1)S(1)}, u32[]{:S(2)}, u32[]{:S(2)}) collective-permute-start(bf16[4,384,256]{2,1,0:T(8,128)(2,1)S(1)} %bitcast.10), channel_id=1, source_target_pairs={{0,1},{1,0},{2,3},{3,2},{4,5},{5,4},{6,7},{7,6},{8,9},{9,8},{10,11... | collective-permute-start | bytes 2359304 | tf_op jit(solution)/shard_map/ppermute | solution.py:214
  160.9 1.9 collective-permute-done.5.other_ref
  165.2 6.3 %feed_forward.1 = (bf16[4,384,256]{2,1,0:T(8,128)(2,1)S(1)}, bf16[4,384,256]{2,1,0:T(8,128)(2,1)S(1)}) custom-call(bf16[384,2048]{1,0:T(8,128)(2,1)} %copy-done.1, bf16[4,512,1024]{2,1,0:T(8,128)(2,1)} %all-gather.9.cloned.1.call-done.first_ref, bf16[512,768]{1,0:T(8,128)(2,1)} %bitcast.4.refs_0_, bf16[512,768]{1,0:T(8,128)(2,1)} %collective-permute-done.1.refs_1_, ...), custom_call_target="tpu_custom_call" | custom-call | flops 2415919104 | bytes 6291456 | tf_op jit(solution)/shard_map/feed_forward/pallas_call | solution.py:290
  171.5 2.3 %collective-permute-start.6 = (bf16[4,384,256]{2,1,0:T(8,128)(2,1)S(1)}, bf16[4,384,256]{2,1,0:T(8,128)(2,1)S(1)}, u32[]{:S(2)}, u32[]{:S(2)}) collective-permute-start(bf16[4,384,256]{2,1,0:T(8,128)(2,1)S(1)} %get-tuple-element.26), channel_id=1, source_target_pairs={{0,1},{1,0},{2,3},{3,2},{4,5},{5,4},{6,7},{7,6},{8,9},{9,8},{10,11... | collective-permute-start | bytes 2359304 | tf_op jit(solution)/shard_map/ppermute | solution.py:232
  173.7 1.9 collective-permute-done.6
  175.8 14.3 %all_to_all.21 = bf16[4,384,256]{2,1,0:T(8,128)(2,1)S(1)} all-to-all(bf16[4,384,256]{2,1,0:T(8,128)(2,1)S(1)} %add_convert_fusion), channel_id=1, replica_groups=mesh['rep'=2,'zl'=4,'y'=8,'x'=4,'c'=2] {'x'}, dimensions={0} | all-to-all | bytes 1572864 | tf_op jit(solution)/shard_map/all_to_all | solution.py:234
  (33 shorter events, 5.1 us)
Async XLA Ops:
  6.5 39.2 %copy-start = (f32[31,2048]{1,0:T(8,128)S(1)}, f32[31,2048]{1,0:T(8,128)}, u32[]{:S(2)}) copy-start(f32[31,2048]{1,0:T(8,128)} %param.14) | copy-start | bytes 761860
  6.5 82.8 %all-gather.7.cloned.1.call-start = ((), (), s32[]{:S(2)}) async-start(), calls=%async_computation.4 | async-start | bytes 2359296 | tf_op jit(solution)/shard_map/all_gather | solution.py:58
  25.9 19.8 %copy-start.5 = (bf16[384,256]{1,0:T(8,128)(2,1)S(1)}, bf16[384,256]{1,0:T(8,128)(2,1)}, u32[]{:S(2)}) copy-start(bf16[384,256]{1,0:T(8,128)(2,1)} %param.10) | copy-start | bytes 589828
  25.9 139.2 %all-gather.9.cloned.1.call-start = ((), (), s32[]{:S(2)}) async-start(), calls=%async_computation.5 | async-start | bytes 4718592 | tf_op jit(solution)/shard_map/all_gather | solution.py:58
  39.4 48.7 %copy-start.2 = (f32[2048]{0:T(1024)S(1)}, f32[2048]{0:T(1024)}, u32[]{:S(2)}) copy-start(f32[2048]{0:T(1024)} %param.11) | copy-start | bytes 24580
  39.4 35.8 %all-to-all-start.1 = ((bf16[8,64,768]{2,1,0:T(8,128)(2,1)}), bf16[8,64,768]{2,1,0:T(8,128)(2,1)}, u32[]{:S(2)}, u32[]{:S(2)}) async-start(bf16[8,64,768]{2,1,0:T(8,128)(2,1)} %get-tuple-element.21), calls=%async_computation.1 | async-start | bytes 1572864 | tf_op jit(solution)/shard_map/all_to_all | solution.py:319
  57.3 30.8 %collective-permute-start = (bf16[4,384,256]{2,1,0:T(8,128)(2,1)S(1)}, bf16[4,384,256]{2,1,0:T(8,128)(2,1)S(1)}, u32[]{:S(2)}, u32[]{:S(2)}) collective-permute-start(bf16[4,384,256]{2,1,0:T(8,128)(2,1)S(1)} %bitcast.8), channel_id=1, source_target_pairs={{0,1},{1,0},{2,3},{3,2},{4,5},{5,4},{6,7},{7,6},{8,9},{9,8},{10,11... | collective-permute-start | bytes 2359304 | tf_op jit(solution)/shard_map/ppermute | solution.py:214
  75.2 28.9 %collective-permute-start.3 = (bf16[512,768]{1,0:T(8,128)(2,1)}, bf16[512,768]{1,0:T(8,128)(2,1)}, u32[]{:S(2)}, u32[]{:S(2)}) collective-permute-start(bf16[512,768]{1,0:T(8,128)(2,1)} %bitcast.4.refs_0_), channel_id=1, source_target_pairs={{448,0},{0,64},{64,128},{128,192},{192,256},{256,320},{320,384},{3... | collective-permute-start | bytes 2359304 | tf_op jit(solution)/shard_map/ppermute | solution.py:64
  78.2 25.9 %collective-permute-start.2 = (bf16[512,768]{1,0:T(8,128)(2,1)}, bf16[512,768]{1,0:T(8,128)(2,1)}, u32[]{:S(2)}, u32[]{:S(2)}) collective-permute-start(bf16[512,768]{1,0:T(8,128)(2,1)} %bitcast.4.refs_0_), channel_id=1, source_target_pairs={{128,0},{448,64},{256,128},{64,192},{384,256},{192,320},{0,384},{3... | collective-permute-start | bytes 2359304 | tf_op jit(solution)/shard_map/ppermute | solution.py:64
  86.2 30.8 %collective-permute-start.1 = (bf16[512,768]{1,0:T(8,128)(2,1)}, bf16[512,768]{1,0:T(8,128)(2,1)}, u32[]{:S(2)}, u32[]{:S(2)}) collective-permute-start(bf16[512,768]{1,0:T(8,128)(2,1)} %bitcast.4.refs_0_), channel_id=1, source_target_pairs={{64,0},{128,64},{192,128},{256,192},{320,256},{384,320},{448,384},... | collective-permute-start | bytes 2359304 | tf_op jit(solution)/shard_map/ppermute | solution.py:64
  89.3 27.7 %copy-start.3 = (f32[2048]{0:T(1024)S(1)}, f32[2048]{0:T(1024)}, u32[]{:S(2)}) copy-start(f32[2048]{0:T(1024)} %param.15) | copy-start | bytes 24580
  94.6 22.4 %all-to-all-start = ((f32[8,1,768]{2,1,0:T(1,128)}), f32[8,1,768]{2,1,0:T(1,128)S(1)}, u32[]{:S(2)}, u32[]{:S(2)}) async-start(f32[8,1,768]{2,1,0:T(1,128)} %get-tuple-element.20), calls=%async_computation | async-start | bytes 49152 | tf_op jit(solution)/shard_map/all_to_all | solution.py:329
  119.3 7.9 %collective-permute-start.4 = (bf16[4,384,256]{2,1,0:T(8,128)(2,1)S(1)}, bf16[4,384,256]{2,1,0:T(8,128)(2,1)S(1)}, u32[]{:S(2)}, u32[]{:S(2)}) collective-permute-start(bf16[4,384,256]{2,1,0:T(8,128)(2,1)S(1)} %get-tuple-element.23), channel_id=1, source_target_pairs={{0,1},{1,0},{2,3},{3,2},{4,5},{5,4},{6,7},{7,6},{8,9},{9,8},{10,11... | collective-permute-start | bytes 2359304 | tf_op jit(solution)/shard_map/ppermute | solution.py:232
  127.4 15.5 %copy-start.6 = (bf16[384,256]{1,0:T(8,128)(2,1)S(1)}, bf16[384,256]{1,0:T(8,128)(2,1)}, u32[]{:S(2)}) copy-start(bf16[384,256]{1,0:T(8,128)(2,1)} %param.10) | copy-start | bytes 589828
  142.8 20.0 %copy-start.4 = (f32[2048]{0:T(1024)S(1)}, f32[2048]{0:T(1024)}, u32[]{:S(2)}) copy-start(f32[2048]{0:T(1024)} %param.17) | copy-start | bytes 24580
  154.5 8.2 %collective-permute-start.5 = (bf16[4,384,256]{2,1,0:T(8,128)(2,1)S(1)}, bf16[4,384,256]{2,1,0:T(8,128)(2,1)S(1)}, u32[]{:S(2)}, u32[]{:S(2)}) collective-permute-start(bf16[4,384,256]{2,1,0:T(8,128)(2,1)S(1)} %bitcast.10), channel_id=1, source_target_pairs={{0,1},{1,0},{2,3},{3,2},{4,5},{5,4},{6,7},{7,6},{8,9},{9,8},{10,11... | collective-permute-start | bytes 2359304 | tf_op jit(solution)/shard_map/ppermute | solution.py:214
  164.0 1.2 copy-start.1
  171.5 4.2 %collective-permute-start.6 = (bf16[4,384,256]{2,1,0:T(8,128)(2,1)S(1)}, bf16[4,384,256]{2,1,0:T(8,128)(2,1)S(1)}, u32[]{:S(2)}, u32[]{:S(2)}) collective-permute-start(bf16[4,384,256]{2,1,0:T(8,128)(2,1)S(1)} %get-tuple-element.26), channel_id=1, source_target_pairs={{0,1},{1,0},{2,3},{3,2},{4,5},{5,4},{6,7},{7,6},{8,9},{9,8},{10,11... | collective-permute-start | bytes 2359304 | tf_op jit(solution)/shard_map/ppermute | solution.py:232
Sparse Core Ops, SparseCore 0:
  26.1 58.3 all-gather.6
  86.6 57.6 all-gather.8
